TPU v7x, 512 devices: a whole 4x8x8 slice. The times are simulated.
512 devices in a mesh: ep: 32 (over z, x), tp: 16 (over y, core).
Axes of the slice: x: 4, y: 8, z: 8, core: 2. Of those that a mesh axis runs over, the one named last changes fastest.
Arguments:
- first_batch: bfloat16 [65536, 2048], P(('ep', 'tp')), may hold values from -6 to 6
- mixer_gain: float32 [2048], replicated, may hold values from 0.1 to 1.9
- mixer_in: bfloat16 [2048, 512], P(None, 'tp'), may hold values from -0.125 to 0.125
- group_maps: bfloat16 [8, 64, 64], replicated, may hold values from -0.75 to 0.75
- pool_scale: float32 [512], replicated, may hold values from 0.1 to 1.9
- mixer_out: bfloat16 [512, 2048], P('tp'), may hold values from -0.25 to 0.25
- second_batch: bfloat16 [4096, 2048], P('ep'), may hold values from -6 to 6
- expert_gain: float32 [2048], replicated, may hold values from 0.1 to 1.9
- expert_choice: int32 [4096, 2], P('ep'), may hold values from 0 to 31, all different within a row; in each aligned block of 128 rows (0 to 127, 128 to 255, ...) at most 16 rows name the same one
- route_scores: float32 [4096, 2], P('ep'), may hold values from -6 to 6
- expert_gate: bfloat16 [32, 2048, 3584], P('ep', None, 'tp'), may hold values from -0.125 to 0.125
- expert_up: bfloat16 [32, 2048, 3584], P('ep', None, 'tp'), may hold values from -0.125 to 0.125
- expert_down: bfloat16 [32, 3584, 2048], P('ep', 'tp'), may hold values from -0.09375 to 0.09375
Outputs:
- mixed_first: bfloat16 [65536, 2048], P(('ep', 'tp'))
- experts_second: bfloat16 [4096, 2048], P('ep')
Inputs may be any that keep to these rules, and one draw needn't show every extreme that they name: `expert_choice`: the two entries of a row differ. Within the rows of one device (aligned blocks of 128 rows) no expert is named more than 16 times, a bound that some block reaches there.
All inputs are finite; a program needn't handle non-finite values.
Results may differ from a plain program's by a relative error of at most 0.018.
Values may be sent and summed in bfloat16 or wider, within the bound.
No kernel may reach another device: no remote copies, remote signals or barrier semaphores. Data moves between devices by JAX's collectives and lax.ppermute only.
A program may use at most 64 MiB of HBM per device.

v0:
```python
import jax
import jax.numpy as jnp
from jax import lax
from jax.sharding import Mesh
from jax.sharding import PartitionSpec as P

GROUP = 64
SEQS = 1
EP_TP = ("ep_0", "ep_1", "tp")
EP = ("ep_0", "ep_1")


epsilon = 1e-06


def extended(block, sides, width):
    for axis, dim in sides:
        count = lax.axis_size(axis)
        forward = [(i, i + 1) for i in range(count - 1)]
        backward = [(target, source) for source, target in forward]
        low = lax.ppermute(
            lax.slice_in_dim(block, block.shape[dim] - width, None, axis=dim), axis, forward
        )
        high = lax.ppermute(lax.slice_in_dim(block, 0, width, axis=dim), axis, backward)
        block = jnp.concatenate([low, block, high], axis=dim)
    return block


def split_up(shard, dim, peers):
    lengths = shard.shape
    blocks = shard.reshape(*lengths[:dim], peers, lengths[dim] // peers, *lengths[dim + 1 :])
    return jnp.moveaxis(blocks, dim, 0)


def summed_on_arrival(shard, axis, dim):
    peers = lax.axis_size(axis)
    blocks = lax.all_to_all(split_up(shard, dim, peers), axis, 0, 0, tiled=True)
    return jnp.sum(blocks.astype(jnp.float32), axis=0)


def laid_out(blocks, dim):
    lengths = list(blocks.shape[1:])
    lengths[dim] *= blocks.shape[0]
    return jnp.moveaxis(blocks, 0, dim).reshape(lengths)


def moved_by_axis(blocks, axes, turns):
    inside = blocks.shape[1:]
    out = blocks.reshape(*(lax.axis_size(a) for a in axes), *inside)
    for k in turns:
        out = lax.all_to_all(out, axes[k], k, k, tiled=True)
    return out.reshape(-1, *inside)


def stepwise_exchange(shard, axes, turns, split_dim, concat_dim):
    blocks = split_up(shard, split_dim, lax.axis_size(axes))
    return laid_out(moved_by_axis(blocks, axes, turns), concat_dim)


def rms_scale(values, gain):
    floats = values.astype(jnp.float32)
    factor = lax.rsqrt(jnp.mean(floats * floats, axis=-1, keepdims=True) + epsilon)
    return (floats * factor * gain).astype(jnp.bfloat16)


def mixer_half(first_batch, mixer_gain, mixer_in, group_maps, pool_scale, mixer_out):
    count_rows = first_batch.shape[0]
    normed = rms_scale(first_batch, mixer_gain)
    pooled_in = jnp.dot(
        normed,
        lax.all_gather(mixer_in, "tp", axis=1, tiled=True),
        preferred_element_type=jnp.float32,
    ).astype(jnp.bfloat16)
    channels = pooled_in.shape[1]
    padded = extended(pooled_in, ((EP_TP, 0),), 8).astype(jnp.float32)
    devices = lax.axis_size(EP) * lax.axis_size("tp")
    seq_length = count_rows * devices // SEQS
    first_row = (lax.axis_index(EP) * lax.axis_size("tp") + lax.axis_index("tp")) * count_rows
    places = first_row + jnp.arange(count_rows, dtype=jnp.int32)
    own_seq = places // seq_length
    group_of = jnp.arange(channels, dtype=jnp.int32) // GROUP
    half_span = jnp.left_shift(jnp.ones_like(group_of), group_of % 4)
    window_sum = jnp.zeros((count_rows, channels), jnp.float32)
    window_count = jnp.zeros((count_rows, channels), jnp.float32)
    for offset in range(-8, 8):
        inside = (
            ((places + offset) // seq_length == own_seq)[:, None]
            & (offset >= -half_span)[None, :]
            & (offset < half_span)[None, :]
        )
        window_sum = window_sum + jnp.where(
            inside, padded[8 + offset : 8 + offset + count_rows], 0.0
        )
        window_count = window_count + inside.astype(jnp.float32)
    centred = (window_sum / window_count - padded[8 : 8 + count_rows]).astype(jnp.bfloat16)
    group_count = group_maps.shape[0]
    identity = jnp.eye(group_count, dtype=jnp.bfloat16)
    block_map = jnp.einsum("gcd,gh->gchd", group_maps, identity).reshape(channels, channels)
    grouped = (jnp.dot(centred, block_map, preferred_element_type=jnp.float32) * pool_scale).astype(
        jnp.bfloat16
    )
    mixed_out = jnp.dot(
        grouped,
        lax.all_gather(mixer_out, "tp", axis=0, tiled=True),
        preferred_element_type=jnp.float32,
    )
    return mixed_out.astype(jnp.bfloat16)


def expert_half(
    second_batch, expert_gain, expert_choice, route_scores, expert_gate, expert_up, expert_down
):
    row_count = second_batch.shape[0]
    model_width = second_batch.shape[1]
    experts = lax.axis_size(EP)
    tp_count = lax.axis_size("tp")
    capacity = 4 * row_count // experts
    share = capacity // tp_count
    normed = rms_scale(second_batch, expert_gain)
    chosen = expert_choice.reshape(-1)
    one_hot = (chosen[:, None] == jnp.arange(experts, dtype=jnp.int32)[None, :]).astype(jnp.int32)
    ranking = jnp.sum(jnp.cumsum(one_hot, axis=0) * one_hot, axis=1) - 1
    slot_place = ranking * experts + chosen
    source_row = jnp.arange(chosen.shape[0], dtype=jnp.int32) // expert_choice.shape[1]
    slot_table = jnp.zeros((capacity * experts,), jnp.int32).at[slot_place].set(source_row + 1)
    outgoing = jnp.where(
        (slot_table > 0)[:, None],
        normed[jnp.maximum(slot_table - 1, 0)],
        jnp.zeros((), jnp.bfloat16),
    )
    outgoing = outgoing.reshape(capacity, experts, model_width)
    arrived = lax.all_to_all(outgoing, EP, split_axis=1, concat_axis=1, tiled=True)
    incoming = arrived.reshape(capacity * experts, model_width)
    gate_weight = expert_gate[0]
    up_weight = expert_up[0]
    down_weight = expert_down[0]
    gate_part = jnp.dot(incoming, gate_weight, preferred_element_type=jnp.float32)
    up_part = jnp.dot(incoming, up_weight, preferred_element_type=jnp.float32)
    hidden = (jax.nn.silu(gate_part) * up_part).astype(jnp.bfloat16)
    summed = summed_on_arrival(
        jnp.dot(hidden, down_weight, preferred_element_type=jnp.float32).astype(jnp.bfloat16),
        "tp",
        0,
    )
    finished = summed.astype(jnp.bfloat16).reshape(share, experts, model_width)
    returned = stepwise_exchange(finished, EP, (0, 1), 1, 1)
    every_slot = lax.all_gather(returned, "tp", axis=0, tiled=True).reshape(
        capacity * experts, model_width
    )
    picked = every_slot[slot_place].reshape(row_count, -1, model_width)
    weight_first = jax.nn.sigmoid(route_scores[:, 0] - route_scores[:, 1])[:, None]
    blended = weight_first * picked[:, 0].astype(jnp.float32) + (1.0 - weight_first) * picked[
        :, 1
    ].astype(jnp.float32)
    return blended.astype(jnp.bfloat16)


def per_device(
    first_batch,
    mixer_gain,
    mixer_in,
    group_maps,
    pool_scale,
    mixer_out,
    second_batch,
    expert_gain,
    expert_choice,
    route_scores,
    expert_gate,
    expert_up,
    expert_down,
):
    mixed_first = mixer_half(first_batch, mixer_gain, mixer_in, group_maps, pool_scale, mixer_out)
    experts_second = expert_half(
        second_batch, expert_gain, expert_choice, route_scores, expert_gate, expert_up, expert_down
    )
    return (mixed_first, experts_second)


def solution(mesh):
    torus = Mesh(mesh.devices.reshape(8, 4, mesh.shape["tp"]), ("ep_0", "ep_1", "tp"))
    placed = (
        P(EP_TP, None),
        P(),
        P(None, "tp"),
        P(),
        P(),
        P("tp", None),
        P(EP, None),
        P(),
        P(EP, None),
        P(EP, None),
        P(EP, None, "tp"),
        P(EP, None, "tp"),
        P(EP, "tp", None),
    )
    return jax.shard_map(
        per_device,
        mesh=torus,
        in_specs=placed,
        out_specs=(P(EP_TP, None), P(EP, None)),
        check_vma=False,
    )
```

profile of v0, /device:TPU:1, one launch (start us, length us, event | category | flops | bytes accessed | tf_op | source)
XLA Modules:
  0.0 232.5 jit_solution(14111558558822395541)
XLA Ops:
  9.4 1.4 scatter_custom_fusion
  10.9 1.2 fusion.5
  12.3 1.2 fusion.7
  13.5 2.5 %gather_fusion = bf16[512,2048]{1,0:T(8,128)(2,1)S(1)} fusion(bf16[128,2048]{1,0:T(8,128)(2,1)S(1)} %fusion.7, s32[1024]{0:T(1024)S(1)} %pad_clamp_fusion.1), kind=kCustom, calls=%fused_computation | custom fusion | bytes 4196352 | tf_op jit(solution)/shard_map/gather | solution.py:128
  16.0 3.8 %copy_select_fusion = bf16[16,32,2048]{2,0,1:T(8,128)(2,1)} fusion(bf16[16,32,2048]{2,1,0:T(8,128)(2,1)S(1)} %bitcast.56, pred[16,32]{0,1:T(8,128)(4,1)S(1)} %copy.35), kind=kLoop, calls=%fused_computation.5 | loop fusion | flops 1048576 | bytes 4194816 | tf_op jit(solution)/shard_map/jit(_where)/select_n | solution.py:126
  19.8 13.7 %all-to-all-start = ((bf16[16,32,2048]{2,0,1:T(8,128)(2,1)}), bf16[16,32,2048]{2,0,1:T(8,128)(2,1)S(1)}, u32[]{:S(2)}, u32[]{:S(2)}) async-start(bf16[16,32,2048]{2,0,1:T(8,128)(2,1)} %copy_select_fusion), calls=%async_computation | async-start | bytes 4194304 | tf_op jit(solution)/shard_map/all_to_all | solution.py:132
  34.2 47.7 %all-to-all-done = bf16[16,32,2048]{2,0,1:T(8,128)(2,1)S(1)} async-done(((bf16[16,32,2048]{2,0,1:T(8,128)(2,1)}), bf16[16,32,2048]{2,0,1:T(8,128)(2,1)S(1)}, u32[]{:S(2)}, u32[]{:S(2)}) %all-to-all-start) | async-done | bytes 2097184 | tf_op jit(solution)/shard_map/all_to_all | solution.py:132
  83.1 1.3 copy-done.1
  85.6 4.5 %convolution_convert_fusion = bf16[512,2048]{1,0:T(8,128)(2,1)} fusion(bf16[512,2048]{1,0:T(8,128)(2,1)} %bitcast.59, bf16[1,224,2048]{2,1,0:T(8,128)(2,1)S(1)} %copy-done, bf16[1,2048,224]{1,2,0:T(8,128)(2,1)S(1)} %copy-done.6, f32[512,224]{0,1:T(8,128)S(1)} %fusion.13), kind=kOutput, calls=%fused_computation.3 | convolution fusion | flops 941260800 | bytes 6488064 | tf_op jit(solution)/shard_map/dot_general | solution.py:141
  90.1 9.8 %all-to-all-start.1 = ((bf16[16,32,2048]{2,1,0:T(8,128)(2,1)}), bf16[16,32,2048]{2,1,0:T(8,128)(2,1)S(1)}, u32[]{:S(2)}, u32[]{:S(2)}) async-start(bf16[16,32,2048]{2,1,0:T(8,128)(2,1)} %bitcast.57), calls=%async_computation.1 | async-start | bytes 4194304 | tf_op jit(solution)/shard_map/all_to_all | solution.py:37
  100.8 56.7 %all-to-all-done.1 = bf16[16,32,2048]{2,1,0:T(8,128)(2,1)S(1)} async-done(((bf16[16,32,2048]{2,1,0:T(8,128)(2,1)}), bf16[16,32,2048]{2,1,0:T(8,128)(2,1)S(1)}, u32[]{:S(2)}, u32[]{:S(2)}) %all-to-all-start.1) | async-done | bytes 2097184 | tf_op jit(solution)/shard_map/all_to_all | solution.py:37
  158.6 3.7 %all-to-all-start.2 = ((bf16[8,4,1,1,2048]{4,1,3,2,0:T(4,128)(2,1)}), bf16[8,4,1,1,2048]{4,1,3,2,0:T(4,128)(2,1)S(1)}, u32[]{:S(2)}, u32[]{:S(2)}) async-start(bf16[8,4,1,1,2048]{4,1,3,2,0:T(4,128)(2,1)} %reshape_transpose_reshape_reshape.3), calls=%async_computation.2 | async-start | bytes 262144 | tf_op jit(solution)/shard_map/all_to_all | solution.py:51
  162.4 7.9 %all-to-all-done.2 = bf16[8,4,1,1,2048]{4,1,3,2,0:T(4,128)(2,1)S(1)} async-done(((bf16[8,4,1,1,2048]{4,1,3,2,0:T(4,128)(2,1)}), bf16[8,4,1,1,2048]{4,1,3,2,0:T(4,128)(2,1)S(1)}, u32[]{:S(2)}, u32[]{:S(2)}) %all-to-all-start.2) | async-done | bytes 131104 | tf_op jit(solution)/shard_map/all_to_all | solution.py:51
  171.0 3.5 %all-to-all-start.3 = ((bf16[8,4,1,1,2048]{4,0,3,2,1:T(8,128)(2,1)}), bf16[8,4,1,1,2048]{4,0,3,2,1:T(8,128)(2,1)S(1)}, u32[]{:S(2)}, u32[]{:S(2)}) async-start(bf16[8,4,1,1,2048]{4,0,3,2,1:T(8,128)(2,1)} %copy.38), calls=%async_computation.3 | async-start | bytes 262144 | tf_op jit(solution)/shard_map/all_to_all | solution.py:51
  174.6 4.7 %all-to-all-done.3 = bf16[8,4,1,1,2048]{4,0,3,2,1:T(8,128)(2,1)S(1)} async-done(((bf16[8,4,1,1,2048]{4,0,3,2,1:T(8,128)(2,1)}), bf16[8,4,1,1,2048]{4,0,3,2,1:T(8,128)(2,1)S(1)}, u32[]{:S(2)}, u32[]{:S(2)}) %all-to-all-start.3) | async-done | bytes 131104 | tf_op jit(solution)/shard_map/all_to_all | solution.py:51
  180.8 2.4 %convolution_convert_fusion.2 = bf16[128,512]{1,0:T(8,128)(2,1)S(1)} fusion(bf16[2048,512]{0,1:T(8,128)(2,1)} %all-gather.4.cloned.1.call-done, bf16[128,2048]{1,0:T(8,128)(2,1)S(1)} %copy-done.2, f32[2048]{0:T(1024)S(1)} %copy-done.7, f32[128]{0:T(128)S(1)} %add_rsqrt_fusion.1), kind=kOutput, calls=%fused_computation.14 | convolution fusion | flops 269549568 | bytes 2761216 | tf_op jit(solution)/shard_map/dot_general | solution.py:69
  183.3 6.1 %collective-permute-start = (bf16[8,512]{1,0:T(8,128)(2,1)S(1)}, bf16[8,512]{1,0:T(8,128)(2,1)S(1)}, u32[]{:S(2)}, u32[]{:S(2)}) collective-permute-start(bf16[8,512]{1,0:T(8,128)(2,1)S(1)} %get-tuple-element.6), channel_id=1, source_target_pairs={{0,1},{1,2},{2,3},{3,4},{4,5},{5,6},{6,7},{7,8},{8,9},{9,10},{10,1... | collective-permute-start | bytes 24584 | tf_op jit(solution)/shard_map/ppermute | solution.py:21
  189.4 1.9 collective-permute-start.1
  192.0 2.5 %collective-permute-done.1 = bf16[8,512]{1,0:T(8,128)(2,1)S(1)} collective-permute-done((bf16[8,512]{1,0:T(8,128)(2,1)S(1)}, bf16[8,512]{1,0:T(8,128)(2,1)S(1)}, u32[]{:S(2)}, u32[]{:S(2)}) %collective-permute-start.1) | collective-permute-done | bytes 8224 | tf_op jit(solution)/shard_map/ppermute | solution.py:24
  194.5 4.2 %convolution_convert_fusion.1 = bf16[128,2048]{1,0:T(8,128)(2,1)} fusion(bf16[512,2048]{1,0:T(8,128)(2,1)} %all-gather.6.cloned.1.call-done, bf16[512,512]{1,0:T(8,128)(2,1)S(1)} %reshape.526, f32[144,512]{1,0:T(8,128)S(1)} %maximum_convert_fusion, f32[512]{0:T(512)S(1)} %copy-done.8, f32[512]{0:T(512)S(1)} %get-tuple-element.53, ...), kind=kOutput, calls=%fused_computation.4 | convolution fusion | flops 342097920 | bytes 7367680 | tf_op jit(solution)/shard_map/dot_general | solution.py:102
  198.8 18.9 %all-gather.8.cloned.1.call-done = bf16[16,32,2048]{2,1,0:T(8,128)(2,1)} async-done(((bf16[1,32,2048]{2,1,0:T(8,128)(2,1)}), bf16[16,32,2048]{2,1,0:T(8,128)(2,1)}) %all-gather.8.cloned.1.call-update) | async-done | bytes 2097168 | tf_op jit(solution)/shard_map/all_gather | solution.py:147
  217.7 4.2 %gather_fusion.1 = bf16[256,2048]{1,0:T(8,128)(2,1)S(1)} fusion(bf16[512,2048]{1,0:T(8,128)(2,1)} %bitcast.55, s32[1024]{0:T(1024)S(1)} %pad_clamp_fusion), kind=kCustom, calls=%fused_computation.1 | custom fusion | bytes 2098176 | tf_op jit(solution)/shard_map/gather | solution.py:150
  222.7 1.5 fusion.173
  224.2 1.8 fusion.9
  (86 shorter events, 11.0 us)
Async XLA Ops:
  7.2 78.1 %copy-start = (bf16[1,224,2048]{2,1,0:T(8,128)(2,1)S(1)}, bf16[1,224,2048]{2,1,0:T(8,128)(2,1)}, u32[]{:S(2)}) copy-start(bf16[1,224,2048]{2,1,0:T(8,128)(2,1)} %param.25) | copy-start | bytes 2752516
  19.8 62.2 %all-to-all-start = ((bf16[16,32,2048]{2,0,1:T(8,128)(2,1)}), bf16[16,32,2048]{2,0,1:T(8,128)(2,1)S(1)}, u32[]{:S(2)}, u32[]{:S(2)}) async-start(bf16[16,32,2048]{2,0,1:T(8,128)(2,1)} %copy_select_fusion), calls=%async_computation | async-start | bytes 4194304 | tf_op jit(solution)/shard_map/all_to_all | solution.py:132
  33.5 147.3 %all-gather.4.cloned.1.call-start = ((), (), s32[]{:S(2)}) async-start(), calls=%async_computation.4 | async-start | bytes 2228224 | tf_op jit(solution)/shard_map/all_gather | solution.py:71
  82.0 2.5 %copy-start.5 = (bf16[1,2048,224]{1,2,0:T(8,128)(2,1)S(1)}, bf16[1,2048,224]{1,2,0:T(8,128)(2,1)}, u32[]{:S(2)}) copy-start(bf16[1,2048,224]{1,2,0:T(8,128)(2,1)} %param.23) | copy-start | bytes 2752516
  83.1 1.3 copy-start.1
  84.5 1.2 copy-start.6
  90.1 67.3 %all-to-all-start.1 = ((bf16[16,32,2048]{2,1,0:T(8,128)(2,1)}), bf16[16,32,2048]{2,1,0:T(8,128)(2,1)S(1)}, u32[]{:S(2)}, u32[]{:S(2)}) async-start(bf16[16,32,2048]{2,1,0:T(8,128)(2,1)} %bitcast.57), calls=%async_computation.1 | async-start | bytes 4194304 | tf_op jit(solution)/shard_map/all_to_all | solution.py:37
  99.9 94.6 %all-gather.6.cloned.1.call-start = ((), (), s32[]{:S(2)}) async-start(), calls=%async_computation.5 | async-start | bytes 2228224 | tf_op jit(solution)/shard_map/all_gather | solution.py:104
  100.7 79.8 %copy-start.4 = (f32[128,2]{0,1:T(2,128)S(1)}, f32[128,2]{0,1:T(2,128)}, u32[]{:S(2)}) copy-start(f32[128,2]{0,1:T(2,128)} %param.22) | copy-start | bytes 3076
  100.8 79.8 %copy-start.3 = (bf16[8,64,64]{2,1,0:T(8,128)(2,1)S(1)}, bf16[8,64,64]{2,1,0:T(8,128)(2,1)}, u32[]{:S(2)}) copy-start(bf16[8,64,64]{2,1,0:T(8,128)(2,1)} %param.16) | copy-start | bytes 196612
  157.9 22.5 %copy-start.2 = (bf16[128,2048]{1,0:T(8,128)(2,1)S(1)}, bf16[128,2048]{1,0:T(8,128)(2,1)}, u32[]{:S(2)}) copy-start(bf16[128,2048]{1,0:T(8,128)(2,1)} %param.13) | copy-start | bytes 1572868
  157.9 22.9 %copy-start.7 = (f32[2048]{0:T(1024)S(1)}, f32[2048]{0:T(1024)}, u32[]{:S(2)}) copy-start(f32[2048]{0:T(1024)} %param.14) | copy-start | bytes 24580
  158.6 11.6 %all-to-all-start.2 = ((bf16[8,4,1,1,2048]{4,1,3,2,0:T(4,128)(2,1)}), bf16[8,4,1,1,2048]{4,1,3,2,0:T(4,128)(2,1)S(1)}, u32[]{:S(2)}, u32[]{:S(2)}) async-start(bf16[8,4,1,1,2048]{4,1,3,2,0:T(4,128)(2,1)} %reshape_transpose_reshape_reshape.3), calls=%async_computation.2 | async-start | bytes 262144 | tf_op jit(solution)/shard_map/all_to_all | solution.py:51
  171.0 8.3 %all-to-all-start.3 = ((bf16[8,4,1,1,2048]{4,0,3,2,1:T(8,128)(2,1)}), bf16[8,4,1,1,2048]{4,0,3,2,1:T(8,128)(2,1)S(1)}, u32[]{:S(2)}, u32[]{:S(2)}) async-start(bf16[8,4,1,1,2048]{4,0,3,2,1:T(8,128)(2,1)} %copy.38), calls=%async_computation.3 | async-start | bytes 262144 | tf_op jit(solution)/shard_map/all_to_all | solution.py:51
  174.5 43.2 %all-gather.8.cloned.1.call-start = ((), (), s32[]{:S(2)}) async-start(), calls=%async_computation.6 | async-start | bytes 2228224 | tf_op jit(solution)/shard_map/all_gather | solution.py:147
  180.8 13.8 %copy-start.8 = (f32[512]{0:T(512)S(1)}, f32[512]{0:T(512)}, u32[]{:S(2)}) copy-start(f32[512]{0:T(512)} %param.17) | copy-start | bytes 6148
  183.3 8.7 %collective-permute-start = (bf16[8,512]{1,0:T(8,128)(2,1)S(1)}, bf16[8,512]{1,0:T(8,128)(2,1)S(1)}, u32[]{:S(2)}, u32[]{:S(2)}) collective-permute-start(bf16[8,512]{1,0:T(8,128)(2,1)S(1)} %get-tuple-element.6), channel_id=1, source_target_pairs={{0,1},{1,2},{2,3},{3,4},{4,5},{5,6},{6,7},{7,8},{8,9},{9,10},{10,1... | collective-permute-start | bytes 24584 | tf_op jit(solution)/shard_map/ppermute | solution.py:21
  189.4 5.1 %collective-permute-start.1 = (bf16[8,512]{1,0:T(8,128)(2,1)S(1)}, bf16[8,512]{1,0:T(8,128)(2,1)S(1)}, u32[]{:S(2)}, u32[]{:S(2)}) collective-permute-start(bf16[8,512]{1,0:T(8,128)(2,1)S(1)} %get-tuple-element.7), channel_id=1, source_target_pairs={{1,0},{2,1},{3,2},{4,3},{5,4},{6,5},{7,6},{8,7},{9,8},{10,9},{11,1... | collective-permute-start | bytes 24584 | tf_op jit(solution)/shard_map/ppermute | solution.py:24
Sparse Core Ops, SparseCore 0:
  36.4 43.6 all-gather.3
  102.8 57.5 all-gather.5
  180.2 37.4 all-gather.7
where the time goes:
time: 233 us; the launch traced here: 232 us
  waiting for transfers between devices  140 us (60%)
  starting transfers between devices  38.8 us (17%)
  local copies, waits for them, and re-layouts  17.7 us (8%)
  between operations  14.2 us (6%)
  matrix products  12 us (5%)
  other arithmetic  9.87 us (4%)
    all_to_all x1, waiting for transfers between devices, summed_on_arrival(): blocks = lax.all_to_all(split_up(shard, dim, peers), axis, 0, 0, tiled=True)  56.7 us
    all_to_all x1, waiting for transfers between devices, expert_half(): lax.all_to_all(outgoing, EP, split_axis=1, concat_axis=1, tiled=True)  47.7 us
    all_gather x1, waiting for transfers between devices, expert_half(): lax.all_gather(returned, 'tp', axis=0, tiled=True)  18.9 us
    all_to_all x1, starting transfers between devices, expert_half(): lax.all_to_all(outgoing, EP, split_axis=1, concat_axis=1, tiled=True)  13.7 us
    all_to_all x2, waiting for transfers between devices, moved_by_axis(): out = lax.all_to_all(out, axes[k], k, k, tiled=True)  12.6 us
    all_to_all x1, starting transfers between devices, summed_on_arrival(): blocks = lax.all_to_all(split_up(shard, dim, peers), axis, 0, 0, tiled=True)  9.75 us
    all_to_all x2, starting transfers between devices, moved_by_axis(): out = lax.all_to_all(out, axes[k], k, k, tiled=True)  7.19 us
    ppermute x1, starting transfers between devices, extended(): lax.ppermute(lax.slice_in_dim(block, block.shape[dim] - width, None, axis...  6.09 us
  transfers between devices with their start and end apart: 9, of which 6 were waited for; matrix products, arithmetic and copies ran while one was open for 7% of the time, Pallas kernels for 0%

commit v1 on v0

v1 whole, which is shorter than its diff:
```python
import jax
import jax.numpy as jnp
from jax import lax
from jax.sharding import Mesh
from jax.sharding import PartitionSpec as P

GROUP = 64
SEQS = 1
ALL = ("z", "x", "y", "c")
EP = ("z", "x")
TP = ("y", "c")
SWAP = [(0, 1), (1, 0)]

epsilon = 1e-06


def rms_scale(values, gain):
    floats = values.astype(jnp.float32)
    factor = lax.rsqrt(jnp.mean(floats * floats, axis=-1, keepdims=True) + epsilon)
    return (floats * factor * gain).astype(jnp.bfloat16)


def extended(block, width):
    count = lax.axis_size(ALL)
    forward = [(i, i + 1) for i in range(count - 1)]
    backward = [(target, source) for source, target in forward]
    low = lax.ppermute(block[block.shape[0] - width :], ALL, forward)
    high = lax.ppermute(block[:width], ALL, backward)
    return jnp.concatenate([low, block, high], axis=0)


def mixer_half(first_batch, mixer_gain, mixer_in, group_maps, pool_scale, mixer_out):
    count_rows = first_batch.shape[0]
    share = mixer_out.shape[0]
    both = jnp.concatenate([mixer_in.T, mixer_out], axis=0)
    gathered = lax.all_gather(both, TP)
    width = gathered.shape[2]
    in_rows = gathered[:, :share].reshape(-1, width)
    out_rows = gathered[:, share:].reshape(-1, width)
    normed = rms_scale(first_batch, mixer_gain)
    pooled_in = lax.dot_general(
        normed, in_rows, (((1,), (1,)), ((), ())), preferred_element_type=jnp.float32
    ).astype(jnp.bfloat16)
    channels = pooled_in.shape[1]
    padded = extended(pooled_in, 8).astype(jnp.float32)
    devices = lax.axis_size(ALL)
    seq_length = count_rows * devices // SEQS
    first_row = lax.axis_index(ALL) * count_rows
    places = first_row + jnp.arange(count_rows, dtype=jnp.int32)
    own_seq = places // seq_length
    group_of = jnp.arange(channels, dtype=jnp.int32) // GROUP
    half_span = jnp.left_shift(jnp.ones_like(group_of), group_of % 4)
    window_sum = jnp.zeros((count_rows, channels), jnp.float32)
    window_count = jnp.zeros((count_rows, channels), jnp.float32)
    for offset in range(-8, 8):
        inside = (
            ((places + offset) // seq_length == own_seq)[:, None]
            & (offset >= -half_span)[None, :]
            & (offset < half_span)[None, :]
        )
        window_sum = window_sum + jnp.where(
            inside, padded[8 + offset : 8 + offset + count_rows], 0.0
        )
        window_count = window_count + inside.astype(jnp.float32)
    centred = (window_sum / window_count - padded[8 : 8 + count_rows]).astype(jnp.bfloat16)
    group_count = group_maps.shape[0]
    identity = jnp.eye(group_count, dtype=jnp.bfloat16)
    block_map = jnp.einsum("gcd,gh->gchd", group_maps, identity).reshape(channels, channels)
    grouped = (jnp.dot(centred, block_map, preferred_element_type=jnp.float32) * pool_scale).astype(
        jnp.bfloat16
    )
    mixed_out = jnp.dot(grouped, out_rows, preferred_element_type=jnp.float32)
    return mixed_out.astype(jnp.bfloat16)


def dot(left, right):
    return jnp.dot(left, right, preferred_element_type=jnp.float32)


def expert_half(
    second_batch, expert_gain, expert_choice, route_scores, expert_gate, expert_up, expert_down
):
    row_count, model_width = second_batch.shape
    experts = lax.axis_size(EP)
    capacity = 4 * row_count // experts
    half_slots = capacity // 2
    half_width = model_width // 2
    core = lax.axis_index("c")

    gate_own, up_own, down_own = expert_gate[0], expert_up[0], expert_down[0]
    gate_far = lax.ppermute(gate_own, "c", SWAP)
    up_far = lax.ppermute(up_own, "c", SWAP)
    down_far = lax.ppermute(down_own, "c", SWAP)

    normed = rms_scale(second_batch, expert_gain)
    expert_ids = jnp.arange(experts, dtype=jnp.int32)
    first_t = expert_choice[:, 0][None, :] == expert_ids[:, None]
    second_t = expert_choice[:, 1][None, :] == expert_ids[:, None]
    named_t = first_t | second_t
    rows = jnp.arange(row_count, dtype=jnp.int32)
    earlier_t = (rows[:, None] < rows[None, :]).astype(jnp.bfloat16)
    rank_t = dot(named_t.astype(jnp.bfloat16), earlier_t).astype(jnp.int32)
    rank_t = jnp.where(named_t, rank_t, -1)

    own_slots = core * half_slots + jnp.arange(half_slots, dtype=jnp.int32)
    spread = (rank_t[:, None, :] == own_slots[None, :, None]).astype(jnp.bfloat16)
    outgoing = dot(spread.reshape(experts * half_slots, row_count), normed).astype(jnp.bfloat16)
    outgoing = outgoing.reshape(experts, half_slots, model_width)
    arrived = lax.all_to_all(outgoing, EP, 0, 0, tiled=True)
    incoming = arrived.reshape(experts * half_slots, model_width)

    def hidden_units(gate, up):
        return (jax.nn.silu(dot(incoming, gate)) * dot(incoming, up)).astype(jnp.bfloat16)

    partial = dot(hidden_units(gate_own, up_own), down_own) + dot(
        hidden_units(gate_far, up_far), down_far
    )
    partial = partial.astype(jnp.bfloat16).reshape(experts, half_slots, 2, half_width)
    leaving = jnp.moveaxis(partial, 2, 1).reshape(2 * experts, half_slots, half_width)
    returned = lax.all_to_all(leaving, EP + ("c",), 0, 0, tiled=True)
    returned = returned.reshape(experts * capacity, half_width)

    weight_first = jax.nn.sigmoid(route_scores[:, 0] - route_scores[:, 1])[None, :]
    weight_t = jnp.where(first_t, weight_first, jnp.where(second_t, 1.0 - weight_first, 0.0))
    slots = jnp.arange(capacity, dtype=jnp.int32)
    blend_t = jnp.where(
        rank_t[:, None, :] == slots[None, :, None], weight_t[:, None, :], 0.0
    ).reshape(experts * capacity, row_count)
    high = lax.reduce_precision(blend_t, 8, 7)
    low = blend_t - high
    both = jnp.concatenate([high, low], axis=1).astype(jnp.bfloat16)
    mixed = lax.dot_general(
        both, returned, (((0,), (0,)), ((), ())), preferred_element_type=jnp.float32
    )
    blended = (mixed[:row_count] + mixed[row_count:]).astype(jnp.bfloat16)

    ring = lax.axis_size("y")
    piece = half_width // ring
    blocks = jnp.moveaxis(blended.reshape(row_count, ring, piece), 1, 0)
    pieces = lax.all_to_all(blocks, "y", 0, 0, tiled=True)
    final = jnp.sum(pieces.astype(jnp.float32), axis=0).astype(jnp.bfloat16)
    whole = lax.all_gather(final, TP)
    whole = whole.reshape(ring, 2, row_count, piece)
    return jnp.transpose(whole, (2, 1, 0, 3)).reshape(row_count, model_width)


def per_device(
    first_batch,
    mixer_gain,
    mixer_in,
    group_maps,
    pool_scale,
    mixer_out,
    second_batch,
    expert_gain,
    expert_choice,
    route_scores,
    expert_gate,
    expert_up,
    expert_down,
):
    experts_second = expert_half(
        second_batch, expert_gain, expert_choice, route_scores, expert_gate, expert_up, expert_down
    )
    mixed_first = mixer_half(first_batch, mixer_gain, mixer_in, group_maps, pool_scale, mixer_out)
    return (mixed_first, experts_second)


def solution(mesh):
    torus = Mesh(mesh.devices.reshape(8, 4, mesh.shape["tp"] // 2, 2), ALL)
    placed = (
        P(ALL, None),
        P(),
        P(None, TP),
        P(),
        P(),
        P(TP, None),
        P(EP, None),
        P(),
        P(EP, None),
        P(EP, None),
        P(EP, None, TP),
        P(EP, None, TP),
        P(EP, TP, None),
    )
    return jax.shard_map(
        per_device,
        mesh=torus,
        in_specs=placed,
        out_specs=(P(ALL, None), P(EP, None)),
        check_vma=False,
    )
```

time: 233 us -> 158 us (0.68)
  waiting for transfers between devices: 140 us -> 53.8 us
  blocking collectives: 0 us -> 16.6 us
  local copies, waits for them, and re-layouts: 17.7 us -> 6.31 us
  matrix products: 12 us -> 17.4 us
  starting transfers between devices: 38.8 us -> 43.2 us
  other arithmetic: 9.87 us -> 5.63 us
    all_to_all x4 -> x3, waiting for transfers between devices: 117 us -> 53.8 us  [the longest x1 26.2 us: expert_half(): returned = lax.all_to_all(leaving, EP + ('c',), 0, 0, tiled=True)]
    all_gather x3 -> x1, waiting for transfers between devices: 19 us -> 0.02 us  [mixer_half(): gathered = lax.all_gather(both, TP)]
    all_gather x0 -> x1, blocking collectives: none -> 16.6 us  [expert_half(): whole = lax.all_gather(final, TP)]
    gather x2 -> x0, local copies, waits for them, and re-layouts: 6.69 us -> none  [the longest x1 4.22 us: expert_half(): picked = every_slot[slot_place].reshape(row_count, -1, model_width)]
    ppermute x2 -> x5, starting transfers between devices: 8.01 us -> 13.9 us  [the longest x1 4.58 us: extended(): high = lax.ppermute(block[:width], ALL, backward)]
    dot_general x4 -> x9, matrix products: 12 us -> 17.4 us  [the longest x6 12.4 us: dot(): return jnp.dot(left, right, preferred_element_type=jnp.float32)]
    select_n x2 -> x1, other arithmetic: 3.78 us -> 0.01 us  [expert_half(): jnp.where(first_t, weight_first, jnp.where(second_t, 1.0 - weight_first,...]
    convert_element_type x4 -> x1, other arithmetic: 3.07 us -> 0.02 us  [mixer_half(): padded = extended(pooled_in, 8).astype(jnp.float32)]
  transfers between devices with their start and end apart: 9 -> 9, of which waited for: 6 -> 3; matrix products, arithmetic and copies ran while one was open for 7% -> 13% of each run, Pallas kernels for 0% -> 0%
where the time goes in v1:
time: 158 us; the launch traced here: 157 us
  waiting for transfers between devices  53.8 us (34%)
  starting transfers between devices  43.2 us (27%)
  matrix products  17.4 us (11%)
  blocking collectives  16.6 us (11%)
  between operations  14.4 us (9%)
  local copies, waits for them, and re-layouts  6.31 us (4%)
  other arithmetic  5.63 us (4%)
    all_to_all x1, waiting for transfers between devices, expert_half(): returned = lax.all_to_all(leaving, EP + ('c',), 0, 0, tiled=True)  26.2 us
    all_to_all x1, waiting for transfers between devices, expert_half(): arrived = lax.all_to_all(outgoing, EP, 0, 0, tiled=True)  17.7 us
    all_gather x1, blocking collectives, expert_half(): whole = lax.all_gather(final, TP)  16.6 us
    all_to_all x1, starting transfers between devices, expert_half(): arrived = lax.all_to_all(outgoing, EP, 0, 0, tiled=True)  13.7 us
    dot_general x6, matrix products, dot(): return jnp.dot(left, right, preferred_element_type=jnp.float32)  12.4 us
    all_to_all x1, waiting for transfers between devices, expert_half(): pieces = lax.all_to_all(blocks, 'y', 0, 0, tiled=True)  9.94 us
    all_to_all x1, starting transfers between devices, expert_half(): returned = lax.all_to_all(leaving, EP + ('c',), 0, 0, tiled=True)  8.74 us
    all_to_all x1, starting transfers between devices, expert_half(): pieces = lax.all_to_all(blocks, 'y', 0, 0, tiled=True)  6.81 us
  transfers between devices with their start and end apart: 9, of which 3 were waited for; matrix products, arithmetic and copies ran while one was open for 13% of the time, Pallas kernels for 0%

profile of v1, /device:TPU:1, one launch (start us, length us, event | category | flops | bytes accessed | tf_op | source)
XLA Modules:
  0.0 157.5 jit_solution(2420704275919234505)
XLA Ops:
  7.2 1.7 %pad_maximum_fusion = bf16[64,2048]{1,0:T(8,128)(2,1)} fusion(bf16[32,2048]{1,0:T(8,128)(2,1)} %param.18, bf16[32,2048]{1,0:T(8,128)(2,1)} %bitcast.88), kind=kLoop, calls=%fused_computation.76 | loop fusion | flops 524288 | bytes 524288 | tf_op jit(solution)/shard_map/concatenate | solution.py:35
  9.1 1.3 fusion.9
  11.3 2.6 %fusion.1 = bf16[32,8,2048]{2,1,0:T(8,128)(2,1)} fusion(bf16[128,2048]{1,0:T(8,128)(2,1)} %param.19, f32[2048]{0:T(1024)} %param.20, f32[128]{0:T(128)S(1)} %add_rsqrt_fusion, s32[256]{0:T(256)S(1)} %eq.222, s32[32,128]{1,0:T(8,128)S(1)} %fusion.5), kind=kOutput, calls=%fused_computation.3 | convolution fusion | flops 135823360 | bytes 1598976 | tf_op jit(solution)/shard_map/dot_general | solution.py:77
  13.9 13.7 %all-to-all-start = ((bf16[32,8,2048]{2,1,0:T(8,128)(2,1)}), bf16[32,8,2048]{2,1,0:T(8,128)(2,1)S(1)}, u32[]{:S(2)}, u32[]{:S(2)}) async-start(bf16[32,8,2048]{2,1,0:T(8,128)(2,1)} %fusion.1), calls=%async_computation | async-start | bytes 2097152 | tf_op jit(solution)/shard_map/all_to_all | solution.py:109
  27.6 2.9 %collective-permute-start.4 = (bf16[224,2048]{1,0:T(8,128)(2,1)}, bf16[224,2048]{1,0:T(8,128)(2,1)}, u32[]{:S(2)}, u32[]{:S(2)}) collective-permute-start(bf16[224,2048]{1,0:T(8,128)(2,1)} %bitcast.15), channel_id=1, source_target_pairs={{0,1},{1,0},{2,3},{3,2},{4,5},{5,4},{6,7},{7,6},{8,9},{9,8},{10,11... | collective-permute-start | bytes 2752520 | tf_op jit(solution)/shard_map/ppermute | solution.py:93
  30.5 1.9 %collective-permute-start.3 = (bf16[2048,224]{0,1:T(8,128)(2,1)S(1)}, bf16[2048,224]{0,1:T(8,128)(2,1)S(1)}, u32[]{:S(2)}, u32[]{:S(2)}) collective-permute-start(bf16[2048,224]{0,1:T(8,128)(2,1)S(1)} %bitcast.87), channel_id=1, source_target_pairs={{0,1},{1,0},{2,3},{3,2},{4,5},{5,4},{6,7},{7,6},{8,9},{9,8},{10,11... | collective-permute-start | bytes 2752520 | tf_op jit(solution)/shard_map/ppermute | solution.py:92
  32.4 2.4 %collective-permute-start.2 = (bf16[2048,224]{0,1:T(8,128)(2,1)}, bf16[2048,224]{0,1:T(8,128)(2,1)}, u32[]{:S(2)}, u32[]{:S(2)}) collective-permute-start(bf16[2048,224]{0,1:T(8,128)(2,1)} %bitcast.13), channel_id=1, source_target_pairs={{0,1},{1,0},{2,3},{3,2},{4,5},{5,4},{6,7},{7,6},{8,9},{9,8},{10,11... | collective-permute-start | bytes 2752520 | tf_op jit(solution)/shard_map/ppermute | solution.py:91
  34.9 1.2 multiply_bitcast_fusion
  36.1 17.7 %all-to-all-done = bf16[32,8,2048]{2,1,0:T(8,128)(2,1)S(1)} async-done(((bf16[32,8,2048]{2,1,0:T(8,128)(2,1)}), bf16[32,8,2048]{2,1,0:T(8,128)(2,1)S(1)}, u32[]{:S(2)}, u32[]{:S(2)}) %all-to-all-start) | async-done | bytes 1048608 | tf_op jit(solution)/shard_map/all_to_all | solution.py:109
  53.8 2.3 %fusion.20 = f32[256,224]{0,1:T(8,128)} fusion(bf16[32,8,2048]{2,1,0:T(8,128)(2,1)S(1)} %all-to-all-done, bf16[1,2048,224]{1,2,0:T(8,128)(2,1)} %param.23), kind=kOutput, calls=%fused_computation.30 | convolution fusion | flops 234881024 | bytes 2195456 | tf_op jit(solution)/shard_map/dot_general | solution.py:77
  56.6 3.0 %fusion.4 = f32[256,2048]{1,0:T(8,128)S(1)} fusion(bf16[32,8,2048]{2,1,0:T(8,128)(2,1)S(1)} %all-to-all-done, f32[256,224]{0,1:T(8,128)} %fusion.20, bf16[1,224,2048]{2,1,0:T(8,128)(2,1)} %param.25, bf16[1,2048,224]{1,2,0:T(8,128)(2,1)} %param.24), kind=kOutput, calls=%fused_computation.14 | convolution fusion | flops 470106112 | bytes 5210112 | tf_op jit(solution)/shard_map/dot_general | solution.py:77
  59.6 3.9 %fusion = bf16[256,2048]{1,0:T(8,128)(2,1)} fusion(f32[256,2048]{1,0:T(8,128)S(1)} %fusion.4, bf16[224,2048]{1,0:T(8,128)(2,1)} %collective-permute-done.4, f32[256,224]{0,1:T(8,128)S(1)} %fusion.14, bf16[2048,224]{0,1:T(8,128)(2,1)} %collective-permute-done.2, bf16[32,8,2048]{2,1,0:T(8,128)(2,1)S(1)} %all-to-all-done), kind=kOutput, calls=%fused_computation.2 | convolution fusion | flops 471154688 | bytes 6258688 | tf_op jit(solution)/shard_map/dot_general | solution.py:77
  63.5 8.7 %all-to-all-start.1 = ((bf16[64,8,1024]{2,1,0:T(8,128)(2,1)}), bf16[64,8,1024]{2,1,0:T(8,128)(2,1)S(1)}, u32[]{:S(2)}, u32[]{:S(2)}) async-start(bf16[64,8,1024]{2,1,0:T(8,128)(2,1)} %bitcast.82), calls=%async_computation.1 | async-start | bytes 2097152 | tf_op jit(solution)/shard_map/all_to_all | solution.py:120
  72.3 1.4 reshape.581
  74.3 26.2 %all-to-all-done.1 = bf16[64,8,1024]{2,1,0:T(8,128)(2,1)S(1)} async-done(((bf16[64,8,1024]{2,1,0:T(8,128)(2,1)}), bf16[64,8,1024]{2,1,0:T(8,128)(2,1)S(1)}, u32[]{:S(2)}, u32[]{:S(2)}) %all-to-all-start.1) | async-done | bytes 1048608 | tf_op jit(solution)/shard_map/all_to_all | solution.py:120
  101.7 6.8 %all-to-all-start.2 = ((bf16[8,128,128]{2,1,0:T(8,128)(2,1)}), bf16[8,128,128]{2,1,0:T(8,128)(2,1)S(1)}, u32[]{:S(2)}, u32[]{:S(2)}) async-start(bf16[8,128,128]{2,1,0:T(8,128)(2,1)} %bitcast_bitcast_fusion), calls=%async_computation.2 | async-start | bytes 524288 | tf_op jit(solution)/shard_map/all_to_all | solution.py:140
  108.7 9.9 %all-to-all-done.2 = bf16[8,128,128]{2,1,0:T(8,128)(2,1)S(1)} async-done(((bf16[8,128,128]{2,1,0:T(8,128)(2,1)}), bf16[8,128,128]{2,1,0:T(8,128)(2,1)S(1)}, u32[]{:S(2)}, u32[]{:S(2)}) %all-to-all-start.2) | async-done | bytes 262176 | tf_op jit(solution)/shard_map/all_to_all | solution.py:140
  118.7 2.6 %fusion.200 = (bf16[16,32,2048]{2,1,0:T(8,128)(2,1)S(1)}, bf16[16,32,2048]{2,1,0:T(8,128)(2,1)S(1)}) fusion(bf16[16,64,2048]{2,1,0:T(8,128)(2,1)} %bitcast.81), kind=kLoop, calls=%fused_computation.292 | loop fusion | bytes 8388608 | tf_op jit(solution)/shard_map/slice | solution.py:38
  121.4 0.9 convolution_convert_fusion.2
  122.3 4.6 %collective-permute-start.1 = (bf16[8,512]{1,0:T(8,128)(2,1)S(1)}, bf16[8,512]{1,0:T(8,128)(2,1)S(1)}, u32[]{:S(2)}, u32[]{:S(2)}) collective-permute-start(bf16[8,512]{1,0:T(8,128)(2,1)S(1)} %get-tuple-element.11), channel_id=1, source_target_pairs={{1,0},{2,1},{3,2},{4,3},{5,4},{6,5},{7,6},{8,7},{9,8},{10,9},{11,1... | collective-permute-start | bytes 24584 | tf_op jit(solution)/shard_map/ppermute | solution.py:28
  126.8 2.1 %collective-permute-start = (bf16[8,512]{1,0:T(8,128)(2,1)S(1)}, bf16[8,512]{1,0:T(8,128)(2,1)S(1)}, u32[]{:S(2)}, u32[]{:S(2)}) collective-permute-start(bf16[8,512]{1,0:T(8,128)(2,1)S(1)} %get-tuple-element.10), channel_id=1, source_target_pairs={{0,1},{1,2},{2,3},{3,4},{4,5},{5,6},{6,7},{7,8},{8,9},{9,10},{10,1... | collective-permute-start | bytes 24584 | tf_op jit(solution)/shard_map/ppermute | solution.py:27
  128.9 16.6 %all-gather.1 = bf16[2048,128]{1,0:T(8,128)(2,1)S(1)} all-gather(bf16[128,128]{1,0:T(8,128)(2,1)S(1)} %reduce_sum.32), channel_id=3, replica_groups=mesh['z'=8,'x'=4,'y'=8,'c'=2] {'y','c'}, dimensions={0}, use_global_device_ids=true | all-gather | bytes 557056 | tf_op jit(solution)/shard_map/all_gather | solution.py:142
  145.9 1.0 copy.19
  146.9 3.7 %convolution_convert_fusion.1 = bf16[128,2048]{1,0:T(8,128)(2,1)} fusion(bf16[512,2048]{1,0:T(8,128)(2,1)S(1)} %bitcast.85, bf16[512,512]{1,0:T(8,128)(2,1)} %reshape.581, f32[144,512]{1,0:T(8,128)S(1)} %maximum_convert_fusion, f32[512]{0:T(512)S(1)} %copy-done.6, f32[512]{0:T(512)S(1)} %get-tuple-element.61, pred[512]{0:T(512)(128)(4,1)S(1)} %get-tuple-element.31, ...), kind=kOutput, calls=%fused_computation.4 | convolution fusion | flops 342097920 | bytes 7367680 | tf_op jit(solution)/shard_map/dot_general | solution.py:72
  (67 shorter events, 3.9 us)
Async XLA Ops:
  7.2 111.6 %all-gather.4.cloned.1.call-start = ((), (), s32[]{:S(2)}) async-start(), calls=%async_computation.3 | async-start | bytes 4456448 | tf_op jit(solution)/shard_map/all_gather | solution.py:36
  9.0 21.4 %copy-start.1 = (bf16[1,2048,224]{1,2,0:T(8,128)(2,1)S(1)}, bf16[1,2048,224]{1,2,0:T(8,128)(2,1)}, u32[]{:S(2)}) copy-start(bf16[1,2048,224]{1,2,0:T(8,128)(2,1)} %param.24) | copy-start | bytes 2752516
  9.0 25.8 %copy-start.4 = (f32[128,2]{0,1:T(2,128)S(1)}, f32[128,2]{0,1:T(2,128)}, u32[]{:S(2)}) copy-start(f32[128,2]{0,1:T(2,128)} %param.22) | copy-start | bytes 3076
  9.1 25.8 %copy-start.3 = (bf16[8,64,64]{2,1,0:T(8,128)(2,1)S(1)}, bf16[8,64,64]{2,1,0:T(8,128)(2,1)}, u32[]{:S(2)}) copy-start(bf16[8,64,64]{2,1,0:T(8,128)(2,1)} %param.16) | copy-start | bytes 196612
  13.9 39.9 %all-to-all-start = ((bf16[32,8,2048]{2,1,0:T(8,128)(2,1)}), bf16[32,8,2048]{2,1,0:T(8,128)(2,1)S(1)}, u32[]{:S(2)}, u32[]{:S(2)}) async-start(bf16[32,8,2048]{2,1,0:T(8,128)(2,1)} %fusion.1), calls=%async_computation | async-start | bytes 2097152 | tf_op jit(solution)/shard_map/all_to_all | solution.py:109
  27.6 32.1 %collective-permute-start.4 = (bf16[224,2048]{1,0:T(8,128)(2,1)}, bf16[224,2048]{1,0:T(8,128)(2,1)}, u32[]{:S(2)}, u32[]{:S(2)}) collective-permute-start(bf16[224,2048]{1,0:T(8,128)(2,1)} %bitcast.15), channel_id=1, source_target_pairs={{0,1},{1,0},{2,3},{3,2},{4,5},{5,4},{6,7},{7,6},{8,9},{9,8},{10,11... | collective-permute-start | bytes 2752520 | tf_op jit(solution)/shard_map/ppermute | solution.py:93
  30.5 25.7 %collective-permute-start.3 = (bf16[2048,224]{0,1:T(8,128)(2,1)S(1)}, bf16[2048,224]{0,1:T(8,128)(2,1)S(1)}, u32[]{:S(2)}, u32[]{:S(2)}) collective-permute-start(bf16[2048,224]{0,1:T(8,128)(2,1)S(1)} %bitcast.87), channel_id=1, source_target_pairs={{0,1},{1,0},{2,3},{3,2},{4,5},{5,4},{6,7},{7,6},{8,9},{9,8},{10,11... | collective-permute-start | bytes 2752520 | tf_op jit(solution)/shard_map/ppermute | solution.py:92
  32.4 27.2 %collective-permute-start.2 = (bf16[2048,224]{0,1:T(8,128)(2,1)}, bf16[2048,224]{0,1:T(8,128)(2,1)}, u32[]{:S(2)}, u32[]{:S(2)}) collective-permute-start(bf16[2048,224]{0,1:T(8,128)(2,1)} %bitcast.13), channel_id=1, source_target_pairs={{0,1},{1,0},{2,3},{3,2},{4,5},{5,4},{6,7},{7,6},{8,9},{9,8},{10,11... | collective-permute-start | bytes 2752520 | tf_op jit(solution)/shard_map/ppermute | solution.py:91
  63.5 8.8 %copy-start = (bf16[8,64,8,64]{3,2,1,0:T(8,128)(2,1)S(1)}, bf16[8,64,8,64]{3,2,1,0:T(8,128)(2,1)}, u32[]{:S(2)}) copy-start(bf16[8,64,8,64]{3,2,1,0:T(8,128)(2,1)} %multiply_bitcast_fusion) | copy-start | bytes 1572868
  63.5 36.9 %all-to-all-start.1 = ((bf16[64,8,1024]{2,1,0:T(8,128)(2,1)}), bf16[64,8,1024]{2,1,0:T(8,128)(2,1)S(1)}, u32[]{:S(2)}, u32[]{:S(2)}) async-start(bf16[64,8,1024]{2,1,0:T(8,128)(2,1)} %bitcast.82), calls=%async_computation.1 | async-start | bytes 2097152 | tf_op jit(solution)/shard_map/all_to_all | solution.py:120
  100.5 8.1 %copy-start.2 = (bf16[128,2048]{1,0:T(8,128)(2,1)S(1)}, bf16[128,2048]{1,0:T(8,128)(2,1)}, u32[]{:S(2)}) copy-start(bf16[128,2048]{1,0:T(8,128)(2,1)} %param.13) | copy-start | bytes 1572868
  101.7 17.0 %all-to-all-start.2 = ((bf16[8,128,128]{2,1,0:T(8,128)(2,1)}), bf16[8,128,128]{2,1,0:T(8,128)(2,1)S(1)}, u32[]{:S(2)}, u32[]{:S(2)}) async-start(bf16[8,128,128]{2,1,0:T(8,128)(2,1)} %bitcast_bitcast_fusion), calls=%async_computation.2 | async-start | bytes 524288 | tf_op jit(solution)/shard_map/all_to_all | solution.py:140
  118.7 2.6 %copy-start.5 = (f32[2048]{0:T(1024)S(1)}, f32[2048]{0:T(1024)}, u32[]{:S(2)}) copy-start(f32[2048]{0:T(1024)} %param.14) | copy-start | bytes 24580
  122.2 24.7 %copy-start.6 = (f32[512]{0:T(512)S(1)}, f32[512]{0:T(512)}, u32[]{:S(2)}) copy-start(f32[512]{0:T(512)} %param.17) | copy-start | bytes 6148
  122.3 24.6 %collective-permute-start.1 = (bf16[8,512]{1,0:T(8,128)(2,1)S(1)}, bf16[8,512]{1,0:T(8,128)(2,1)S(1)}, u32[]{:S(2)}, u32[]{:S(2)}) collective-permute-start(bf16[8,512]{1,0:T(8,128)(2,1)S(1)} %get-tuple-element.11), channel_id=1, source_target_pairs={{1,0},{2,1},{3,2},{4,3},{5,4},{6,5},{7,6},{8,7},{9,8},{10,9},{11,1... | collective-permute-start | bytes 24584 | tf_op jit(solution)/shard_map/ppermute | solution.py:28
  126.8 20.0 %collective-permute-start = (bf16[8,512]{1,0:T(8,128)(2,1)S(1)}, bf16[8,512]{1,0:T(8,128)(2,1)S(1)}, u32[]{:S(2)}, u32[]{:S(2)}) collective-permute-start(bf16[8,512]{1,0:T(8,128)(2,1)S(1)} %get-tuple-element.10), channel_id=1, source_target_pairs={{0,1},{1,2},{2,3},{3,4},{4,5},{5,6},{6,7},{7,8},{8,9},{9,10},{10,1... | collective-permute-start | bytes 24584 | tf_op jit(solution)/shard_map/ppermute | solution.py:27
Sparse Core Ops, SparseCore 0:
  10.7 50.3 all-gather.3

commit v2 on v1

v2 whole, which is shorter than its diff:
```python
import jax
import jax.numpy as jnp
from jax import lax
from jax.experimental import pallas as pl
from jax.experimental.pallas import tpu as pltpu
from jax.sharding import Mesh
from jax.sharding import PartitionSpec as P

GROUP = 64
SEQS = 1
ALL = ("z", "x", "y", "c")
EP = ("z", "x")
TP = ("y", "c")
PARTS = 4
STACK_VMEM = 6 << 20
FFN_VMEM = 14 << 20
SWAP = [(0, 1), (1, 0)]

epsilon = 1e-06


def rms_scale(values, gain):
    floats = values.astype(jnp.float32)
    factor = lax.rsqrt(jnp.mean(floats * floats, axis=-1, keepdims=True) + epsilon)
    return (floats * factor * gain).astype(jnp.bfloat16)


def extended(block, width):
    count = lax.axis_size(ALL)
    forward = [(i, i + 1) for i in range(count - 1)]
    backward = [(target, source) for source, target in forward]
    low = lax.ppermute(block[block.shape[0] - width :], ALL, forward)
    high = lax.ppermute(block[:width], ALL, backward)
    return jnp.concatenate([low, block, high], axis=0)


def ring_gather(shard):
    size = lax.axis_size("y")
    forward = [(i, (i + 1) % size) for i in range(size)]
    backward = [(target, source) for source, target in forward]
    blocks = {0: shard}
    low = high = shard
    for step in range(1, size // 2 + 1):
        low = lax.ppermute(low, "y", forward)
        blocks[size - step] = low
        if step < size // 2:
            high = lax.ppermute(high, "y", backward)
            blocks[step] = high
    return [blocks[r] for r in range(size)]


def mixer_half(first_batch, mixer_gain, shard, group_maps, pool_scale):
    count_rows = first_batch.shape[0]
    share = shard.shape[0] // 2
    channels = pool_scale.shape[0]
    ring = lax.axis_size("y")
    blocks = ring_gather(shard)
    own = pl.pallas_call(
        stack_body,
        out_shape=jax.ShapeDtypeStruct((len(blocks) * 2 * share, shard.shape[1]), shard.dtype),
        compiler_params=pltpu.CompilerParams(vmem_limit_bytes=STACK_VMEM),
    )(*blocks)
    far = lax.ppermute(own, "c", SWAP)
    half = channels // 2
    local = jnp.arange(channels, dtype=jnp.int32)
    core = (lax.axis_index("c") + local // half) % 2
    step = (local % half) // share
    place = ((lax.axis_index("y") + step) % ring * 2 + core) * share + local % share
    order = (place[:, None] == jnp.arange(channels, dtype=jnp.int32)[None, :]).astype(jnp.bfloat16)

    normed = rms_scale(first_batch, mixer_gain)
    by_row = (((1,), (1,)), ((), ()))
    pooled_own = lax.dot_general(
        normed, own[:half], by_row, preferred_element_type=jnp.float32
    ).astype(jnp.bfloat16)
    pooled_far = lax.dot_general(
        normed, far[:half], by_row, preferred_element_type=jnp.float32
    ).astype(jnp.bfloat16)
    pooled_in = (dot(pooled_own, order[:half]) + dot(pooled_far, order[half:])).astype(jnp.bfloat16)

    padded = extended(pooled_in, 8).astype(jnp.float32)
    length = count_rows * lax.axis_size(ALL) // SEQS
    first_row = lax.axis_index(ALL) * count_rows
    places = (first_row + jnp.arange(count_rows, dtype=jnp.int32))[:, None]
    kind = (jnp.arange(channels, dtype=jnp.int32) // GROUP % 4)[None, :]
    sums = padded
    window_sum = jnp.zeros((count_rows, channels), jnp.float32)
    for k in range(4):
        span = 1 << k
        sums = sums[:-span] + sums[span:]
        window_sum = jnp.where(kind == k, sums[8 - span : 8 - span + count_rows], window_sum)
    span = jnp.left_shift(jnp.ones_like(kind), kind)
    window_count = jnp.minimum(places + span, length) - jnp.maximum(places - span, 0)
    centred = window_sum / window_count.astype(jnp.float32) - padded[8 : 8 + count_rows]
    centred = centred.astype(jnp.bfloat16)

    group_count = group_maps.shape[0]
    identity = jnp.eye(group_count, dtype=jnp.bfloat16)
    block_map = jnp.einsum("gcd,gh->gchd", group_maps, identity).reshape(channels, channels)
    grouped = (dot(centred, block_map) * pool_scale).astype(jnp.bfloat16)
    grouped = lax.dot_general(
        grouped, order, by_row, preferred_element_type=jnp.float32
    ).astype(jnp.bfloat16)
    mixed_out = dot(grouped[:, :half], own[half:]) + dot(grouped[:, half:], far[half:])
    return mixed_out.astype(jnp.bfloat16)


def on_chip():
    return pl.BlockSpec(memory_space=pltpu.VMEM)


def stack_body(*refs):
    out = refs[-1]
    half = out.shape[0] // 2
    for r, block in enumerate(refs[:-1]):
        share = block.shape[0] // 2
        out[r * share : (r + 1) * share, :] = block[:share, :]
        out[half + r * share : half + (r + 1) * share, :] = block[share:, :]


def ffn_body(rows, gate_a, up_a, down_a, gate_b, up_b, down_b, out, held, done):
    values = rows[...]
    by_row = (((1,), (1,)), ((), ()))

    def hidden(gate, up):
        left = lax.dot_general(values, gate[...], by_row, preferred_element_type=jnp.float32)
        right = lax.dot_general(values, up[...], by_row, preferred_element_type=jnp.float32)
        return (left / (1.0 + jnp.exp(-left)) * right).astype(jnp.bfloat16)

    hidden_a = hidden(gate_a, up_a)
    hidden_b = hidden(gate_b, up_b)
    width = held.shape[1] // PARTS
    copies = []
    for k in range(PARTS):
        span = pl.ds(k * width, width)
        total = dot(hidden_a, down_a[:, span]) + dot(hidden_b, down_b[:, span])
        held[:, span] = total.astype(jnp.bfloat16)
        copies.append(pltpu.make_async_copy(held.at[:, span], out.at[:, span], done.at[k]))
        copies[-1].start()
    for copy in copies:
        copy.wait()


def dot(left, right):
    return jnp.dot(left, right, preferred_element_type=jnp.float32)


def expert_half(
    shard,
    second_batch,
    expert_gain,
    expert_choice,
    route_scores,
    expert_gate,
    expert_up,
    expert_down,
):
    row_count, model_width = second_batch.shape
    experts = lax.axis_size(EP)
    capacity = 4 * row_count // experts
    half_slots = capacity // 2
    core = lax.axis_index("c")

    gate_own, up_own, down_own = expert_gate[0].T, expert_up[0].T, expert_down[0]
    gate_far = lax.ppermute(gate_own, "c", SWAP)
    up_far = lax.ppermute(up_own, "c", SWAP)
    down_far = lax.ppermute(down_own, "c", SWAP)

    normed = rms_scale(second_batch, expert_gain)
    expert_ids = jnp.arange(experts, dtype=jnp.int32)
    first_t = expert_choice[:, 0][None, :] == expert_ids[:, None]
    second_t = expert_choice[:, 1][None, :] == expert_ids[:, None]
    named_t = first_t | second_t
    rows = jnp.arange(row_count, dtype=jnp.int32)
    earlier_t = (rows[:, None] < rows[None, :]).astype(jnp.bfloat16)
    rank_t = dot(named_t.astype(jnp.bfloat16), earlier_t).astype(jnp.int32)
    rank_t = jnp.where(named_t, rank_t, -1)

    own_slots = core * half_slots + jnp.arange(half_slots, dtype=jnp.int32)
    spread = (rank_t[:, None, :] == own_slots[None, :, None]).astype(jnp.bfloat16)
    outgoing = dot(spread.reshape(experts * half_slots, row_count), normed).astype(jnp.bfloat16)
    outgoing = outgoing.reshape(experts, half_slots, model_width)
    shard, outgoing = lax.optimization_barrier((shard, outgoing))
    arrived = lax.all_to_all(outgoing, EP, 0, 0, tiled=True)
    incoming = arrived.reshape(experts * half_slots, model_width)

    partial = pl.pallas_call(
        ffn_body,
        out_shape=jax.ShapeDtypeStruct(incoming.shape, jnp.bfloat16),
        in_specs=[on_chip()] * 7,
        out_specs=pl.BlockSpec(memory_space=pltpu.HBM),
        scratch_shapes=[
            pltpu.VMEM(incoming.shape, jnp.bfloat16),
            pltpu.SemaphoreType.DMA((PARTS,)),
        ],
        compiler_params=pltpu.CompilerParams(vmem_limit_bytes=FFN_VMEM),
        cost_estimate=pl.CostEstimate(
            flops=12 * incoming.size * gate_own.shape[0],
            transcendentals=2 * incoming.shape[0] * gate_own.shape[0],
            bytes_accessed=4 * incoming.size + 12 * gate_own.size,
        ),
    )(incoming, gate_own, up_own, down_own, gate_far, up_far, down_far)
    shares = lax.axis_size(TP)
    piece = model_width // shares
    leaving = partial.reshape(experts, half_slots, shares, piece)
    leaving = jnp.moveaxis(leaving, 2, 1).reshape(experts * shares, half_slots, piece)
    returned = lax.all_to_all(leaving, ALL, 0, 0, tiled=True)
    returned = returned.reshape(experts, shares // 2, 2, half_slots, piece)
    results = jnp.sum(returned.astype(jnp.float32), axis=1).astype(jnp.bfloat16)
    results = results.reshape(experts * capacity, piece)

    weight_first = jax.nn.sigmoid(route_scores[:, 0] - route_scores[:, 1])[None, :]
    weight_t = jnp.where(first_t, weight_first, jnp.where(second_t, 1.0 - weight_first, 0.0))
    slots = jnp.arange(capacity, dtype=jnp.int32)
    blend_t = jnp.where(
        rank_t[:, None, :] == slots[None, :, None], weight_t[:, None, :], 0.0
    ).reshape(experts * capacity, row_count)
    high = lax.reduce_precision(blend_t, 8, 7)
    low = blend_t - high
    both = jnp.concatenate([high, low], axis=1).astype(jnp.bfloat16)
    mixed = lax.dot_general(
        both, results, (((0,), (0,)), ((), ())), preferred_element_type=jnp.float32
    )
    blended = (mixed[:row_count] + mixed[row_count:]).astype(jnp.bfloat16)

    whole = lax.all_gather(blended, TP)
    return jnp.transpose(whole, (1, 0, 2)).reshape(row_count, model_width), shard


def per_device(
    first_batch,
    mixer_gain,
    mixer_in,
    group_maps,
    pool_scale,
    mixer_out,
    second_batch,
    expert_gain,
    expert_choice,
    route_scores,
    expert_gate,
    expert_up,
    expert_down,
):
    shard = jnp.concatenate([mixer_in.T, mixer_out], axis=0)
    experts_second, shard = expert_half(
        shard,
        second_batch,
        expert_gain,
        expert_choice,
        route_scores,
        expert_gate,
        expert_up,
        expert_down,
    )
    mixed_first = mixer_half(first_batch, mixer_gain, shard, group_maps, pool_scale)
    return (mixed_first, experts_second)


def solution(mesh):
    torus = Mesh(mesh.devices.reshape(8, 4, mesh.shape["tp"] // 2, 2), ALL)
    placed = (
        P(ALL, None),
        P(),
        P(None, TP),
        P(),
        P(),
        P(TP, None),
        P(EP, None),
        P(),
        P(EP, None),
        P(EP, None),
        P(EP, None, TP),
        P(EP, None, TP),
        P(EP, TP, None),
    )
    return jax.shard_map(
        per_device,
        mesh=torus,
        in_specs=placed,
        out_specs=(P(ALL, None), P(EP, None)),
        check_vma=False,
    )
```

time: 158 us -> 163 us (1.032)
  starting transfers between devices: 43.2 us -> 74.3 us
  waiting for transfers between devices: 53.8 us -> 22.8 us
  between operations: 14.4 us -> 1.01 us
  local copies, waits for them, and re-layouts: 6.31 us -> 15.2 us
  other arithmetic: 5.63 us -> 14 us
  Pallas kernels: 0 us -> 5.26 us
  matrix products: 17.4 us -> 12.7 us
    all_to_all x2 -> x1, waiting for transfers between devices: 36.1 us -> 6.22 us  [expert_half(): returned = lax.all_to_all(leaving, ALL, 0, 0, tiled=True)]
    ppermute x0 -> x8, starting transfers between devices: none -> 25.6 us  [the longest x3 13.1 us: ring_gather(): high = lax.ppermute(high, 'y', backward)]
    all_to_all x1, waiting for transfers between devices: 17.7 us -> 6.26 us  [expert_half(): arrived = lax.all_to_all(outgoing, EP, 0, 0, tiled=True)]
    unnamed x15 -> x44, local copies, waits for them, and re-layouts: 1.05 us -> 11.1 us
    ppermute x1, starting transfers between devices: 2.41 us -> 12.1 us  [expert_half(): gate_far = lax.ppermute(gate_own, 'c', SWAP)]
    ppermute x1, waiting for transfers between devices: 0.01 us -> 6.1 us  [extended(): high = lax.ppermute(block[:width], ALL, backward)]
    all_to_all x1, starting transfers between devices: 13.7 us -> 8.25 us  [expert_half(): arrived = lax.all_to_all(outgoing, EP, 0, 0, tiled=True)]
    pallas_call x0 -> x2, Pallas kernels: none -> 5.26 us  [the longest x1 5.13 us: expert_half(): pl.pallas_call(ffn_body, out_shape=jax.ShapeDtypeStruct(incoming.shape, j...]
  transfers between devices with their start and end apart: 9 -> 15, of which waited for: 3 -> 6; matrix products, arithmetic and copies ran while one was open for 13% -> 14% of each run, Pallas kernels for 0% -> 3%
where the time goes in v2:
time: 163 us; the launch traced here: 161 us
  starting transfers between devices  74.3 us (46%)
  waiting for transfers between devices  22.8 us (14%)
  blocking collectives  16.2 us (10%)
  local copies, waits for them, and re-layouts  15.2 us (9%)
  other arithmetic  14 us (9%)
  matrix products  12.7 us (8%)
  Pallas kernels  5.26 us (3%)
    all_to_all x1, starting transfers between devices, expert_half(): returned = lax.all_to_all(leaving, ALL, 0, 0, tiled=True)  16.4 us
    all_gather x1, blocking collectives, expert_half(): whole = lax.all_gather(blended, TP)  16.2 us
    ppermute x3, starting transfers between devices, ring_gather(): high = lax.ppermute(high, 'y', backward)  13.1 us
    ppermute x1, starting transfers between devices, expert_half(): gate_far = lax.ppermute(gate_own, 'c', SWAP)  12.1 us
    unnamed x44, local copies, waits for them, and re-layouts  11.1 us
    ppermute x4, starting transfers between devices, ring_gather(): low = lax.ppermute(low, 'y', forward)  10.3 us
    dot_general x6, matrix products, dot(): return jnp.dot(left, right, preferred_element_type=jnp.float32)  10 us
    all_to_all x1, starting transfers between devices, expert_half(): arrived = lax.all_to_all(outgoing, EP, 0, 0, tiled=True)  8.25 us
  transfers between devices with their start and end apart: 15, of which 6 were waited for; matrix products, arithmetic and copies ran while one was open for 14% of the time, Pallas kernels for 3%

profile of v2, /device:TPU:1, one launch (start us, length us, event | category | flops | bytes accessed | tf_op | source)
XLA Modules:
  0.0 161.4 jit_solution(9319097716251662732)
XLA Ops:
  3.9 2.5 %fusion = bf16[32,8,2048]{2,1,0:T(8,128)(2,1)} fusion(bf16[128,2048]{1,0:T(8,128)(2,1)} %param.19, f32[2048]{0:T(1024)} %param.20, f32[128]{0:T(128)S(1)} %add_rsqrt_fusion, s32[256]{0:T(256)S(1)} %eq.147, s32[32,128]{1,0:T(8,128)S(1)} %fusion.5), kind=kOutput, calls=%fused_computation.1 | convolution fusion | flops 135823360 | bytes 1598976 | tf_op jit(solution)/shard_map/dot_general | solution.py:145
  6.4 4.0 %collective-permute-start.3 = (bf16[64,2048]{1,0:T(8,128)(2,1)S(1)}, bf16[64,2048]{1,0:T(8,128)(2,1)S(1)}, u32[]{:S(2)}, u32[]{:S(2)}) collective-permute-start(bf16[64,2048]{1,0:T(8,128)(2,1)S(1)} %pad_maximum_fusion.refs_0_), channel_id=1, source_target_pairs={{0,2},{2,4},{4,6},{6,8},{8,10},{10,12},{12,14},{14,0},{1,3},{3,5},... | collective-permute-start | bytes 786440 | tf_op jit(solution)/shard_map/ppermute | solution.py:44
  10.4 3.8 %collective-permute-start = (bf16[64,2048]{1,0:T(8,128)(2,1)S(1)}, bf16[64,2048]{1,0:T(8,128)(2,1)S(1)}, u32[]{:S(2)}, u32[]{:S(2)}) collective-permute-start(bf16[64,2048]{1,0:T(8,128)(2,1)S(1)} %pad_maximum_fusion.refs_0_), channel_id=1, source_target_pairs={{2,0},{4,2},{6,4},{8,6},{10,8},{12,10},{14,12},{0,14},{3,1},{5,3},... | collective-permute-start | bytes 786440 | tf_op jit(solution)/shard_map/ppermute | solution.py:47
  16.1 2.5 %collective-permute-start.4 = (bf16[64,2048]{1,0:T(8,128)(2,1)S(1)}, bf16[64,2048]{1,0:T(8,128)(2,1)S(1)}, u32[]{:S(2)}, u32[]{:S(2)}) collective-permute-start(bf16[64,2048]{1,0:T(8,128)(2,1)S(1)} %collective-permute-done.3.refs_7_), channel_id=1, source_target_pairs={{0,2},{2,4},{4,6},{6,8},{8,10},{10,12},{12,14},{14,0},{1,3},{3,5},... | collective-permute-start | bytes 786440 | tf_op jit(solution)/shard_map/ppermute | solution.py:44
  19.3 4.7 %collective-permute-start.1 = (bf16[64,2048]{1,0:T(8,128)(2,1)S(1)}, bf16[64,2048]{1,0:T(8,128)(2,1)S(1)}, u32[]{:S(2)}, u32[]{:S(2)}) collective-permute-start(bf16[64,2048]{1,0:T(8,128)(2,1)S(1)} %collective-permute-done.refs_1_), channel_id=1, source_target_pairs={{2,0},{4,2},{6,4},{8,6},{10,8},{12,10},{14,12},{0,14},{3,1},{5,3},... | collective-permute-start | bytes 786440 | tf_op jit(solution)/shard_map/ppermute | solution.py:47
  25.1 1.9 %collective-permute-start.5 = (bf16[64,2048]{1,0:T(8,128)(2,1)S(1)}, bf16[64,2048]{1,0:T(8,128)(2,1)S(1)}, u32[]{:S(2)}, u32[]{:S(2)}) collective-permute-start(bf16[64,2048]{1,0:T(8,128)(2,1)S(1)} %collective-permute-done.4.refs_6_), channel_id=1, source_target_pairs={{0,2},{2,4},{4,6},{6,8},{8,10},{10,12},{12,14},{14,0},{1,3},{3,5},... | collective-permute-start | bytes 786440 | tf_op jit(solution)/shard_map/ppermute | solution.py:44
  27.8 4.6 %collective-permute-start.2 = (bf16[64,2048]{1,0:T(8,128)(2,1)S(1)}, bf16[64,2048]{1,0:T(8,128)(2,1)S(1)}, u32[]{:S(2)}, u32[]{:S(2)}) collective-permute-start(bf16[64,2048]{1,0:T(8,128)(2,1)S(1)} %collective-permute-done.1.refs_2_), channel_id=1, source_target_pairs={{2,0},{4,2},{6,4},{8,6},{10,8},{12,10},{14,12},{0,14},{3,1},{5,3},... | collective-permute-start | bytes 786440 | tf_op jit(solution)/shard_map/ppermute | solution.py:47
  32.3 2.0 %collective-permute-done.5.refs_5_ = bf16[64,2048]{1,0:T(8,128)(2,1)S(1)} collective-permute-done((bf16[64,2048]{1,0:T(8,128)(2,1)S(1)}, bf16[64,2048]{1,0:T(8,128)(2,1)S(1)}, u32[]{:S(2)}, u32[]{:S(2)}) %collective-permute-start.5) | collective-permute-done | bytes 262176 | tf_op jit(solution)/shard_map/ppermute | solution.py:44
  36.2 12.1 %collective-permute-start.10 = (bf16[224,2048]{1,0:T(8,128)(2,1)}, bf16[224,2048]{1,0:T(8,128)(2,1)}, u32[]{:S(2)}, u32[]{:S(2)}) collective-permute-start(bf16[224,2048]{1,0:T(8,128)(2,1)} %bitcast.11.gate_a), channel_id=1, source_target_pairs={{0,1},{1,0},{2,3},{3,2},{4,5},{5,4},{6,7},{7,6},{8,9},{9,8},{10,11... | collective-permute-start | bytes 2752520 | tf_op jit(solution)/shard_map/ppermute | solution.py:165
  48.3 1.9 %collective-permute-start.11 = (bf16[224,2048]{1,0:T(8,128)(2,1)}, bf16[224,2048]{1,0:T(8,128)(2,1)}, u32[]{:S(2)}, u32[]{:S(2)}) collective-permute-start(bf16[224,2048]{1,0:T(8,128)(2,1)} %bitcast.13.up_a), channel_id=1, source_target_pairs={{0,1},{1,0},{2,3},{3,2},{4,5},{5,4},{6,7},{7,6},{8,9},{9,8},{10,11... | collective-permute-start | bytes 2752520 | tf_op jit(solution)/shard_map/ppermute | solution.py:166
  50.3 2.4 %collective-permute-start.12 = (bf16[224,2048]{1,0:T(8,128)(2,1)}, bf16[224,2048]{1,0:T(8,128)(2,1)}, u32[]{:S(2)}, u32[]{:S(2)}) collective-permute-start(bf16[224,2048]{1,0:T(8,128)(2,1)} %bitcast.14.down_a), channel_id=1, source_target_pairs={{0,1},{1,0},{2,3},{3,2},{4,5},{5,4},{6,7},{7,6},{8,9},{9,8},{10,11... | collective-permute-start | bytes 2752520 | tf_op jit(solution)/shard_map/ppermute | solution.py:167
  52.7 8.3 %all-to-all-start = ((bf16[32,8,2048]{2,1,0:T(8,128)(2,1)}), bf16[32,8,2048]{2,1,0:T(8,128)(2,1)S(1)}, u32[]{:S(2)}, u32[]{:S(2)}) async-start(bf16[32,8,2048]{2,1,0:T(8,128)(2,1)} %fusion), calls=%async_computation | async-start | bytes 2097152 | tf_op jit(solution)/shard_map/all_to_all | solution.py:184
  69.7 2.2 %collective-permute-start.7 = (bf16[512,2048]{1,0:T(8,128)(2,1)S(1)}, bf16[512,2048]{1,0:T(8,128)(2,1)}, u32[]{:S(2)}, u32[]{:S(2)}) collective-permute-start(bf16[512,2048]{1,0:T(8,128)(2,1)S(1)} %shard_map.140), channel_id=1, source_target_pairs={{0,1},{1,0},{2,3},{3,2},{4,5},{5,4},{6,7},{7,6},{8,9},{9,8},{10,11... | collective-permute-start | bytes 6291464 | tf_op jit(solution)/shard_map/ppermute | solution.py:63
  79.5 2.5 %fusion.4 = f32[128,512]{1,0:T(8,128)} fusion(bf16[512,2048]{1,0:T(8,128)(2,1)S(1)} %shard_map.140, pred[512,512]{1,0:T(32,128)(4,1)S(1)} %iota_compare_fusion, bf16[128,2048]{1,0:T(8,128)(2,1)} %param.13, f32[2048]{0:T(1024)} %param.14, f32[128]{0:T(128)} %add_rsqrt_fusion.1), kind=kOutput, calls=%fused_computation.15 | convolution fusion | flops 168853504 | bytes 1974784 | tf_op jit(solution)/shard_map/dot_general | solution.py:145
  82.0 6.3 %all-to-all-done = bf16[32,8,2048]{2,1,0:T(8,128)(2,1)S(1)} async-done(((bf16[32,8,2048]{2,1,0:T(8,128)(2,1)}), bf16[32,8,2048]{2,1,0:T(8,128)(2,1)S(1)}, u32[]{:S(2)}, u32[]{:S(2)}) %all-to-all-start) | async-done | bytes 1048608 | tf_op jit(solution)/shard_map/all_to_all | solution.py:184
  88.2 5.1 %shard_map.141 = bf16[256,2048]{1,0:T(8,128)(2,1)S(1)} custom-call(bf16[256,2048]{1,0:T(8,128)(2,1)S(1)} %bitcast.53, bf16[224,2048]{1,0:T(8,128)(2,1)} %bitcast.11.gate_a, bf16[224,2048]{1,0:T(8,128)(2,1)} %bitcast.13.up_a, bf16[224,2048]{1,0:T(8,128)(2,1)} %bitcast.14.down_a, bf16[224,2048]{1,0:T(8,128)(2,1)} %collective-permute-done.10.gate_b, ...), custom_call_target="tpu_custom_call" | custom-call | flops 1409286144 | bytes 7602176 | tf_op jit(solution)/shard_map/pallas_call | solution.py:187
  94.3 16.4 %all-to-all-start.1 = ((bf16[512,8,128]{2,1,0:T(8,128)(2,1)}), bf16[512,8,128]{2,1,0:T(8,128)(2,1)}, u32[]{:S(2)}, u32[]{:S(2)}) async-start(bf16[512,8,128]{2,1,0:T(8,128)(2,1)} %bitcast.54), calls=%async_computation.1 | async-start | bytes 2097152 | tf_op jit(solution)/shard_map/all_to_all | solution.py:207
  110.8 2.2 %fusion.2 = bf16[128,512]{1,0:T(8,128)(2,1)S(1)} fusion(f32[128,512]{1,0:T(8,128)} %fusion.4, bf16[512,2048]{1,0:T(8,128)(2,1)} %collective-permute-done.7, pred[512,512]{1,0:T(32,128)(4,1)S(1)} %iota_compare_fusion, bf16[128,2048]{1,0:T(8,128)(2,1)} %param.13, f32[2048]{0:T(1024)} %param.14, f32[128]{0:T(128)} %add_rsqrt_fusion.1), kind=kOutput, calls=%fused_computation.10 | convolution fusion | flops 168984576 | bytes 2105856 | tf_op jit(solution)/shard_map/dot_general | solution.py:145
  112.9 3.5 %collective-permute-start.8 = (bf16[8,512]{1,0:T(8,128)(2,1)S(1)}, bf16[8,512]{1,0:T(8,128)(2,1)S(1)}, u32[]{:S(2)}, u32[]{:S(2)}) collective-permute-start(bf16[8,512]{1,0:T(8,128)(2,1)S(1)} %get-tuple-element.10), channel_id=1, source_target_pairs={{0,1},{1,2},{2,3},{3,4},{4,5},{5,6},{6,7},{7,8},{8,9},{9,10},{10,1... | collective-permute-start | bytes 24584 | tf_op jit(solution)/shard_map/ppermute | solution.py:32
  116.5 4.0 %collective-permute-start.9 = (bf16[8,512]{1,0:T(8,128)(2,1)S(1)}, bf16[8,512]{1,0:T(8,128)(2,1)S(1)}, u32[]{:S(2)}, u32[]{:S(2)}) collective-permute-start(bf16[8,512]{1,0:T(8,128)(2,1)S(1)} %get-tuple-element.11), channel_id=1, source_target_pairs={{1,0},{2,1},{3,2},{4,3},{5,4},{6,5},{7,6},{8,7},{9,8},{10,9},{11,1... | collective-permute-start | bytes 24584 | tf_op jit(solution)/shard_map/ppermute | solution.py:33
  124.1 6.1 %collective-permute-done.9 = bf16[8,512]{1,0:T(8,128)(2,1)S(1)} collective-permute-done((bf16[8,512]{1,0:T(8,128)(2,1)S(1)}, bf16[8,512]{1,0:T(8,128)(2,1)S(1)}, u32[]{:S(2)}, u32[]{:S(2)}) %collective-permute-start.9) | collective-permute-done | bytes 8224 | tf_op jit(solution)/shard_map/ppermute | solution.py:33
  131.2 2.4 %convolution_convert_fusion.1 = bf16[128,512]{1,0:T(8,128)(2,1)} fusion(bf16[512,512]{1,0:T(8,128)(2,1)} %reshape.268, f32[144,512]{1,0:T(8,128)S(1)} %maximum_convert_fusion, f32[143,512]{1,0:T(8,128)S(1)} %slice_add_fusion.2, f32[141,512]{1,0:T(8,128)S(1)} %slice_add_fusion.1, f32[137,512]{1,0:T(8,128)S(1)} %slice_add_fusion, ...), kind=kOutput, calls=%fused_computation.12 | convolution fusion | flops 135593984 | bytes 2236928 | tf_op jit(solution)/shard_map/dot_general | solution.py:101
  136.3 6.2 %all-to-all-done.1 = bf16[512,8,128]{2,1,0:T(8,128)(2,1)} async-done(((bf16[512,8,128]{2,1,0:T(8,128)(2,1)}), bf16[512,8,128]{2,1,0:T(8,128)(2,1)}, u32[]{:S(2)}, u32[]{:S(2)}) %all-to-all-start.1) | async-done | bytes 1048608 | tf_op jit(solution)/shard_map/all_to_all | solution.py:207
  144.3 16.2 %all-gather = bf16[2048,128]{1,0:T(8,128)(2,1)S(1)} all-gather(bf16[128,128]{1,0:T(8,128)(2,1)S(1)} %fusion.59), channel_id=2, replica_groups=mesh['z'=8,'x'=4,'y'=8,'c'=2] {'y','c'}, dimensions={0}, use_global_device_ids=true | all-gather | bytes 557056 | tf_op jit(solution)/shard_map/all_gather | solution.py:226
  (93 shorter events, 36.6 us)
Async XLA Ops:
  2.6 50.0 %copy-start.20 = (s32[128]{0:T(128)}, s32[128]{0:T(128)S(1)}, u32[]{:S(2)}) copy-start(s32[128]{0:T(128)S(1)} %get-tuple-element.14) | copy-start | bytes 1540
  2.7 50.0 %copy-start.21 = (s32[128]{0:T(128)}, s32[128]{0:T(128)S(1)}, u32[]{:S(2)}) copy-start(s32[128]{0:T(128)S(1)} %get-tuple-element.15) | copy-start | bytes 1540
  6.4 9.7 %collective-permute-start.3 = (bf16[64,2048]{1,0:T(8,128)(2,1)S(1)}, bf16[64,2048]{1,0:T(8,128)(2,1)S(1)}, u32[]{:S(2)}, u32[]{:S(2)}) collective-permute-start(bf16[64,2048]{1,0:T(8,128)(2,1)S(1)} %pad_maximum_fusion.refs_0_), channel_id=1, source_target_pairs={{0,2},{2,4},{4,6},{6,8},{8,10},{10,12},{12,14},{14,0},{1,3},{3,5},... | collective-permute-start | bytes 786440 | tf_op jit(solution)/shard_map/ppermute | solution.py:44
  10.4 8.9 %collective-permute-start = (bf16[64,2048]{1,0:T(8,128)(2,1)S(1)}, bf16[64,2048]{1,0:T(8,128)(2,1)S(1)}, u32[]{:S(2)}, u32[]{:S(2)}) collective-permute-start(bf16[64,2048]{1,0:T(8,128)(2,1)S(1)} %pad_maximum_fusion.refs_0_), channel_id=1, source_target_pairs={{2,0},{4,2},{6,4},{8,6},{10,8},{12,10},{14,12},{0,14},{3,1},{5,3},... | collective-permute-start | bytes 786440 | tf_op jit(solution)/shard_map/ppermute | solution.py:47
  16.1 9.1 %collective-permute-start.4 = (bf16[64,2048]{1,0:T(8,128)(2,1)S(1)}, bf16[64,2048]{1,0:T(8,128)(2,1)S(1)}, u32[]{:S(2)}, u32[]{:S(2)}) collective-permute-start(bf16[64,2048]{1,0:T(8,128)(2,1)S(1)} %collective-permute-done.3.refs_7_), channel_id=1, source_target_pairs={{0,2},{2,4},{4,6},{6,8},{8,10},{10,12},{12,14},{14,0},{1,3},{3,5},... | collective-permute-start | bytes 786440 | tf_op jit(solution)/shard_map/ppermute | solution.py:44
  19.3 8.4 %collective-permute-start.1 = (bf16[64,2048]{1,0:T(8,128)(2,1)S(1)}, bf16[64,2048]{1,0:T(8,128)(2,1)S(1)}, u32[]{:S(2)}, u32[]{:S(2)}) collective-permute-start(bf16[64,2048]{1,0:T(8,128)(2,1)S(1)} %collective-permute-done.refs_1_), channel_id=1, source_target_pairs={{2,0},{4,2},{6,4},{8,6},{10,8},{12,10},{14,12},{0,14},{3,1},{5,3},... | collective-permute-start | bytes 786440 | tf_op jit(solution)/shard_map/ppermute | solution.py:47
  25.1 9.2 %collective-permute-start.5 = (bf16[64,2048]{1,0:T(8,128)(2,1)S(1)}, bf16[64,2048]{1,0:T(8,128)(2,1)S(1)}, u32[]{:S(2)}, u32[]{:S(2)}) collective-permute-start(bf16[64,2048]{1,0:T(8,128)(2,1)S(1)} %collective-permute-done.4.refs_6_), channel_id=1, source_target_pairs={{0,2},{2,4},{4,6},{6,8},{8,10},{10,12},{12,14},{14,0},{1,3},{3,5},... | collective-permute-start | bytes 786440 | tf_op jit(solution)/shard_map/ppermute | solution.py:44
  27.8 33.8 %copy-start.7 = (bf16[64,2048]{1,0:T(8,128)(2,1)}, bf16[64,2048]{1,0:T(8,128)(2,1)S(1)}, u32[]{:S(2)}) copy-start(bf16[64,2048]{1,0:T(8,128)(2,1)S(1)} %collective-permute-done.1.refs_2_) | copy-start | bytes 786436
  27.8 33.8 %collective-permute-start.2 = (bf16[64,2048]{1,0:T(8,128)(2,1)S(1)}, bf16[64,2048]{1,0:T(8,128)(2,1)S(1)}, u32[]{:S(2)}, u32[]{:S(2)}) collective-permute-start(bf16[64,2048]{1,0:T(8,128)(2,1)S(1)} %collective-permute-done.1.refs_2_), channel_id=1, source_target_pairs={{2,0},{4,2},{6,4},{8,6},{10,8},{12,10},{14,12},{0,14},{3,1},{5,3},... | collective-permute-start | bytes 786440 | tf_op jit(solution)/shard_map/ppermute | solution.py:47
  34.3 27.2 %copy-start.9 = (bf16[64,2048]{1,0:T(8,128)(2,1)}, bf16[64,2048]{1,0:T(8,128)(2,1)S(1)}, u32[]{:S(2)}) copy-start(bf16[64,2048]{1,0:T(8,128)(2,1)S(1)} %collective-permute-done.5.refs_5_) | copy-start | bytes 786436
  34.3 27.9 %collective-permute-start.6 = (bf16[64,2048]{1,0:T(8,128)(2,1)S(1)}, bf16[64,2048]{1,0:T(8,128)(2,1)S(1)}, u32[]{:S(2)}, u32[]{:S(2)}) collective-permute-start(bf16[64,2048]{1,0:T(8,128)(2,1)S(1)} %collective-permute-done.5.refs_5_), channel_id=1, source_target_pairs={{0,2},{2,4},{4,6},{6,8},{8,10},{10,12},{12,14},{14,0},{1,3},{3,5},... | collective-permute-start | bytes 786440 | tf_op jit(solution)/shard_map/ppermute | solution.py:44
  36.2 45.7 %collective-permute-start.10 = (bf16[224,2048]{1,0:T(8,128)(2,1)}, bf16[224,2048]{1,0:T(8,128)(2,1)}, u32[]{:S(2)}, u32[]{:S(2)}) collective-permute-start(bf16[224,2048]{1,0:T(8,128)(2,1)} %bitcast.11.gate_a), channel_id=1, source_target_pairs={{0,1},{1,0},{2,3},{3,2},{4,5},{5,4},{6,7},{7,6},{8,9},{9,8},{10,11... | collective-permute-start | bytes 2752520 | tf_op jit(solution)/shard_map/ppermute | solution.py:165
  48.3 33.6 %collective-permute-start.11 = (bf16[224,2048]{1,0:T(8,128)(2,1)}, bf16[224,2048]{1,0:T(8,128)(2,1)}, u32[]{:S(2)}, u32[]{:S(2)}) collective-permute-start(bf16[224,2048]{1,0:T(8,128)(2,1)} %bitcast.13.up_a), channel_id=1, source_target_pairs={{0,1},{1,0},{2,3},{3,2},{4,5},{5,4},{6,7},{7,6},{8,9},{9,8},{10,11... | collective-permute-start | bytes 2752520 | tf_op jit(solution)/shard_map/ppermute | solution.py:166
  50.3 31.7 %collective-permute-start.12 = (bf16[224,2048]{1,0:T(8,128)(2,1)}, bf16[224,2048]{1,0:T(8,128)(2,1)}, u32[]{:S(2)}, u32[]{:S(2)}) collective-permute-start(bf16[224,2048]{1,0:T(8,128)(2,1)} %bitcast.14.down_a), channel_id=1, source_target_pairs={{0,1},{1,0},{2,3},{3,2},{4,5},{5,4},{6,7},{7,6},{8,9},{9,8},{10,11... | collective-permute-start | bytes 2752520 | tf_op jit(solution)/shard_map/ppermute | solution.py:167
  52.7 35.5 %all-to-all-start = ((bf16[32,8,2048]{2,1,0:T(8,128)(2,1)}), bf16[32,8,2048]{2,1,0:T(8,128)(2,1)S(1)}, u32[]{:S(2)}, u32[]{:S(2)}) async-start(bf16[32,8,2048]{2,1,0:T(8,128)(2,1)} %fusion), calls=%async_computation | async-start | bytes 2097152 | tf_op jit(solution)/shard_map/all_to_all | solution.py:184
  69.6 8.7 %copy-start.16 = (bf16[8,64,64]{2,1,0:T(8,128)(2,1)S(1)}, bf16[8,64,64]{2,1,0:T(8,128)(2,1)}, u32[]{:S(2)}) copy-start(bf16[8,64,64]{2,1,0:T(8,128)(2,1)} %param.16) | copy-start | bytes 196612
  69.7 41.0 %collective-permute-start.7 = (bf16[512,2048]{1,0:T(8,128)(2,1)S(1)}, bf16[512,2048]{1,0:T(8,128)(2,1)}, u32[]{:S(2)}, u32[]{:S(2)}) collective-permute-start(bf16[512,2048]{1,0:T(8,128)(2,1)S(1)} %shard_map.140), channel_id=1, source_target_pairs={{0,1},{1,0},{2,3},{3,2},{4,5},{5,4},{6,7},{7,6},{8,9},{9,8},{10,11... | collective-permute-start | bytes 6291464 | tf_op jit(solution)/shard_map/ppermute | solution.py:63
  94.3 26.8 %copy-start.15 = (bf16[8,64,8,64]{3,2,1,0:T(8,128)(2,1)S(1)}, bf16[8,64,8,64]{3,2,1,0:T(8,128)(2,1)}, u32[]{:S(2)}) copy-start(bf16[8,64,8,64]{3,2,1,0:T(8,128)(2,1)} %multiply_bitcast_fusion) | copy-start | bytes 1572868
  94.3 48.2 %all-to-all-start.1 = ((bf16[512,8,128]{2,1,0:T(8,128)(2,1)}), bf16[512,8,128]{2,1,0:T(8,128)(2,1)}, u32[]{:S(2)}, u32[]{:S(2)}) async-start(bf16[512,8,128]{2,1,0:T(8,128)(2,1)} %bitcast.54), calls=%async_computation.1 | async-start | bytes 2097152 | tf_op jit(solution)/shard_map/all_to_all | solution.py:207
  112.9 11.2 %collective-permute-start.8 = (bf16[8,512]{1,0:T(8,128)(2,1)S(1)}, bf16[8,512]{1,0:T(8,128)(2,1)S(1)}, u32[]{:S(2)}, u32[]{:S(2)}) collective-permute-start(bf16[8,512]{1,0:T(8,128)(2,1)S(1)} %get-tuple-element.10), channel_id=1, source_target_pairs={{0,1},{1,2},{2,3},{3,4},{4,5},{5,6},{6,7},{7,8},{8,9},{9,10},{10,1... | collective-permute-start | bytes 24584 | tf_op jit(solution)/shard_map/ppermute | solution.py:32
  116.5 13.8 %collective-permute-start.9 = (bf16[8,512]{1,0:T(8,128)(2,1)S(1)}, bf16[8,512]{1,0:T(8,128)(2,1)S(1)}, u32[]{:S(2)}, u32[]{:S(2)}) collective-permute-start(bf16[8,512]{1,0:T(8,128)(2,1)S(1)} %get-tuple-element.11), channel_id=1, source_target_pairs={{1,0},{2,1},{3,2},{4,3},{5,4},{6,5},{7,6},{8,7},{9,8},{10,9},{11,1... | collective-permute-start | bytes 24584 | tf_op jit(solution)/shard_map/ppermute | solution.py:33
  133.6 1.6 %copy-start.19 = (bf16[128,512]{1,0:T(8,128)(2,1)S(1)}, bf16[128,512]{1,0:T(8,128)(2,1)}, u32[]{:S(2)}) copy-start(bf16[128,512]{1,0:T(8,128)(2,1)} %convolution_convert_fusion.1) | copy-start | bytes 393220
  135.2 8.7 %copy-start.17 = (bf16[512,128]{1,0:T(8,128)(2,1)S(1)}, bf16[512,128]{1,0:T(8,128)(2,1)}, u32[]{:S(2)}) copy-start(bf16[512,128]{1,0:T(8,128)(2,1)} %get-tuple-element.12) | copy-start | bytes 393220
  135.2 8.7 %copy-start.18 = (bf16[512,128]{1,0:T(8,128)(2,1)S(1)}, bf16[512,128]{1,0:T(8,128)(2,1)}, u32[]{:S(2)}) copy-start(bf16[512,128]{1,0:T(8,128)(2,1)} %get-tuple-element.13) | copy-start | bytes 393220
  (13 other events, 11.1 us)

commit v3 on v2

v3 whole, which is shorter than its diff:
```python
import jax
import jax.numpy as jnp
from jax import lax
from jax.experimental import pallas as pl
from jax.experimental.pallas import tpu as pltpu
from jax.sharding import Mesh
from jax.sharding import PartitionSpec as P

GROUP = 64
ALL = ("z", "x", "y", "c")
EP = ("z", "x")
TP = ("y", "c")
PARTS = 4
EXPERTS = 32
SWAP = [(0, 1), (1, 0)]

epsilon = 1e-06


def neighbours(block, width):
    count = lax.axis_size(ALL)
    forward = [(i, i + 1) for i in range(count - 1)]
    backward = [(target, source) for source, target in forward]
    low = lax.ppermute(block[block.shape[0] - width :], ALL, forward)
    high = lax.ppermute(block[:width], ALL, backward)
    return low, high


def in_place():
    return pl.BlockSpec(memory_space=pl.ANY)


def in_scalars():
    return pl.BlockSpec(memory_space=pltpu.SMEM)


def limit(mib):
    return pltpu.CompilerParams(vmem_limit_bytes=mib << 20)


def norm(values, gain):
    floats = values.astype(jnp.float32)
    factor = lax.rsqrt(jnp.mean(floats * floats, axis=-1, keepdims=True) + epsilon)
    return (floats * factor * gain).astype(jnp.bfloat16)


def gathered_blocks(shard):
    size = lax.axis_size("y")
    far = lax.ppermute(shard, "c", SWAP)
    passed = jnp.concatenate([shard, far], axis=0)
    ways = [(2 * i, 2 * ((i + 1) % size)) for i in range(size)]
    ways += [(2 * i + 1, 2 * ((i - 1) % size) + 1) for i in range(size)]
    blocks = [passed]
    for _ in range(1, size // 2 + 1):
        passed = lax.ppermute(passed, TP, ways)
        blocks.append(passed)
    for step in range(1, size // 2):
        blocks.append(lax.ppermute(blocks[step], "c", SWAP))
    return blocks


def fetch(place, blocks, half, rows, done):
    size = len(blocks)
    share = rows.shape[0] // (2 * size)
    y, core = place[0], place[1]
    sign = 1 - 2 * core
    copies = []
    for k, block in enumerate(blocks):
        ours = k <= size // 2
        steps = -k if ours else k - size // 2
        group = lax.rem(y + sign * steps + size, size)
        first = core if ours else 1 - core
        for part in range(2):
            held = first if part == 0 else 1 - first
            start = pl.multiple_of((group * 2 + held) * share, share)
            base = (2 * part + half) * share
            copy = pltpu.make_async_copy(
                block.at[pl.ds(base, share), :],
                rows.at[pl.ds(start, share), :],
                done.at[2 * k + part],
            )
            copy.start()
            copies.append(copy)
    return copies


def project_body(place, rows, gain, *refs):
    blocks, pooled, in_rows, done = refs[:-3], refs[-3], refs[-2], refs[-1]
    copies = fetch(place, blocks, 0, in_rows, done)
    normed = norm(rows[...], gain[...])
    for copy in copies:
        copy.wait()
    product = lax.dot_general(
        normed, in_rows[...], (((1,), (1,)), ((), ())), preferred_element_type=jnp.float32
    )
    pooled[...] = product.astype(jnp.bfloat16)


def pool_body(place, pooled, low, high, maps, scale, *refs):
    blocks, out, out_rows, done = refs[:-3], refs[-3], refs[-2], refs[-1]
    copies = fetch(place, blocks, 1, out_rows, done)
    count_rows, channels = pooled.shape
    width = low.shape[0]
    pairs = maps.shape[0]
    lanes = maps.shape[1]
    middle = pooled[...].astype(jnp.float32)
    sums = jnp.concatenate(
        [low[...].astype(jnp.float32), middle, high[...].astype(jnp.float32)], axis=0
    )
    shape = (count_rows, channels)
    kind = lax.broadcasted_iota(jnp.int32, shape, 1) // GROUP % 4
    places = place[2] * count_rows + lax.broadcasted_iota(jnp.int32, shape, 0)
    length = place[3] * count_rows
    window_sum = jnp.zeros(shape, jnp.float32)
    for k in range(4):
        span = 1 << k
        kept = sums.shape[0] - span
        sums = sums[:kept] + sums[span:]
        window_sum = jnp.where(
            kind == k, sums[width - span : width - span + count_rows], window_sum
        )
    span = jnp.left_shift(jnp.ones(shape, jnp.int32), kind)
    window_count = jnp.minimum(places + span, length) - jnp.maximum(places - span, 0)
    centred = (window_sum / window_count.astype(jnp.float32) - middle).astype(jnp.bfloat16)
    pieces = []
    for k in range(pairs):
        lane = slice(k * lanes, (k + 1) * lanes)
        pieces.append((dot(centred[:, lane], maps[k]) * scale[:, lane]).astype(jnp.bfloat16))
    grouped = jnp.concatenate(pieces, axis=1)
    for copy in copies:
        copy.wait()
    out[...] = dot(grouped, out_rows[...]).astype(jnp.bfloat16)


def mixer_half(first_batch, mixer_gain, shard, pair_maps, pool_scale):
    count_rows, width = first_batch.shape
    channels = pool_scale.shape[0]
    blocks = gathered_blocks(shard)
    place = jnp.stack(
        [
            lax.axis_index("y"),
            lax.axis_index("c"),
            lax.axis_index(ALL),
            jnp.int32(lax.axis_size(ALL)),
        ]
    ).astype(jnp.int32)
    held = [
        pltpu.VMEM((channels, width), jnp.bfloat16),
        pltpu.SemaphoreType.DMA((2 * len(blocks),)),
    ]
    cost = pl.CostEstimate(
        flops=2 * count_rows * width * channels,
        transcendentals=0,
        bytes_accessed=4 * channels * width,
    )
    whole = pl.BlockSpec()
    pooled_in = pl.pallas_call(
        project_body,
        out_shape=jax.ShapeDtypeStruct((count_rows, channels), jnp.bfloat16),
        in_specs=[in_scalars(), whole, whole] + [in_place()] * len(blocks),
        scratch_shapes=held,
        compiler_params=limit(10),
        cost_estimate=cost,
    )(place, first_batch, mixer_gain[None, :], *blocks)
    low, high = neighbours(pooled_in, 8)
    return pl.pallas_call(
        pool_body,
        out_shape=jax.ShapeDtypeStruct((count_rows, width), jnp.bfloat16),
        in_specs=[in_scalars()] + [whole] * 5 + [in_place()] * len(blocks),
        scratch_shapes=held,
        compiler_params=limit(10),
        cost_estimate=cost,
    )(place, pooled_in, low, high, pair_maps, pool_scale[None, :], *blocks)


def ranked(choice, experts):
    count = choice.shape[1]
    names = lax.broadcasted_iota(jnp.int32, (experts, count), 0)
    first = choice[0:1, :] == names
    second = choice[1:2, :] == names
    named = first | second
    rows = lax.broadcasted_iota(jnp.int32, (count, count), 0)
    others = lax.broadcasted_iota(jnp.int32, (count, count), 1)
    earlier = jnp.where(rows < others, 1.0, 0.0).astype(jnp.bfloat16)
    rank = dot(jnp.where(named, 1.0, 0.0).astype(jnp.bfloat16), earlier)
    return first, second, jnp.where(named, rank, -1.0).astype(jnp.bfloat16)


def repeated(values, repeats):
    experts = values.shape[0]
    shape = (experts * repeats, experts)
    owner = lax.broadcasted_iota(jnp.int32, shape, 0) // repeats
    match = owner == lax.broadcasted_iota(jnp.int32, shape, 1)
    return dot(jnp.where(match, 1.0, 0.0).astype(jnp.bfloat16), values)


def dispatch_body(core, rows, gain, choice, out):
    count = rows.shape[0]
    slots = out.shape[0]
    half = slots // EXPERTS
    rank = repeated(ranked(choice[...], EXPERTS)[2], half)
    slot = core[0] * half + lax.broadcasted_iota(jnp.int32, (slots, count), 0) % half
    spread = jnp.where(rank == slot.astype(jnp.float32), 1.0, 0.0).astype(jnp.bfloat16)
    out[...] = dot(spread, norm(rows[...], gain[...])).astype(jnp.bfloat16)


def blend_body(choice, scores, out):
    count = choice.shape[1]
    slots = out.shape[0]
    first, second, rank = ranked(choice[...], EXPERTS)
    repeats = slots // EXPERTS
    weight = 1.0 / (1.0 + jnp.exp(scores[1:2, :] - scores[0:1, :]))
    weights = jnp.where(first, weight, jnp.where(second, 1.0 - weight, 0.0))
    high = weights.astype(jnp.bfloat16)
    low = (weights - high.astype(jnp.float32)).astype(jnp.bfloat16)
    slot = lax.broadcasted_iota(jnp.int32, (slots, count), 0) % repeats
    match = repeated(rank, repeats) == slot.astype(jnp.float32)
    out[:, :count] = jnp.where(match, repeated(high, repeats), 0.0).astype(jnp.bfloat16)
    out[:, count:] = jnp.where(match, repeated(low, repeats), 0.0).astype(jnp.bfloat16)


def ffn_body(*refs):
    sources, out, held, done = refs[:7], refs[7], refs[8:16], refs[16]
    fetches = []
    for k in range(7):
        fetches.append(pltpu.make_async_copy(sources[k], held[k], done.at[PARTS + k]))
        fetches[-1].start()
    rows, _, _, down_a, _, _, down_b, result = held
    fetches[0].wait()
    values = rows[...]

    def product(k):
        fetches[k].wait()
        return lax.dot_general(
            values, held[k][...], (((1,), (1,)), ((), ())), preferred_element_type=jnp.float32
        )

    def hidden(gate, up):
        return (gate / (1.0 + jnp.exp(-gate)) * up).astype(jnp.bfloat16)

    hidden_a = hidden(product(1), product(2))
    hidden_b = hidden(product(4), product(5))
    fetches[3].wait()
    fetches[6].wait()
    width = result.shape[1] // PARTS
    copies = []
    for k in range(PARTS):
        span = pl.ds(k * width, width)
        total = dot(hidden_a, down_a[:, span]) + dot(hidden_b, down_b[:, span])
        result[:, span] = total.astype(jnp.bfloat16)
        copies.append(pltpu.make_async_copy(result.at[:, span], out.at[:, span], done.at[k]))
        copies[-1].start()
    for copy in copies:
        copy.wait()


def dot(left, right):
    return jnp.dot(left, right, preferred_element_type=jnp.float32)


def expert_half(
    mixer_in,
    mixer_out,
    second_batch,
    expert_gain,
    expert_choice,
    route_scores,
    expert_gate,
    expert_up,
    expert_down,
):
    row_count, model_width = second_batch.shape
    experts = lax.axis_size(EP)
    capacity = 4 * row_count // experts
    half_slots = capacity // 2
    core = lax.axis_index("c")

    gate_own, up_own, down_own = expert_gate[0].T, expert_up[0].T, expert_down[0]
    gate_far = lax.ppermute(gate_own, "c", SWAP)
    up_far = lax.ppermute(up_own, "c", SWAP)
    down_far = lax.ppermute(down_own, "c", SWAP)

    outgoing = pl.pallas_call(
        dispatch_body,
        out_shape=jax.ShapeDtypeStruct((experts * half_slots, model_width), jnp.bfloat16),
        in_specs=[in_scalars()] + [pl.BlockSpec()] * 3,
        compiler_params=limit(8),
        cost_estimate=pl.CostEstimate(
            flops=2 * experts * half_slots * second_batch.size,
            transcendentals=row_count,
            bytes_accessed=6 * second_batch.size,
        ),
    )(core[None].astype(jnp.int32), second_batch, expert_gain[None, :], expert_choice.T)
    outgoing = outgoing.reshape(experts, half_slots, model_width)
    mixer_in, mixer_out, outgoing = lax.optimization_barrier((mixer_in, mixer_out, outgoing))
    shard = jnp.concatenate([mixer_in.T, mixer_out], axis=0)
    arrived = lax.all_to_all(outgoing, EP, 0, 0, tiled=True)
    incoming = arrived.reshape(experts * half_slots, model_width)

    partial = pl.pallas_call(
        ffn_body,
        out_shape=jax.ShapeDtypeStruct(incoming.shape, jnp.bfloat16),
        in_specs=[in_place()] * 7,
        out_specs=in_place(),
        scratch_shapes=[pltpu.VMEM(incoming.shape, jnp.bfloat16)]
        + [pltpu.VMEM(gate_own.shape, jnp.bfloat16)] * 6
        + [pltpu.VMEM(incoming.shape, jnp.bfloat16), pltpu.SemaphoreType.DMA((PARTS + 7,))],
        compiler_params=limit(14),
        cost_estimate=pl.CostEstimate(
            flops=12 * incoming.size * gate_own.shape[0],
            transcendentals=2 * incoming.shape[0] * gate_own.shape[0],
            bytes_accessed=4 * incoming.size + 12 * gate_own.size,
        ),
    )(incoming, gate_own, up_own, down_own, gate_far, up_far, down_far)
    shares = lax.axis_size(TP)
    piece = model_width // shares
    leaving = partial.reshape(experts, half_slots, shares, piece)
    leaving = jnp.moveaxis(leaving, 2, 1).reshape(experts * shares, half_slots, piece)
    returned = lax.all_to_all(leaving, ALL, 0, 0, tiled=True)
    returned = returned.reshape(experts, shares // 2, 2, half_slots, piece)
    results = jnp.sum(returned.astype(jnp.float32), axis=1).astype(jnp.bfloat16)
    results = results.reshape(experts * capacity, piece)

    both = pl.pallas_call(
        blend_body,
        out_shape=jax.ShapeDtypeStruct((experts * capacity, 2 * row_count), jnp.bfloat16),
        compiler_params=limit(6),
    )(expert_choice.T, route_scores.T)
    mixed = lax.dot_general(
        both, results, (((0,), (0,)), ((), ())), preferred_element_type=jnp.float32
    )
    blended = (mixed[:row_count] + mixed[row_count:]).astype(jnp.bfloat16)

    whole = lax.all_gather(blended, TP)
    return jnp.transpose(whole, (1, 0, 2)).reshape(row_count, model_width), shard


def per_device(
    first_batch,
    mixer_gain,
    mixer_in,
    group_maps,
    pool_scale,
    mixer_out,
    second_batch,
    expert_gain,
    expert_choice,
    route_scores,
    expert_gate,
    expert_up,
    expert_down,
):
    experts_second, shard = expert_half(
        mixer_in,
        mixer_out,
        second_batch,
        expert_gain,
        expert_choice,
        route_scores,
        expert_gate,
        expert_up,
        expert_down,
    )
    groups, inner, outer = group_maps.shape
    same = jnp.eye(2, dtype=jnp.bfloat16)
    pair_maps = jnp.einsum("pgcd,gh->pgchd", group_maps.reshape(groups // 2, 2, inner, outer), same)
    pair_maps = pair_maps.reshape(groups // 2, 2 * inner, 2 * outer)
    mixed_first = mixer_half(first_batch, mixer_gain, shard, pair_maps, pool_scale)
    return (mixed_first, experts_second)


def solution(mesh):
    torus = Mesh(mesh.devices.reshape(8, 4, mesh.shape["tp"] // 2, 2), ALL)
    placed = (
        P(ALL, None),
        P(),
        P(None, TP),
        P(),
        P(),
        P(TP, None),
        P(EP, None),
        P(),
        P(EP, None),
        P(EP, None),
        P(EP, None, TP),
        P(EP, None, TP),
        P(EP, TP, None),
    )
    return jax.shard_map(
        per_device,
        mesh=torus,
        in_specs=placed,
        out_specs=(P(ALL, None), P(EP, None)),
        check_vma=False,
    )
```

time: 163 us -> 167 us (1.025)
  the two profiles are of different devices: /device:TPU:1 before, /device:TPU:265 now
where the time goes in v3:
time: 167 us; the launch traced here: 166 us
  starting transfers between devices  65.3 us (39%)
  waiting for transfers between devices  42.1 us (25%)
  blocking collectives  24.4 us (15%)
  Pallas kernels  17.2 us (10%)
  local copies, waits for them, and re-layouts  13.4 us (8%)
  other arithmetic  1.85 us (1%)
    ppermute x4, waiting for transfers between devices, gathered_blocks(): passed = lax.ppermute(passed, TP, ways)  32.6 us
    all_gather x1, blocking collectives, expert_half(): whole = lax.all_gather(blended, TP)  24.4 us
    all_to_all x1, starting transfers between devices, expert_half(): returned = lax.all_to_all(leaving, ALL, 0, 0, tiled=True)  22.4 us
    ppermute x4, starting transfers between devices, gathered_blocks(): passed = lax.ppermute(passed, TP, ways)  11.1 us
    unnamed x42, local copies, waits for them, and re-layouts  11 us
    all_to_all x1, starting transfers between devices, expert_half(): arrived = lax.all_to_all(outgoing, EP, 0, 0, tiled=True)  9.43 us
    all_to_all x1, waiting for transfers between devices, expert_half(): arrived = lax.all_to_all(outgoing, EP, 0, 0, tiled=True)  7.9 us
    ppermute x3, starting transfers between devices, gathered_blocks(): blocks.append(lax.ppermute(blocks[step], 'c', SWAP))  7.45 us
  transfers between devices with their start and end apart: 15, of which 5 were waited for; matrix products, arithmetic and copies ran while one was open for 1% of the time, Pallas kernels for 9%

profile of v3, /device:TPU:265, one launch (start us, length us, event | category | flops | bytes accessed | tf_op | source)
XLA Modules:
  0.0 165.5 jit_solution(7056802006199983594)
XLA Ops:
  2.4 1.6 shard_map.140
  4.0 9.4 %all-to-all-start = ((bf16[32,8,2048]{2,1,0:T(8,128)(2,1)}), bf16[32,8,2048]{2,1,0:T(8,128)(2,1)S(1)}, u32[]{:S(2)}, u32[]{:S(2)}) async-start(bf16[32,8,2048]{2,1,0:T(8,128)(2,1)} %bitcast.6), calls=%async_computation | async-start | bytes 2097152 | tf_op jit(solution)/shard_map/all_to_all | solution.py:297
  13.5 3.1 %collective-permute-start.10 = (bf16[224,2048]{1,0:T(8,128)(2,1)S(1)}, bf16[224,2048]{1,0:T(8,128)(2,1)S(1)}, u32[]{:S(2)}, u32[]{:S(2)}) collective-permute-start(bf16[224,2048]{1,0:T(8,128)(2,1)S(1)} %bitcast.40), channel_id=1, source_target_pairs={{0,1},{1,0},{2,3},{3,2},{4,5},{5,4},{6,7},{7,6},{8,9},{9,8},{10,11... | collective-permute-start | bytes 2752520 | tf_op jit(solution)/shard_map/ppermute | solution.py:279
  16.6 1.9 %collective-permute-start.11 = (bf16[224,2048]{1,0:T(8,128)(2,1)}, bf16[224,2048]{1,0:T(8,128)(2,1)S(1)}, u32[]{:S(2)}, u32[]{:S(2)}) collective-permute-start(bf16[224,2048]{1,0:T(8,128)(2,1)} %bitcast.17.refs_2_), channel_id=1, source_target_pairs={{0,1},{1,0},{2,3},{3,2},{4,5},{5,4},{6,7},{7,6},{8,9},{9,8},{10,11... | collective-permute-start | bytes 2752520 | tf_op jit(solution)/shard_map/ppermute | solution.py:280
  18.6 2.4 %collective-permute-start.12 = (bf16[224,2048]{1,0:T(8,128)(2,1)}, bf16[224,2048]{1,0:T(8,128)(2,1)S(1)}, u32[]{:S(2)}, u32[]{:S(2)}) collective-permute-start(bf16[224,2048]{1,0:T(8,128)(2,1)} %bitcast.18.refs_3_), channel_id=1, source_target_pairs={{0,1},{1,0},{2,3},{3,2},{4,5},{5,4},{6,7},{7,6},{8,9},{9,8},{10,11... | collective-permute-start | bytes 2752520 | tf_op jit(solution)/shard_map/ppermute | solution.py:281
  21.0 1.9 %collective-permute-start = (bf16[64,2048]{1,0:T(8,128)(2,1)S(1)}, bf16[64,2048]{1,0:T(8,128)(2,1)S(1)}, u32[]{:S(2)}, u32[]{:S(2)}) collective-permute-start(bf16[64,2048]{1,0:T(8,128)(2,1)S(1)} %pad_maximum_fusion.1), channel_id=1, source_target_pairs={{0,1},{1,0},{2,3},{3,2},{4,5},{5,4},{6,7},{7,6},{8,9},{9,8},{10,11... | collective-permute-start | bytes 786440 | tf_op jit(solution)/shard_map/ppermute | solution.py:49
  24.5 2.1 %collective-permute-start.1 = (bf16[128,2048]{1,0:T(8,128)(2,1)S(1)}, bf16[128,2048]{1,0:T(8,128)(2,1)S(1)}, u32[]{:S(2)}, u32[]{:S(2)}) collective-permute-start(bf16[128,2048]{1,0:T(8,128)(2,1)S(1)} %pad_maximum_fusion.refs_0_), channel_id=1, source_target_pairs={{0,2},{2,4},{4,6},{6,8},{8,10},{10,12},{12,14},{14,0},{1,15},{3,1}... | collective-permute-start | bytes 1572872 | tf_op jit(solution)/shard_map/ppermute | solution.py:55
  29.4 7.9 %all-to-all-done = bf16[32,8,2048]{2,1,0:T(8,128)(2,1)S(1)} async-done(((bf16[32,8,2048]{2,1,0:T(8,128)(2,1)}), bf16[32,8,2048]{2,1,0:T(8,128)(2,1)S(1)}, u32[]{:S(2)}, u32[]{:S(2)}) %all-to-all-start) | async-done | bytes 1048608 | tf_op jit(solution)/shard_map/all_to_all | solution.py:297
  40.9 5.4 %shard_map.144 = bf16[256,2048]{1,0:T(8,128)(2,1)} custom-call(bf16[256,2048]{1,0:T(8,128)(2,1)S(1)} %bitcast.39, bf16[224,2048]{1,0:T(8,128)(2,1)S(1)} %bitcast.41, bf16[224,2048]{1,0:T(8,128)(2,1)} %bitcast.17.refs_2_, bf16[224,2048]{1,0:T(8,128)(2,1)} %bitcast.18.refs_3_, bf16[224,2048]{1,0:T(8,128)(2,1)S(1)} %copy-done.2, ...), custom_call_target="tpu_custom_call" | custom-call | flops 1409286144 | bytes 7602176 | tf_op jit(solution)/shard_map/pallas_call | solution.py:300
  46.3 22.4 %all-to-all-start.1 = ((bf16[512,8,128]{2,1,0:T(8,128)(2,1)}), bf16[512,8,128]{2,1,0:T(8,128)(2,1)}, u32[]{:S(2)}, u32[]{:S(2)}) async-start(bf16[512,8,128]{2,1,0:T(8,128)(2,1)} %bitcast.23), calls=%async_computation.1 | async-start | bytes 2097152 | tf_op jit(solution)/shard_map/all_to_all | solution.py:319
  68.7 2.1 %collective-permute-start.2 = (bf16[128,2048]{1,0:T(8,128)(2,1)S(1)}, bf16[128,2048]{1,0:T(8,128)(2,1)S(1)}, u32[]{:S(2)}, u32[]{:S(2)}) collective-permute-start(bf16[128,2048]{1,0:T(8,128)(2,1)S(1)} %collective-permute-done.1.refs_1_), channel_id=1, source_target_pairs={{0,2},{2,4},{4,6},{6,8},{8,10},{10,12},{12,14},{14,0},{1,15},{3,1}... | collective-permute-start | bytes 1572872 | tf_op jit(solution)/shard_map/ppermute | solution.py:55
  70.8 22.9 %collective-permute-done.2.refs_2_ = bf16[128,2048]{1,0:T(8,128)(2,1)S(1)} collective-permute-done((bf16[128,2048]{1,0:T(8,128)(2,1)S(1)}, bf16[128,2048]{1,0:T(8,128)(2,1)S(1)}, u32[]{:S(2)}, u32[]{:S(2)}) %collective-permute-start.2) | collective-permute-done | bytes 524320 | tf_op jit(solution)/shard_map/ppermute | solution.py:55
  93.7 2.0 %collective-permute-start.3 = (bf16[128,2048]{1,0:T(8,128)(2,1)S(1)}, bf16[128,2048]{1,0:T(8,128)(2,1)S(1)}, u32[]{:S(2)}, u32[]{:S(2)}) collective-permute-start(bf16[128,2048]{1,0:T(8,128)(2,1)S(1)} %collective-permute-done.2.refs_2_), channel_id=1, source_target_pairs={{0,2},{2,4},{4,6},{6,8},{8,10},{10,12},{12,14},{14,0},{1,15},{3,1}... | collective-permute-start | bytes 1572872 | tf_op jit(solution)/shard_map/ppermute | solution.py:55
  95.7 2.4 %collective-permute-start.5 = (bf16[128,2048]{1,0:T(8,128)(2,1)S(1)}, bf16[128,2048]{1,0:T(8,128)(2,1)S(1)}, u32[]{:S(2)}, u32[]{:S(2)}) collective-permute-start(bf16[128,2048]{1,0:T(8,128)(2,1)S(1)} %collective-permute-done.1.refs_1_), channel_id=1, source_target_pairs={{0,1},{1,0},{2,3},{3,2},{4,5},{5,4},{6,7},{7,6},{8,9},{9,8},{10,11... | collective-permute-start | bytes 1572872 | tf_op jit(solution)/shard_map/ppermute | solution.py:58
  98.2 1.9 %collective-permute-start.6 = (bf16[128,2048]{1,0:T(8,128)(2,1)S(1)}, bf16[128,2048]{1,0:T(8,128)(2,1)S(1)}, u32[]{:S(2)}, u32[]{:S(2)}) collective-permute-start(bf16[128,2048]{1,0:T(8,128)(2,1)S(1)} %collective-permute-done.2.refs_2_), channel_id=1, source_target_pairs={{0,1},{1,0},{2,3},{3,2},{4,5},{5,4},{6,7},{7,6},{8,9},{9,8},{10,11... | collective-permute-start | bytes 1572872 | tf_op jit(solution)/shard_map/ppermute | solution.py:58
  100.1 3.8 %collective-permute-done.3.refs_3_ = bf16[128,2048]{1,0:T(8,128)(2,1)S(1)} collective-permute-done((bf16[128,2048]{1,0:T(8,128)(2,1)S(1)}, bf16[128,2048]{1,0:T(8,128)(2,1)S(1)}, u32[]{:S(2)}, u32[]{:S(2)}) %collective-permute-start.3) | collective-permute-done | bytes 524320 | tf_op jit(solution)/shard_map/ppermute | solution.py:55
  103.9 3.1 %collective-permute-start.7 = (bf16[128,2048]{1,0:T(8,128)(2,1)S(1)}, bf16[128,2048]{1,0:T(8,128)(2,1)}, u32[]{:S(2)}, u32[]{:S(2)}) collective-permute-start(bf16[128,2048]{1,0:T(8,128)(2,1)S(1)} %collective-permute-done.3.refs_3_), channel_id=1, source_target_pairs={{0,1},{1,0},{2,3},{3,2},{4,5},{5,4},{6,7},{7,6},{8,9},{9,8},{10,11... | collective-permute-start | bytes 1572872 | tf_op jit(solution)/shard_map/ppermute | solution.py:58
  107.0 4.9 %collective-permute-start.4 = (bf16[128,2048]{1,0:T(8,128)(2,1)S(1)}, bf16[128,2048]{1,0:T(8,128)(2,1)}, u32[]{:S(2)}, u32[]{:S(2)}) collective-permute-start(bf16[128,2048]{1,0:T(8,128)(2,1)S(1)} %collective-permute-done.3.refs_3_), channel_id=1, source_target_pairs={{0,2},{2,4},{4,6},{6,8},{8,10},{10,12},{12,14},{14,0},{1,15},{3,1}... | collective-permute-start | bytes 1572872 | tf_op jit(solution)/shard_map/ppermute | solution.py:55
  112.0 6.0 %collective-permute-done.4.refs_4_ = bf16[128,2048]{1,0:T(8,128)(2,1)} collective-permute-done((bf16[128,2048]{1,0:T(8,128)(2,1)S(1)}, bf16[128,2048]{1,0:T(8,128)(2,1)}, u32[]{:S(2)}, u32[]{:S(2)}) %collective-permute-start.4) | collective-permute-done | bytes 524320 | tf_op jit(solution)/shard_map/ppermute | solution.py:55
  119.0 4.6 %shard_map.141.pooled = bf16[128,512]{1,0:T(8,128)(2,1)S(1)} custom-call(s32[4]{0:T(128)S(1)} %pad_add_fusion.place, bf16[128,2048]{1,0:T(8,128)(2,1)S(1)} %copy-done.8, f32[1,2048]{1,0:T(1,128)S(1)} %bitcast.43, bf16[128,2048]{1,0:T(8,128)(2,1)S(1)} %pad_maximum_fusion.refs_0_, bf16[128,2048]{1,0:T(8,128)(2,1)S(1)} %collective-permute-done.1.refs_1_, ...), custom_call_target="tpu_custom_call" | custom-call | flops 268435456 | bytes 4194304 | tf_op jit(solution)/shard_map/pallas_call | solution.py:157
  124.2 3.3 %collective-permute-start.9 = (bf16[8,512]{1,0:T(8,128)(2,1)}, bf16[8,512]{1,0:T(8,128)(2,1)S(1)}, u32[]{:S(2)}, u32[]{:S(2)}) collective-permute-start(bf16[8,512]{1,0:T(8,128)(2,1)} %get-tuple-element.8), channel_id=1, source_target_pairs={{1,0},{2,1},{3,2},{4,3},{5,4},{6,5},{7,6},{8,7},{9,8},{10,9},{11,1... | collective-permute-start | bytes 24584 | tf_op jit(solution)/shard_map/ppermute | solution.py:25
  127.6 2.2 %collective-permute-start.8 = (bf16[8,512]{1,0:T(8,128)(2,1)}, bf16[8,512]{1,0:T(8,128)(2,1)S(1)}, u32[]{:S(2)}, u32[]{:S(2)}) collective-permute-start(bf16[8,512]{1,0:T(8,128)(2,1)} %get-tuple-element.9), channel_id=1, source_target_pairs={{0,1},{1,2},{2,3},{3,4},{4,5},{5,6},{6,7},{7,8},{8,9},{9,10},{10,1... | collective-permute-start | bytes 24584 | tf_op jit(solution)/shard_map/ppermute | solution.py:24
  133.3 5.2 %shard_map.142 = bf16[128,2048]{1,0:T(8,128)(2,1)} custom-call(s32[4]{0:T(128)S(1)} %copy-done.13, bf16[128,512]{1,0:T(8,128)(2,1)S(1)} %shard_map.141.pooled, bf16[8,512]{1,0:T(8,128)(2,1)S(1)} %collective-permute-done.8.low, bf16[8,512]{1,0:T(8,128)(2,1)S(1)} %collective-permute-done.9.high, bf16[4,128,128]{2,1,0:T(8,128)(2,1)S(1)} %copy-done.9, ...), custom_call_target="tpu_custom_call" | custom-call | flops 268435456 | bytes 4194304 | tf_op jit(solution)/shard_map/pallas_call | solution.py:166
  140.2 24.4 %all-gather = bf16[2048,128]{1,0:T(8,128)(2,1)S(1)} all-gather(bf16[128,128]{1,0:T(8,128)(2,1)S(1)} %fusion), channel_id=2, replica_groups=mesh['z'=8,'x'=4,'y'=8,'c'=2] {'y','c'}, dimensions={0}, use_global_device_ids=true | all-gather | bytes 557056 | tf_op jit(solution)/shard_map/all_gather | solution.py:334
  (65 shorter events, 17.4 us)
Async XLA Ops:
  4.0 9.4 %copy-start = (bf16[1,2048,224]{1,2,0:T(8,128)(2,1)S(1)}, bf16[1,2048,224]{1,2,0:T(8,128)(2,1)}, u32[]{:S(2)}) copy-start(bf16[1,2048,224]{1,2,0:T(8,128)(2,1)} %param.23) | copy-start | bytes 2752516
  4.0 17.0 %copy-start.18 = (bf16[32,2048]{1,0:T(8,128)(2,1)S(1)}, bf16[32,2048]{1,0:T(8,128)(2,1)}, u32[]{:S(2)}) copy-start(bf16[32,2048]{1,0:T(8,128)(2,1)} %param.18) | copy-start | bytes 393220
  4.0 17.0 %copy-start.19 = (bf16[2048,32]{0,1:T(8,128)(2,1)S(1)}, bf16[2048,32]{0,1:T(8,128)(2,1)}, u32[]{:S(2)}) copy-start(bf16[2048,32]{0,1:T(8,128)(2,1)} %param.15) | copy-start | bytes 393220
  4.0 33.3 %all-to-all-start = ((bf16[32,8,2048]{2,1,0:T(8,128)(2,1)}), bf16[32,8,2048]{2,1,0:T(8,128)(2,1)S(1)}, u32[]{:S(2)}, u32[]{:S(2)}) async-start(bf16[32,8,2048]{2,1,0:T(8,128)(2,1)} %bitcast.6), calls=%async_computation | async-start | bytes 2097152 | tf_op jit(solution)/shard_map/all_to_all | solution.py:297
  13.5 13.1 %collective-permute-start.10 = (bf16[224,2048]{1,0:T(8,128)(2,1)S(1)}, bf16[224,2048]{1,0:T(8,128)(2,1)S(1)}, u32[]{:S(2)}, u32[]{:S(2)}) collective-permute-start(bf16[224,2048]{1,0:T(8,128)(2,1)S(1)} %bitcast.40), channel_id=1, source_target_pairs={{0,1},{1,0},{2,3},{3,2},{4,5},{5,4},{6,7},{7,6},{8,9},{9,8},{10,11... | collective-permute-start | bytes 2752520 | tf_op jit(solution)/shard_map/ppermute | solution.py:279
  16.6 10.9 %collective-permute-start.11 = (bf16[224,2048]{1,0:T(8,128)(2,1)}, bf16[224,2048]{1,0:T(8,128)(2,1)S(1)}, u32[]{:S(2)}, u32[]{:S(2)}) collective-permute-start(bf16[224,2048]{1,0:T(8,128)(2,1)} %bitcast.17.refs_2_), channel_id=1, source_target_pairs={{0,1},{1,0},{2,3},{3,2},{4,5},{5,4},{6,7},{7,6},{8,9},{9,8},{10,11... | collective-permute-start | bytes 2752520 | tf_op jit(solution)/shard_map/ppermute | solution.py:280
  18.6 9.9 %collective-permute-start.12 = (bf16[224,2048]{1,0:T(8,128)(2,1)}, bf16[224,2048]{1,0:T(8,128)(2,1)S(1)}, u32[]{:S(2)}, u32[]{:S(2)}) collective-permute-start(bf16[224,2048]{1,0:T(8,128)(2,1)} %bitcast.18.refs_3_), channel_id=1, source_target_pairs={{0,1},{1,0},{2,3},{3,2},{4,5},{5,4},{6,7},{7,6},{8,9},{9,8},{10,11... | collective-permute-start | bytes 2752520 | tf_op jit(solution)/shard_map/ppermute | solution.py:281
  21.0 3.4 %collective-permute-start = (bf16[64,2048]{1,0:T(8,128)(2,1)S(1)}, bf16[64,2048]{1,0:T(8,128)(2,1)S(1)}, u32[]{:S(2)}, u32[]{:S(2)}) collective-permute-start(bf16[64,2048]{1,0:T(8,128)(2,1)S(1)} %pad_maximum_fusion.1), channel_id=1, source_target_pairs={{0,1},{1,0},{2,3},{3,2},{4,5},{5,4},{6,7},{7,6},{8,9},{9,8},{10,11... | collective-permute-start | bytes 786440 | tf_op jit(solution)/shard_map/ppermute | solution.py:49
  24.5 44.2 %collective-permute-start.1 = (bf16[128,2048]{1,0:T(8,128)(2,1)S(1)}, bf16[128,2048]{1,0:T(8,128)(2,1)S(1)}, u32[]{:S(2)}, u32[]{:S(2)}) collective-permute-start(bf16[128,2048]{1,0:T(8,128)(2,1)S(1)} %pad_maximum_fusion.refs_0_), channel_id=1, source_target_pairs={{0,2},{2,4},{4,6},{6,8},{8,10},{10,12},{12,14},{14,0},{1,15},{3,1}... | collective-permute-start | bytes 1572872 | tf_op jit(solution)/shard_map/ppermute | solution.py:55
  37.3 1.2 copy-start.2
  38.5 1.2 copy-start.4
  39.7 1.2 copy-start.6
  46.3 92.2 %all-to-all-start.1 = ((bf16[512,8,128]{2,1,0:T(8,128)(2,1)}), bf16[512,8,128]{2,1,0:T(8,128)(2,1)}, u32[]{:S(2)}, u32[]{:S(2)}) async-start(bf16[512,8,128]{2,1,0:T(8,128)(2,1)} %bitcast.23), calls=%async_computation.1 | async-start | bytes 2097152 | tf_op jit(solution)/shard_map/all_to_all | solution.py:319
  68.7 25.0 %collective-permute-start.2 = (bf16[128,2048]{1,0:T(8,128)(2,1)S(1)}, bf16[128,2048]{1,0:T(8,128)(2,1)S(1)}, u32[]{:S(2)}, u32[]{:S(2)}) collective-permute-start(bf16[128,2048]{1,0:T(8,128)(2,1)S(1)} %collective-permute-done.1.refs_1_), channel_id=1, source_target_pairs={{0,2},{2,4},{4,6},{6,8},{8,10},{10,12},{12,14},{14,0},{1,15},{3,1}... | collective-permute-start | bytes 1572872 | tf_op jit(solution)/shard_map/ppermute | solution.py:55
  93.7 10.2 %collective-permute-start.3 = (bf16[128,2048]{1,0:T(8,128)(2,1)S(1)}, bf16[128,2048]{1,0:T(8,128)(2,1)S(1)}, u32[]{:S(2)}, u32[]{:S(2)}) collective-permute-start(bf16[128,2048]{1,0:T(8,128)(2,1)S(1)} %collective-permute-done.2.refs_2_), channel_id=1, source_target_pairs={{0,2},{2,4},{4,6},{6,8},{8,10},{10,12},{12,14},{14,0},{1,15},{3,1}... | collective-permute-start | bytes 1572872 | tf_op jit(solution)/shard_map/ppermute | solution.py:55
  95.7 16.3 %collective-permute-start.5 = (bf16[128,2048]{1,0:T(8,128)(2,1)S(1)}, bf16[128,2048]{1,0:T(8,128)(2,1)S(1)}, u32[]{:S(2)}, u32[]{:S(2)}) collective-permute-start(bf16[128,2048]{1,0:T(8,128)(2,1)S(1)} %collective-permute-done.1.refs_1_), channel_id=1, source_target_pairs={{0,1},{1,0},{2,3},{3,2},{4,5},{5,4},{6,7},{7,6},{8,9},{9,8},{10,11... | collective-permute-start | bytes 1572872 | tf_op jit(solution)/shard_map/ppermute | solution.py:58
  98.2 13.8 %collective-permute-start.6 = (bf16[128,2048]{1,0:T(8,128)(2,1)S(1)}, bf16[128,2048]{1,0:T(8,128)(2,1)S(1)}, u32[]{:S(2)}, u32[]{:S(2)}) collective-permute-start(bf16[128,2048]{1,0:T(8,128)(2,1)S(1)} %collective-permute-done.2.refs_2_), channel_id=1, source_target_pairs={{0,1},{1,0},{2,3},{3,2},{4,5},{5,4},{6,7},{7,6},{8,9},{9,8},{10,11... | collective-permute-start | bytes 1572872 | tf_op jit(solution)/shard_map/ppermute | solution.py:58
  103.9 8.1 %collective-permute-start.7 = (bf16[128,2048]{1,0:T(8,128)(2,1)S(1)}, bf16[128,2048]{1,0:T(8,128)(2,1)}, u32[]{:S(2)}, u32[]{:S(2)}) collective-permute-start(bf16[128,2048]{1,0:T(8,128)(2,1)S(1)} %collective-permute-done.3.refs_3_), channel_id=1, source_target_pairs={{0,1},{1,0},{2,3},{3,2},{4,5},{5,4},{6,7},{7,6},{8,9},{9,8},{10,11... | collective-permute-start | bytes 1572872 | tf_op jit(solution)/shard_map/ppermute | solution.py:58
  107.0 11.0 %collective-permute-start.4 = (bf16[128,2048]{1,0:T(8,128)(2,1)S(1)}, bf16[128,2048]{1,0:T(8,128)(2,1)}, u32[]{:S(2)}, u32[]{:S(2)}) collective-permute-start(bf16[128,2048]{1,0:T(8,128)(2,1)S(1)} %collective-permute-done.3.refs_3_), channel_id=1, source_target_pairs={{0,2},{2,4},{4,6},{6,8},{8,10},{10,12},{12,14},{14,0},{1,15},{3,1}... | collective-permute-start | bytes 1572872 | tf_op jit(solution)/shard_map/ppermute | solution.py:55
  111.9 6.1 %copy-start.11 = (f32[2048]{0:T(1024)S(1)}, f32[2048]{0:T(1024)}, u32[]{:S(2)}) copy-start(f32[2048]{0:T(1024)} %param.14) | copy-start | bytes 24580
  112.0 6.0 %copy-start.12 = (s32[4]{0:T(128)}, s32[4]{0:T(128)S(1)}, u32[]{:S(2)}) copy-start(s32[4]{0:T(128)S(1)} %pad_add_fusion.place) | copy-start | bytes 52
  119.0 10.8 %copy-start.20 = (bf16[8,64,64]{2,1,0:T(8,128)(2,1)S(1)}, bf16[8,64,64]{2,1,0:T(8,128)(2,1)}, u32[]{:S(2)}) copy-start(bf16[8,64,64]{2,1,0:T(8,128)(2,1)} %param.16) | copy-start | bytes 196612
  124.2 8.5 %collective-permute-start.9 = (bf16[8,512]{1,0:T(8,128)(2,1)}, bf16[8,512]{1,0:T(8,128)(2,1)S(1)}, u32[]{:S(2)}, u32[]{:S(2)}) collective-permute-start(bf16[8,512]{1,0:T(8,128)(2,1)} %get-tuple-element.8), channel_id=1, source_target_pairs={{1,0},{2,1},{3,2},{4,3},{5,4},{6,5},{7,6},{8,7},{9,8},{10,9},{11,1... | collective-permute-start | bytes 24584 | tf_op jit(solution)/shard_map/ppermute | solution.py:25
  127.6 5.1 %collective-permute-start.8 = (bf16[8,512]{1,0:T(8,128)(2,1)}, bf16[8,512]{1,0:T(8,128)(2,1)S(1)}, u32[]{:S(2)}, u32[]{:S(2)}) collective-permute-start(bf16[8,512]{1,0:T(8,128)(2,1)} %get-tuple-element.9), channel_id=1, source_target_pairs={{0,1},{1,2},{2,3},{3,4},{4,5},{5,6},{6,7},{7,8},{8,9},{9,10},{10,1... | collective-permute-start | bytes 24584 | tf_op jit(solution)/shard_map/ppermute | solution.py:24
  (12 other events, 10.0 us)

commit v4 on v3

--- a/solution.py
+++ b/solution.py
@@ -44,49 +44,22 @@
     return (floats * factor * gain).astype(jnp.bfloat16)
 
 
-def gathered_blocks(shard):
-    size = lax.axis_size("y")
-    far = lax.ppermute(shard, "c", SWAP)
-    passed = jnp.concatenate([shard, far], axis=0)
-    ways = [(2 * i, 2 * ((i + 1) % size)) for i in range(size)]
-    ways += [(2 * i + 1, 2 * ((i - 1) % size) + 1) for i in range(size)]
-    blocks = [passed]
-    for _ in range(1, size // 2 + 1):
-        passed = lax.ppermute(passed, TP, ways)
-        blocks.append(passed)
-    for step in range(1, size // 2):
-        blocks.append(lax.ppermute(blocks[step], "c", SWAP))
-    return blocks
-
-
-def fetch(place, blocks, half, rows, done):
-    size = len(blocks)
-    share = rows.shape[0] // (2 * size)
-    y, core = place[0], place[1]
-    sign = 1 - 2 * core
+def fetch(blocks, half, rows, done):
+    share = blocks.shape[1] // 2
     copies = []
-    for k, block in enumerate(blocks):
-        ours = k <= size // 2
-        steps = -k if ours else k - size // 2
-        group = lax.rem(y + sign * steps + size, size)
-        first = core if ours else 1 - core
-        for part in range(2):
-            held = first if part == 0 else 1 - first
-            start = pl.multiple_of((group * 2 + held) * share, share)
-            base = (2 * part + half) * share
-            copy = pltpu.make_async_copy(
-                block.at[pl.ds(base, share), :],
-                rows.at[pl.ds(start, share), :],
-                done.at[2 * k + part],
-            )
-            copy.start()
-            copies.append(copy)
+    for k in range(blocks.shape[0]):
+        copy = pltpu.make_async_copy(
+            blocks.at[k, pl.ds(half * share, share), :],
+            rows.at[pl.ds(k * share, share), :],
+            done.at[k],
+        )
+        copy.start()
+        copies.append(copy)
     return copies
 
 
-def project_body(place, rows, gain, *refs):
-    blocks, pooled, in_rows, done = refs[:-3], refs[-3], refs[-2], refs[-1]
-    copies = fetch(place, blocks, 0, in_rows, done)
+def project_body(rows, gain, blocks, pooled, in_rows, done):
+    copies = fetch(blocks, 0, in_rows, done)
     normed = norm(rows[...], gain[...])
     for copy in copies:
         copy.wait()
@@ -96,9 +69,8 @@
     pooled[...] = product.astype(jnp.bfloat16)
 
 
-def pool_body(place, pooled, low, high, maps, scale, *refs):
-    blocks, out, out_rows, done = refs[:-3], refs[-3], refs[-2], refs[-1]
-    copies = fetch(place, blocks, 1, out_rows, done)
+def pool_body(place, pooled, low, high, maps, scale, blocks, out, out_rows, done):
+    copies = fetch(blocks, 1, out_rows, done)
     count_rows, channels = pooled.shape
     width = low.shape[0]
     pairs = maps.shape[0]
@@ -109,8 +81,8 @@
     )
     shape = (count_rows, channels)
     kind = lax.broadcasted_iota(jnp.int32, shape, 1) // GROUP % 4
-    places = place[2] * count_rows + lax.broadcasted_iota(jnp.int32, shape, 0)
-    length = place[3] * count_rows
+    places = place[0] * count_rows + lax.broadcasted_iota(jnp.int32, shape, 0)
+    length = place[1] * count_rows
     window_sum = jnp.zeros(shape, jnp.float32)
     for k in range(4):
         span = 1 << k
@@ -135,18 +107,11 @@
 def mixer_half(first_batch, mixer_gain, shard, pair_maps, pool_scale):
     count_rows, width = first_batch.shape
     channels = pool_scale.shape[0]
-    blocks = gathered_blocks(shard)
-    place = jnp.stack(
-        [
-            lax.axis_index("y"),
-            lax.axis_index("c"),
-            lax.axis_index(ALL),
-            jnp.int32(lax.axis_size(ALL)),
-        ]
-    ).astype(jnp.int32)
+    blocks = lax.all_gather(shard, TP)
+    place = jnp.stack([lax.axis_index(ALL), jnp.int32(lax.axis_size(ALL))]).astype(jnp.int32)
     held = [
         pltpu.VMEM((channels, width), jnp.bfloat16),
-        pltpu.SemaphoreType.DMA((2 * len(blocks),)),
+        pltpu.SemaphoreType.DMA((blocks.shape[0],)),
     ]
     cost = pl.CostEstimate(
         flops=2 * count_rows * width * channels,
@@ -157,20 +122,20 @@
     pooled_in = pl.pallas_call(
         project_body,
         out_shape=jax.ShapeDtypeStruct((count_rows, channels), jnp.bfloat16),
-        in_specs=[in_scalars(), whole, whole] + [in_place()] * len(blocks),
+        in_specs=[whole, whole, in_place()],
         scratch_shapes=held,
-        compiler_params=limit(10),
+        compiler_params=limit(59),
         cost_estimate=cost,
-    )(place, first_batch, mixer_gain[None, :], *blocks)
+    )(first_batch, mixer_gain[None, :], blocks)
     low, high = neighbours(pooled_in, 8)
     return pl.pallas_call(
         pool_body,
         out_shape=jax.ShapeDtypeStruct((count_rows, width), jnp.bfloat16),
-        in_specs=[in_scalars()] + [whole] * 5 + [in_place()] * len(blocks),
+        in_specs=[in_scalars()] + [whole] * 5 + [in_place()],
         scratch_shapes=held,
-        compiler_params=limit(10),
+        compiler_params=limit(59),
         cost_estimate=cost,
-    )(place, pooled_in, low, high, pair_maps, pool_scale[None, :], *blocks)
+    )(place, pooled_in, low, high, pair_maps, pool_scale[None, :], blocks)
 
 
 def ranked(choice, experts):
@@ -305,7 +270,7 @@
         scratch_shapes=[pltpu.VMEM(incoming.shape, jnp.bfloat16)]
         + [pltpu.VMEM(gate_own.shape, jnp.bfloat16)] * 6
         + [pltpu.VMEM(incoming.shape, jnp.bfloat16), pltpu.SemaphoreType.DMA((PARTS + 7,))],
-        compiler_params=limit(14),
+        compiler_params=limit(60),
         cost_estimate=pl.CostEstimate(
             flops=12 * incoming.size * gate_own.shape[0],
             transcendentals=2 * incoming.shape[0] * gate_own.shape[0],

time: 167 us -> 150 us (0.90)
  the two profiles are of different devices: /device:TPU:265 before, /device:TPU:1 now
where the time goes in v4:
time: 150 us; the launch traced here: 149 us
  waiting for transfers between devices  48.5 us (32%)
  starting transfers between devices  42.4 us (28%)
  Pallas kernels  16.2 us (11%)
  blocking collectives  16.2 us (11%)
  between operations  14.3 us (10%)
  local copies, waits for them, and re-layouts  8.34 us (6%)
  other arithmetic  2.84 us (2%)
    all_to_all x1, waiting for transfers between devices, expert_half(): returned = lax.all_to_all(leaving, ALL, 0, 0, tiled=True)  31.4 us
    all_to_all x1, waiting for transfers between devices, expert_half(): arrived = lax.all_to_all(outgoing, EP, 0, 0, tiled=True)  16.5 us
    all_gather x1, blocking collectives, expert_half(): whole = lax.all_gather(blended, TP)  16.2 us
    all_to_all x1, starting transfers between devices, expert_half(): returned = lax.all_to_all(leaving, ALL, 0, 0, tiled=True)  15.9 us
    all_to_all x1, starting transfers between devices, expert_half(): arrived = lax.all_to_all(outgoing, EP, 0, 0, tiled=True)  13.7 us
    pallas_call x1, Pallas kernels, expert_half(): pl.pallas_call(ffn_body, out_shape=jax.ShapeDtypeStruct(incoming.shape, j...  5.95 us
    unnamed x26, local copies, waits for them, and re-layouts  5.88 us
    pallas_call x1, Pallas kernels, mixer_half(): pl.pallas_call(project_body, out_shape=jax.ShapeDtypeStruct((count_rows,...  4.26 us
  transfers between devices with their start and end apart: 8, of which 3 were waited for; matrix products, arithmetic and copies ran while one was open for 2% of the time, Pallas kernels for 4%

profile of v4, /device:TPU:1, one launch (start us, length us, event | category | flops | bytes accessed | tf_op | source)
XLA Modules:
  0.0 149.0 jit_solution(11689731619151108110)
XLA Ops:
  7.2 1.0 copy-done
  8.3 0.7 copy-done.1
  9.0 0.7 copy-done.2
  9.6 1.7 %shard_map.140 = bf16[256,2048]{1,0:T(8,128)(2,1)} custom-call(s32[1]{0:T(128)} %bitcast.2.core, bf16[128,2048]{1,0:T(8,128)(2,1)S(1)} %copy-done, f32[1,2048]{1,0:T(1,128)S(1)} %bitcast.39, s32[2,128]{1,0:T(2,128)S(1)} %bitcast.40), custom_call_target="tpu_custom_call" | custom-call | flops 134217728 | bytes 1572864 | tf_op jit(solution)/shard_map/pallas_call | solution.py:248
  11.3 1.7 %pad_maximum_fusion = bf16[64,2048]{1,0:T(8,128)(2,1)} fusion(bf16[32,2048]{1,0:T(8,128)(2,1)} %param.18, bf16[32,2048]{1,0:T(8,128)(2,1)} %bitcast.58), kind=kLoop, calls=%fused_computation.1 | loop fusion | flops 524288 | bytes 524288 | tf_op jit(solution)/shard_map/concatenate | solution.py:261
  13.0 13.7 %all-to-all-start = ((bf16[32,8,2048]{2,1,0:T(8,128)(2,1)}), bf16[32,8,2048]{2,1,0:T(8,128)(2,1)S(1)}, u32[]{:S(2)}, u32[]{:S(2)}) async-start(bf16[32,8,2048]{2,1,0:T(8,128)(2,1)} %bitcast.5), calls=%async_computation | async-start | bytes 2097152 | tf_op jit(solution)/shard_map/all_to_all | solution.py:262
  26.7 2.9 %collective-permute-start.2 = (bf16[224,2048]{1,0:T(8,128)(2,1)S(1)}, bf16[224,2048]{1,0:T(8,128)(2,1)S(1)}, u32[]{:S(2)}, u32[]{:S(2)}) collective-permute-start(bf16[224,2048]{1,0:T(8,128)(2,1)S(1)} %bitcast.50), channel_id=1, source_target_pairs={{0,1},{1,0},{2,3},{3,2},{4,5},{5,4},{6,7},{7,6},{8,9},{9,8},{10,11... | collective-permute-start | bytes 2752520 | tf_op jit(solution)/shard_map/ppermute | solution.py:244
  29.6 1.9 %collective-permute-start.3 = (bf16[224,2048]{1,0:T(8,128)(2,1)S(1)}, bf16[224,2048]{1,0:T(8,128)(2,1)S(1)}, u32[]{:S(2)}, u32[]{:S(2)}) collective-permute-start(bf16[224,2048]{1,0:T(8,128)(2,1)S(1)} %bitcast.52), channel_id=1, source_target_pairs={{0,1},{1,0},{2,3},{3,2},{4,5},{5,4},{6,7},{7,6},{8,9},{9,8},{10,11... | collective-permute-start | bytes 2752520 | tf_op jit(solution)/shard_map/ppermute | solution.py:245
  31.5 2.4 %collective-permute-start.4 = (bf16[224,2048]{1,0:T(8,128)(2,1)}, bf16[224,2048]{1,0:T(8,128)(2,1)}, u32[]{:S(2)}, u32[]{:S(2)}) collective-permute-start(bf16[224,2048]{1,0:T(8,128)(2,1)} %bitcast.53), channel_id=1, source_target_pairs={{0,1},{1,0},{2,3},{3,2},{4,5},{5,4},{6,7},{7,6},{8,9},{9,8},{10,11... | collective-permute-start | bytes 2752520 | tf_op jit(solution)/shard_map/ppermute | solution.py:246
  34.0 0.9 copy-done.8
  34.9 1.0 copy-done.9
  36.4 16.5 %all-to-all-done = bf16[32,8,2048]{2,1,0:T(8,128)(2,1)S(1)} async-done(((bf16[32,8,2048]{2,1,0:T(8,128)(2,1)}), bf16[32,8,2048]{2,1,0:T(8,128)(2,1)S(1)}, u32[]{:S(2)}, u32[]{:S(2)}) %all-to-all-start) | async-done | bytes 1048608 | tf_op jit(solution)/shard_map/all_to_all | solution.py:262
  52.9 1.0 copy-done.5
  53.9 6.0 %shard_map.144 = bf16[256,2048]{1,0:T(8,128)(2,1)} custom-call(bf16[256,2048]{1,0:T(8,128)(2,1)} %bitcast.47, bf16[224,2048]{1,0:T(8,128)(2,1)} %bitcast.49, bf16[224,2048]{1,0:T(8,128)(2,1)} %bitcast.51, bf16[224,2048]{1,0:T(8,128)(2,1)} %bitcast.54, bf16[224,2048]{1,0:T(8,128)(2,1)} %copy-done.8, bf16[224,2048]{1,0:T(8,128)(2,1)} %copy-done.9, ...), custom_call_target="tpu_custom_call" | custom-call | flops 1409286144 | bytes 7602176 | tf_op jit(solution)/shard_map/pallas_call | solution.py:265
  59.9 15.9 %all-to-all-start.1 = ((bf16[512,8,128]{2,1,0:T(8,128)(2,1)}), bf16[512,8,128]{2,1,0:T(8,128)(2,1)S(1)}, u32[]{:S(2)}, u32[]{:S(2)}) async-start(bf16[512,8,128]{2,1,0:T(8,128)(2,1)} %bitcast.46), calls=%async_computation.1 | async-start | bytes 2097152 | tf_op jit(solution)/shard_map/all_to_all | solution.py:284
  76.1 0.8 reshape.36.maps
  78.0 31.4 %all-to-all-done.1 = bf16[512,8,128]{2,1,0:T(8,128)(2,1)S(1)} async-done(((bf16[512,8,128]{2,1,0:T(8,128)(2,1)}), bf16[512,8,128]{2,1,0:T(8,128)(2,1)S(1)}, u32[]{:S(2)}, u32[]{:S(2)}) %all-to-all-start.1) | async-done | bytes 1048608 | tf_op jit(solution)/shard_map/all_to_all | solution.py:284
  109.9 4.3 %shard_map.141.pooled = bf16[128,512]{1,0:T(8,128)(2,1)} custom-call(bf16[128,2048]{1,0:T(8,128)(2,1)} %rows.3, f32[1,2048]{1,0:T(1,128)} %bitcast.59, bf16[16,64,2048]{2,1,0:T(8,128)(2,1)} %bitcast.43), custom_call_target="tpu_custom_call" | custom-call | flops 268435456 | bytes 4194304 | tf_op jit(solution)/shard_map/pallas_call | solution.py:122
  114.1 0.7 fusion.1
  114.8 2.1 %collective-permute-start.1 = (bf16[8,512]{1,0:T(8,128)(2,1)S(1)}, bf16[8,512]{1,0:T(8,128)(2,1)S(1)}, u32[]{:S(2)}, u32[]{:S(2)}) collective-permute-start(bf16[8,512]{1,0:T(8,128)(2,1)S(1)} %get-tuple-element.8), channel_id=1, source_target_pairs={{1,0},{2,1},{3,2},{4,3},{5,4},{6,5},{7,6},{8,7},{9,8},{10,9},{11,1... | collective-permute-start | bytes 24584 | tf_op jit(solution)/shard_map/ppermute | solution.py:25
  117.0 3.4 %collective-permute-start = (bf16[8,512]{1,0:T(8,128)(2,1)S(1)}, bf16[8,512]{1,0:T(8,128)(2,1)S(1)}, u32[]{:S(2)}, u32[]{:S(2)}) collective-permute-start(bf16[8,512]{1,0:T(8,128)(2,1)S(1)} %get-tuple-element.9), channel_id=1, source_target_pairs={{0,1},{1,2},{2,3},{3,4},{4,5},{5,6},{6,7},{7,8},{8,9},{9,10},{10,1... | collective-permute-start | bytes 24584 | tf_op jit(solution)/shard_map/ppermute | solution.py:24
  120.4 16.2 %all-gather.1 = bf16[2048,128]{1,0:T(8,128)(2,1)S(1)} all-gather(bf16[128,128]{1,0:T(8,128)(2,1)S(1)} %fusion), channel_id=3, replica_groups=mesh['z'=8,'x'=4,'y'=8,'c'=2] {'y','c'}, dimensions={0}, use_global_device_ids=true | all-gather | bytes 557056 | tf_op jit(solution)/shard_map/all_gather | solution.py:299
  136.6 0.9 copy.18
  138.2 4.0 %shard_map.142 = bf16[128,2048]{1,0:T(8,128)(2,1)} custom-call(s32[2]{0:T(128)} %pad_add_fusion.place, bf16[128,512]{1,0:T(8,128)(2,1)} %shard_map.141.pooled, bf16[8,512]{1,0:T(8,128)(2,1)} %copy-done.12, bf16[8,512]{1,0:T(8,128)(2,1)} %copy-done.11, bf16[4,128,128]{2,1,0:T(8,128)(2,1)} %reshape.36.maps, f32[1,512]{1,0:T(1,128)} %bitcast.60, ...), custom_call_target="tpu_custom_call" | custom-call | flops 268435456 | bytes 4194304 | tf_op jit(solution)/shard_map/pallas_call | solution.py:131
  (35 shorter events, 3.0 us)
Async XLA Ops:
  7.2 102.7 %all-gather.4.cloned.1.call-start = ((), (), s32[]{:S(2)}) async-start(), calls=%async_computation.2 | async-start | bytes 4456448 | tf_op jit(solution)/shard_map/all_gather | solution.py:110
  7.2 1.0 copy-start
  8.3 0.7 copy-start.1
  9.0 0.7 copy-start.2
  9.6 17.1 %copy-start.6 = (bf16[1,2048,224]{1,2,0:T(8,128)(2,1)S(1)}, bf16[1,2048,224]{1,2,0:T(8,128)(2,1)}, u32[]{:S(2)}) copy-start(bf16[1,2048,224]{1,2,0:T(8,128)(2,1)} %param.23) | copy-start | bytes 2752516
  9.6 20.0 %copy-start.7 = (bf16[1,2048,224]{1,2,0:T(8,128)(2,1)S(1)}, bf16[1,2048,224]{1,2,0:T(8,128)(2,1)}, u32[]{:S(2)}) copy-start(bf16[1,2048,224]{1,2,0:T(8,128)(2,1)} %param.24) | copy-start | bytes 2752516
  13.0 39.9 %all-to-all-start = ((bf16[32,8,2048]{2,1,0:T(8,128)(2,1)}), bf16[32,8,2048]{2,1,0:T(8,128)(2,1)S(1)}, u32[]{:S(2)}, u32[]{:S(2)}) async-start(bf16[32,8,2048]{2,1,0:T(8,128)(2,1)} %bitcast.5), calls=%async_computation | async-start | bytes 2097152 | tf_op jit(solution)/shard_map/all_to_all | solution.py:262
  26.7 7.2 %collective-permute-start.2 = (bf16[224,2048]{1,0:T(8,128)(2,1)S(1)}, bf16[224,2048]{1,0:T(8,128)(2,1)S(1)}, u32[]{:S(2)}, u32[]{:S(2)}) collective-permute-start(bf16[224,2048]{1,0:T(8,128)(2,1)S(1)} %bitcast.50), channel_id=1, source_target_pairs={{0,1},{1,0},{2,3},{3,2},{4,5},{5,4},{6,7},{7,6},{8,9},{9,8},{10,11... | collective-permute-start | bytes 2752520 | tf_op jit(solution)/shard_map/ppermute | solution.py:244
  29.6 4.4 %collective-permute-start.3 = (bf16[224,2048]{1,0:T(8,128)(2,1)S(1)}, bf16[224,2048]{1,0:T(8,128)(2,1)S(1)}, u32[]{:S(2)}, u32[]{:S(2)}) collective-permute-start(bf16[224,2048]{1,0:T(8,128)(2,1)S(1)} %bitcast.52), channel_id=1, source_target_pairs={{0,1},{1,0},{2,3},{3,2},{4,5},{5,4},{6,7},{7,6},{8,9},{9,8},{10,11... | collective-permute-start | bytes 2752520 | tf_op jit(solution)/shard_map/ppermute | solution.py:245
  31.5 4.8 %collective-permute-start.4 = (bf16[224,2048]{1,0:T(8,128)(2,1)}, bf16[224,2048]{1,0:T(8,128)(2,1)}, u32[]{:S(2)}, u32[]{:S(2)}) collective-permute-start(bf16[224,2048]{1,0:T(8,128)(2,1)} %bitcast.53), channel_id=1, source_target_pairs={{0,1},{1,0},{2,3},{3,2},{4,5},{5,4},{6,7},{7,6},{8,9},{9,8},{10,11... | collective-permute-start | bytes 2752520 | tf_op jit(solution)/shard_map/ppermute | solution.py:246
  34.0 0.9 copy-start.8
  34.9 1.0 copy-start.9
  52.9 1.0 copy-start.5
  53.9 21.9 %copy-start.10 = (bf16[8,64,64]{2,1,0:T(8,128)(2,1)S(1)}, bf16[8,64,64]{2,1,0:T(8,128)(2,1)}, u32[]{:S(2)}) copy-start(bf16[8,64,64]{2,1,0:T(8,128)(2,1)} %param.16) | copy-start | bytes 196612
  53.9 23.0 %copy-start.3 = (s32[128,2]{0,1:T(2,128)S(1)}, s32[128,2]{0,1:T(2,128)}, u32[]{:S(2)}) copy-start(s32[128,2]{0,1:T(2,128)} %param.21) | copy-start | bytes 3076
  53.9 23.0 %copy-start.4 = (f32[128,2]{0,1:T(2,128)S(1)}, f32[128,2]{0,1:T(2,128)}, u32[]{:S(2)}) copy-start(f32[128,2]{0,1:T(2,128)} %param.22) | copy-start | bytes 3076
  59.9 49.5 %all-to-all-start.1 = ((bf16[512,8,128]{2,1,0:T(8,128)(2,1)}), bf16[512,8,128]{2,1,0:T(8,128)(2,1)S(1)}, u32[]{:S(2)}, u32[]{:S(2)}) async-start(bf16[512,8,128]{2,1,0:T(8,128)(2,1)} %bitcast.46), calls=%async_computation.1 | async-start | bytes 2097152 | tf_op jit(solution)/shard_map/all_to_all | solution.py:284
  114.8 22.7 %collective-permute-start.1 = (bf16[8,512]{1,0:T(8,128)(2,1)S(1)}, bf16[8,512]{1,0:T(8,128)(2,1)S(1)}, u32[]{:S(2)}, u32[]{:S(2)}) collective-permute-start(bf16[8,512]{1,0:T(8,128)(2,1)S(1)} %get-tuple-element.8), channel_id=1, source_target_pairs={{1,0},{2,1},{3,2},{4,3},{5,4},{6,5},{7,6},{8,7},{9,8},{10,9},{11,1... | collective-permute-start | bytes 24584 | tf_op jit(solution)/shard_map/ppermute | solution.py:25
  117.0 20.6 %collective-permute-start = (bf16[8,512]{1,0:T(8,128)(2,1)S(1)}, bf16[8,512]{1,0:T(8,128)(2,1)S(1)}, u32[]{:S(2)}, u32[]{:S(2)}) collective-permute-start(bf16[8,512]{1,0:T(8,128)(2,1)S(1)} %get-tuple-element.9), channel_id=1, source_target_pairs={{0,1},{1,2},{2,3},{3,4},{4,5},{5,6},{6,7},{7,8},{8,9},{9,10},{10,1... | collective-permute-start | bytes 24584 | tf_op jit(solution)/shard_map/ppermute | solution.py:24
  137.6 0.6 copy-start.11
  137.6 0.6 copy-start.12
Sparse Core Ops, SparseCore 0:
  13.1 50.3 all-gather.3

commit v5 on v4

--- a/solution.py
+++ b/solution.py
@@ -159,13 +159,22 @@
     return dot(jnp.where(match, 1.0, 0.0).astype(jnp.bfloat16), values)
 
 
-def dispatch_body(core, rows, gain, choice, out):
+def dispatch_body(core, rows_from, gain_from, choice_from, out, rows, gain, choice, done):
+    copies = []
+    for k, (source, held) in enumerate(
+        ((choice_from, choice), (rows_from, rows), (gain_from, gain))
+    ):
+        copies.append(pltpu.make_async_copy(source, held, done.at[k]))
+        copies[-1].start()
     count = rows.shape[0]
     slots = out.shape[0]
     half = slots // EXPERTS
+    slot = core[0] * half + lax.broadcasted_iota(jnp.int32, (slots, count), 0) % half
+    copies[0].wait()
     rank = repeated(ranked(choice[...], EXPERTS)[2], half)
-    slot = core[0] * half + lax.broadcasted_iota(jnp.int32, (slots, count), 0) % half
     spread = jnp.where(rank == slot.astype(jnp.float32), 1.0, 0.0).astype(jnp.bfloat16)
+    copies[1].wait()
+    copies[2].wait()
     out[...] = dot(spread, norm(rows[...], gain[...])).astype(jnp.bfloat16)
 
 
@@ -248,8 +257,14 @@
     outgoing = pl.pallas_call(
         dispatch_body,
         out_shape=jax.ShapeDtypeStruct((experts * half_slots, model_width), jnp.bfloat16),
-        in_specs=[in_scalars()] + [pl.BlockSpec()] * 3,
-        compiler_params=limit(8),
+        in_specs=[in_scalars()] + [in_place()] * 3,
+        scratch_shapes=[
+            pltpu.VMEM(second_batch.shape, second_batch.dtype),
+            pltpu.VMEM((1, model_width), jnp.float32),
+            pltpu.VMEM((expert_choice.shape[1], row_count), jnp.int32),
+            pltpu.SemaphoreType.DMA((3,)),
+        ],
+        compiler_params=limit(61),
         cost_estimate=pl.CostEstimate(
             flops=2 * experts * half_slots * second_batch.size,
             transcendentals=row_count,
@@ -270,7 +285,7 @@
         scratch_shapes=[pltpu.VMEM(incoming.shape, jnp.bfloat16)]
         + [pltpu.VMEM(gate_own.shape, jnp.bfloat16)] * 6
         + [pltpu.VMEM(incoming.shape, jnp.bfloat16), pltpu.SemaphoreType.DMA((PARTS + 7,))],
-        compiler_params=limit(60),
+        compiler_params=limit(51),
         cost_estimate=pl.CostEstimate(
             flops=12 * incoming.size * gate_own.shape[0],
             transcendentals=2 * incoming.shape[0] * gate_own.shape[0],

time: 150 us -> 147 us (0.980)
  local copies, waits for them, and re-layouts: 8.34 us -> 4.96 us
    unnamed x26 -> x20, local copies, waits for them, and re-layouts: 5.88 us -> 2.5 us
where the time goes in v5:
time: 147 us
  waiting for transfers between devices  48.5 us (33%)
  starting transfers between devices  42.5 us (29%)
  Pallas kernels  17.1 us (12%)
  blocking collectives  16.2 us (11%)
  between operations  14.3 us (10%)
  local copies, waits for them, and re-layouts  4.96 us (3%)
  other arithmetic  2.83 us (2%)
    all_to_all x1, waiting for transfers between devices, expert_half(): returned = lax.all_to_all(leaving, ALL, 0, 0, tiled=True)  31.4 us
    all_to_all x1, waiting for transfers between devices, expert_half(): arrived = lax.all_to_all(outgoing, EP, 0, 0, tiled=True)  16.7 us
    all_gather x1, blocking collectives, expert_half(): whole = lax.all_gather(blended, TP)  16.2 us
    all_to_all x1, starting transfers between devices, expert_half(): returned = lax.all_to_all(leaving, ALL, 0, 0, tiled=True)  15.9 us
    all_to_all x1, starting transfers between devices, expert_half(): arrived = lax.all_to_all(outgoing, EP, 0, 0, tiled=True)  13.8 us
    pallas_call x1, Pallas kernels, expert_half(): pl.pallas_call(ffn_body, out_shape=jax.ShapeDtypeStruct(incoming.shape, j...  5.72 us
    pallas_call x1, Pallas kernels, mixer_half(): pl.pallas_call(project_body, out_shape=jax.ShapeDtypeStruct((count_rows,...  4.26 us
    pallas_call x1, Pallas kernels, mixer_half(): pl.pallas_call(pool_body, out_shape=jax.ShapeDtypeStruct((count_rows, wid...  3.97 us
  transfers between devices with their start and end apart: 8, of which 3 were waited for; matrix products, arithmetic and copies ran while one was open for 2% of the time, Pallas kernels for 4%

profile of v5, /device:TPU:1, one launch (start us, length us, event | category | flops | bytes accessed | tf_op | source)
XLA Modules:
  0.0 146.7 jit_solution(3078752278475718444)
XLA Ops:
  7.2 2.8 %shard_map.140 = bf16[256,2048]{1,0:T(8,128)(2,1)} custom-call(s32[1]{0:T(128)} %bitcast.2.core, bf16[128,2048]{1,0:T(8,128)(2,1)} %rows_from.1, f32[1,2048]{1,0:T(1,128)} %bitcast.58, s32[2,128]{1,0:T(2,128)} %bitcast.45), custom_call_target="tpu_custom_call" | custom-call | flops 134217728 | bytes 1572864 | tf_op jit(solution)/shard_map/pallas_call | solution.py:257
  10.1 1.7 %pad_maximum_fusion = bf16[64,2048]{1,0:T(8,128)(2,1)} fusion(bf16[32,2048]{1,0:T(8,128)(2,1)} %param.18, bf16[32,2048]{1,0:T(8,128)(2,1)} %bitcast.57), kind=kLoop, calls=%fused_computation.1 | loop fusion | flops 524288 | bytes 524288 | tf_op jit(solution)/shard_map/concatenate | solution.py:276
  11.8 13.8 %all-to-all-start = ((bf16[32,8,2048]{2,1,0:T(8,128)(2,1)}), bf16[32,8,2048]{2,1,0:T(8,128)(2,1)}, u32[]{:S(2)}, u32[]{:S(2)}) async-start(bf16[32,8,2048]{2,1,0:T(8,128)(2,1)} %bitcast.51), calls=%async_computation | async-start | bytes 2097152 | tf_op jit(solution)/shard_map/all_to_all | solution.py:277
  25.6 2.9 %collective-permute-start.2 = (bf16[224,2048]{1,0:T(8,128)(2,1)S(1)}, bf16[224,2048]{1,0:T(8,128)(2,1)S(1)}, u32[]{:S(2)}, u32[]{:S(2)}) collective-permute-start(bf16[224,2048]{1,0:T(8,128)(2,1)S(1)} %bitcast.39), channel_id=1, source_target_pairs={{0,1},{1,0},{2,3},{3,2},{4,5},{5,4},{6,7},{7,6},{8,9},{9,8},{10,11... | collective-permute-start | bytes 2752520 | tf_op jit(solution)/shard_map/ppermute | solution.py:253
  28.5 1.9 %collective-permute-start.3 = (bf16[224,2048]{1,0:T(8,128)(2,1)S(1)}, bf16[224,2048]{1,0:T(8,128)(2,1)S(1)}, u32[]{:S(2)}, u32[]{:S(2)}) collective-permute-start(bf16[224,2048]{1,0:T(8,128)(2,1)S(1)} %bitcast.41), channel_id=1, source_target_pairs={{0,1},{1,0},{2,3},{3,2},{4,5},{5,4},{6,7},{7,6},{8,9},{9,8},{10,11... | collective-permute-start | bytes 2752520 | tf_op jit(solution)/shard_map/ppermute | solution.py:254
  30.5 2.4 %collective-permute-start.4 = (bf16[224,2048]{1,0:T(8,128)(2,1)S(1)}, bf16[224,2048]{1,0:T(8,128)(2,1)}, u32[]{:S(2)}, u32[]{:S(2)}) collective-permute-start(bf16[224,2048]{1,0:T(8,128)(2,1)S(1)} %bitcast.43), channel_id=1, source_target_pairs={{0,1},{1,0},{2,3},{3,2},{4,5},{5,4},{6,7},{7,6},{8,9},{9,8},{10,11... | collective-permute-start | bytes 2752520 | tf_op jit(solution)/shard_map/ppermute | solution.py:255
  32.9 0.9 copy-done.5
  33.8 1.0 copy-done.6
  35.1 16.7 %all-to-all-done = bf16[32,8,2048]{2,1,0:T(8,128)(2,1)} async-done(((bf16[32,8,2048]{2,1,0:T(8,128)(2,1)}), bf16[32,8,2048]{2,1,0:T(8,128)(2,1)}, u32[]{:S(2)}, u32[]{:S(2)}) %all-to-all-start) | async-done | bytes 1048608 | tf_op jit(solution)/shard_map/all_to_all | solution.py:277
  51.8 5.7 %shard_map.144 = bf16[256,2048]{1,0:T(8,128)(2,1)} custom-call(bf16[256,2048]{1,0:T(8,128)(2,1)} %bitcast.13.refs_0_, bf16[224,2048]{1,0:T(8,128)(2,1)S(1)} %bitcast.40, bf16[224,2048]{1,0:T(8,128)(2,1)S(1)} %bitcast.42, bf16[224,2048]{1,0:T(8,128)(2,1)S(1)} %bitcast.44, bf16[224,2048]{1,0:T(8,128)(2,1)} %copy-done.5, bf16[224,2048]{1,0:T(8,128)(2,1)} %copy-done.6, ...), custom_call_target="tpu_custom_call" | custom-call | flops 1409286144 | bytes 7602176 | tf_op jit(solution)/shard_map/pallas_call | solution.py:280
  57.5 15.9 %all-to-all-start.1 = ((bf16[512,8,128]{2,1,0:T(8,128)(2,1)}), bf16[512,8,128]{2,1,0:T(8,128)(2,1)S(1)}, u32[]{:S(2)}, u32[]{:S(2)}) async-start(bf16[512,8,128]{2,1,0:T(8,128)(2,1)} %bitcast.52), calls=%async_computation.1 | async-start | bytes 2097152 | tf_op jit(solution)/shard_map/all_to_all | solution.py:299
  73.5 0.3 multiply_bitcast_fusion
  73.8 0.8 reshape.36.maps
  74.6 0.4 shard_map.143
  75.0 0.7 pad_add_fusion.place
  75.6 31.4 %all-to-all-done.1 = bf16[512,8,128]{2,1,0:T(8,128)(2,1)S(1)} async-done(((bf16[512,8,128]{2,1,0:T(8,128)(2,1)}), bf16[512,8,128]{2,1,0:T(8,128)(2,1)S(1)}, u32[]{:S(2)}, u32[]{:S(2)}) %all-to-all-start.1) | async-done | bytes 1048608 | tf_op jit(solution)/shard_map/all_to_all | solution.py:299
  107.5 4.3 %shard_map.141.pooled = bf16[128,512]{1,0:T(8,128)(2,1)} custom-call(bf16[128,2048]{1,0:T(8,128)(2,1)} %rows.1, f32[1,2048]{1,0:T(1,128)} %bitcast.59, bf16[16,64,2048]{2,1,0:T(8,128)(2,1)} %bitcast.48), custom_call_target="tpu_custom_call" | custom-call | flops 268435456 | bytes 4194304 | tf_op jit(solution)/shard_map/pallas_call | solution.py:122
  111.8 0.7 fusion.1
  112.5 2.1 %collective-permute-start.1 = (bf16[8,512]{1,0:T(8,128)(2,1)S(1)}, bf16[8,512]{1,0:T(8,128)(2,1)S(1)}, u32[]{:S(2)}, u32[]{:S(2)}) collective-permute-start(bf16[8,512]{1,0:T(8,128)(2,1)S(1)} %get-tuple-element.8), channel_id=1, source_target_pairs={{1,0},{2,1},{3,2},{4,3},{5,4},{6,5},{7,6},{8,7},{9,8},{10,9},{11,1... | collective-permute-start | bytes 24584 | tf_op jit(solution)/shard_map/ppermute | solution.py:25
  114.6 3.5 %collective-permute-start = (bf16[8,512]{1,0:T(8,128)(2,1)S(1)}, bf16[8,512]{1,0:T(8,128)(2,1)S(1)}, u32[]{:S(2)}, u32[]{:S(2)}) collective-permute-start(bf16[8,512]{1,0:T(8,128)(2,1)S(1)} %get-tuple-element.9), channel_id=1, source_target_pairs={{0,1},{1,2},{2,3},{3,4},{4,5},{5,6},{6,7},{7,8},{8,9},{9,10},{10,1... | collective-permute-start | bytes 24584 | tf_op jit(solution)/shard_map/ppermute | solution.py:24
  118.1 16.2 %all-gather.1 = bf16[2048,128]{1,0:T(8,128)(2,1)S(1)} all-gather(bf16[128,128]{1,0:T(8,128)(2,1)S(1)} %fusion), channel_id=3, replica_groups=mesh['z'=8,'x'=4,'y'=8,'c'=2] {'y','c'}, dimensions={0}, use_global_device_ids=true | all-gather | bytes 557056 | tf_op jit(solution)/shard_map/all_gather | solution.py:314
  134.3 0.9 copy.18
  135.3 0.6 copy-done.8
  135.9 4.0 %shard_map.142 = bf16[128,2048]{1,0:T(8,128)(2,1)} custom-call(s32[2]{0:T(128)} %pad_add_fusion.place, bf16[128,512]{1,0:T(8,128)(2,1)} %shard_map.141.pooled, bf16[8,512]{1,0:T(8,128)(2,1)} %copy-done.9, bf16[8,512]{1,0:T(8,128)(2,1)} %copy-done.8, bf16[4,128,128]{2,1,0:T(8,128)(2,1)} %reshape.36.maps, f32[1,512]{1,0:T(1,128)} %bitcast.60, ...), custom_call_target="tpu_custom_call" | custom-call | flops 268435456 | bytes 4194304 | tf_op jit(solution)/shard_map/pallas_call | solution.py:131
  (29 shorter events, 0.9 us)
Async XLA Ops:
  7.2 18.5 %copy-start = (bf16[1,2048,224]{1,2,0:T(8,128)(2,1)S(1)}, bf16[1,2048,224]{1,2,0:T(8,128)(2,1)}, u32[]{:S(2)}) copy-start(bf16[1,2048,224]{1,2,0:T(8,128)(2,1)} %param.23) | copy-start | bytes 2752516
  7.2 21.3 %copy-start.1 = (bf16[1,2048,224]{1,2,0:T(8,128)(2,1)S(1)}, bf16[1,2048,224]{1,2,0:T(8,128)(2,1)}, u32[]{:S(2)}) copy-start(bf16[1,2048,224]{1,2,0:T(8,128)(2,1)} %param.24) | copy-start | bytes 2752516
  7.2 23.3 %copy-start.2 = (bf16[1,224,2048]{2,1,0:T(8,128)(2,1)S(1)}, bf16[1,224,2048]{2,1,0:T(8,128)(2,1)}, u32[]{:S(2)}) copy-start(bf16[1,224,2048]{2,1,0:T(8,128)(2,1)} %param.25) | copy-start | bytes 2752516
  7.2 100.3 %all-gather.4.cloned.1.call-start = ((), (), s32[]{:S(2)}) async-start(), calls=%async_computation.2 | async-start | bytes 4456448 | tf_op jit(solution)/shard_map/all_gather | solution.py:110
  11.8 40.0 %all-to-all-start = ((bf16[32,8,2048]{2,1,0:T(8,128)(2,1)}), bf16[32,8,2048]{2,1,0:T(8,128)(2,1)}, u32[]{:S(2)}, u32[]{:S(2)}) async-start(bf16[32,8,2048]{2,1,0:T(8,128)(2,1)} %bitcast.51), calls=%async_computation | async-start | bytes 2097152 | tf_op jit(solution)/shard_map/all_to_all | solution.py:277
  25.6 7.2 %collective-permute-start.2 = (bf16[224,2048]{1,0:T(8,128)(2,1)S(1)}, bf16[224,2048]{1,0:T(8,128)(2,1)S(1)}, u32[]{:S(2)}, u32[]{:S(2)}) collective-permute-start(bf16[224,2048]{1,0:T(8,128)(2,1)S(1)} %bitcast.39), channel_id=1, source_target_pairs={{0,1},{1,0},{2,3},{3,2},{4,5},{5,4},{6,7},{7,6},{8,9},{9,8},{10,11... | collective-permute-start | bytes 2752520 | tf_op jit(solution)/shard_map/ppermute | solution.py:253
  28.5 4.4 %collective-permute-start.3 = (bf16[224,2048]{1,0:T(8,128)(2,1)S(1)}, bf16[224,2048]{1,0:T(8,128)(2,1)S(1)}, u32[]{:S(2)}, u32[]{:S(2)}) collective-permute-start(bf16[224,2048]{1,0:T(8,128)(2,1)S(1)} %bitcast.41), channel_id=1, source_target_pairs={{0,1},{1,0},{2,3},{3,2},{4,5},{5,4},{6,7},{7,6},{8,9},{9,8},{10,11... | collective-permute-start | bytes 2752520 | tf_op jit(solution)/shard_map/ppermute | solution.py:254
  30.5 4.6 %collective-permute-start.4 = (bf16[224,2048]{1,0:T(8,128)(2,1)S(1)}, bf16[224,2048]{1,0:T(8,128)(2,1)}, u32[]{:S(2)}, u32[]{:S(2)}) collective-permute-start(bf16[224,2048]{1,0:T(8,128)(2,1)S(1)} %bitcast.43), channel_id=1, source_target_pairs={{0,1},{1,0},{2,3},{3,2},{4,5},{5,4},{6,7},{7,6},{8,9},{9,8},{10,11... | collective-permute-start | bytes 2752520 | tf_op jit(solution)/shard_map/ppermute | solution.py:255
  32.9 0.9 copy-start.5
  33.8 1.0 copy-start.6
  51.8 21.6 %copy-start.7 = (bf16[8,64,64]{2,1,0:T(8,128)(2,1)S(1)}, bf16[8,64,64]{2,1,0:T(8,128)(2,1)}, u32[]{:S(2)}) copy-start(bf16[8,64,64]{2,1,0:T(8,128)(2,1)} %param.16) | copy-start | bytes 196612
  51.8 22.8 %copy-start.3 = (s32[128,2]{0,1:T(2,128)S(1)}, s32[128,2]{0,1:T(2,128)}, u32[]{:S(2)}) copy-start(s32[128,2]{0,1:T(2,128)} %param.21) | copy-start | bytes 3076
  51.8 22.8 %copy-start.4 = (f32[128,2]{0,1:T(2,128)S(1)}, f32[128,2]{0,1:T(2,128)}, u32[]{:S(2)}) copy-start(f32[128,2]{0,1:T(2,128)} %param.22) | copy-start | bytes 3076
  57.5 49.5 %all-to-all-start.1 = ((bf16[512,8,128]{2,1,0:T(8,128)(2,1)}), bf16[512,8,128]{2,1,0:T(8,128)(2,1)S(1)}, u32[]{:S(2)}, u32[]{:S(2)}) async-start(bf16[512,8,128]{2,1,0:T(8,128)(2,1)} %bitcast.52), calls=%async_computation.1 | async-start | bytes 2097152 | tf_op jit(solution)/shard_map/all_to_all | solution.py:299
  112.5 22.7 %collective-permute-start.1 = (bf16[8,512]{1,0:T(8,128)(2,1)S(1)}, bf16[8,512]{1,0:T(8,128)(2,1)S(1)}, u32[]{:S(2)}, u32[]{:S(2)}) collective-permute-start(bf16[8,512]{1,0:T(8,128)(2,1)S(1)} %get-tuple-element.8), channel_id=1, source_target_pairs={{1,0},{2,1},{3,2},{4,3},{5,4},{6,5},{7,6},{8,7},{9,8},{10,9},{11,1... | collective-permute-start | bytes 24584 | tf_op jit(solution)/shard_map/ppermute | solution.py:25
  114.6 20.6 %collective-permute-start = (bf16[8,512]{1,0:T(8,128)(2,1)S(1)}, bf16[8,512]{1,0:T(8,128)(2,1)S(1)}, u32[]{:S(2)}, u32[]{:S(2)}) collective-permute-start(bf16[8,512]{1,0:T(8,128)(2,1)S(1)} %get-tuple-element.9), channel_id=1, source_target_pairs={{0,1},{1,2},{2,3},{3,4},{4,5},{5,6},{6,7},{7,8},{8,9},{9,10},{10,1... | collective-permute-start | bytes 24584 | tf_op jit(solution)/shard_map/ppermute | solution.py:24
  135.2 0.6 copy-start.8
  135.3 0.6 copy-start.9
Sparse Core Ops, SparseCore 0:
  11.9 49.9 all-gather.3

commit v6 on v5

--- a/solution.py
+++ b/solution.py
@@ -58,27 +58,32 @@
     return copies
 
 
-def project_body(rows, gain, blocks, pooled, in_rows, done):
-    copies = fetch(blocks, 0, in_rows, done)
-    normed = norm(rows[...], gain[...])
+def projected(rows, gain, in_rows):
+    product = lax.dot_general(
+        norm(rows, gain), in_rows, (((1,), (1,)), ((), ())), preferred_element_type=jnp.float32
+    )
+    return product.astype(jnp.bfloat16).astype(jnp.float32)
+
+
+def mixer_body(place, gain, maps, scale, rows_from, low_from, high_from, blocks, out, *held):
+    rows, low, high, in_rows, out_rows, done_rows, done_in, done_out = held
+    copies = []
+    for k, (source, target) in enumerate(((rows_from, rows), (low_from, low), (high_from, high))):
+        copies.append(pltpu.make_async_copy(source, target, done_rows.at[k]))
+        copies[-1].start()
+    copies += fetch(blocks, 0, in_rows, done_in)
+    later = fetch(blocks, 1, out_rows, done_out)
     for copy in copies:
         copy.wait()
-    product = lax.dot_general(
-        normed, in_rows[...], (((1,), (1,)), ((), ())), preferred_element_type=jnp.float32
-    )
-    pooled[...] = product.astype(jnp.bfloat16)
-
-
-def pool_body(place, pooled, low, high, maps, scale, blocks, out, out_rows, done):
-    copies = fetch(blocks, 1, out_rows, done)
-    count_rows, channels = pooled.shape
+    count_rows, channels = rows.shape[0], scale.shape[1]
     width = low.shape[0]
     pairs = maps.shape[0]
     lanes = maps.shape[1]
-    middle = pooled[...].astype(jnp.float32)
-    sums = jnp.concatenate(
-        [low[...].astype(jnp.float32), middle, high[...].astype(jnp.float32)], axis=0
-    )
+    weights = in_rows[...]
+    edges = jnp.concatenate([low[...].astype(jnp.float32), high[...].astype(jnp.float32)], axis=0)
+    edges = projected(edges, gain[...], weights)
+    middle = projected(rows[...], gain[...], weights)
+    sums = jnp.concatenate([edges[:width], middle, edges[width:]], axis=0)
     shape = (count_rows, channels)
     kind = lax.broadcasted_iota(jnp.int32, shape, 1) // GROUP % 4
     places = place[0] * count_rows + lax.broadcasted_iota(jnp.int32, shape, 0)
@@ -99,7 +104,7 @@
         lane = slice(k * lanes, (k + 1) * lanes)
         pieces.append((dot(centred[:, lane], maps[k]) * scale[:, lane]).astype(jnp.bfloat16))
     grouped = jnp.concatenate(pieces, axis=1)
-    for copy in copies:
+    for copy in later:
         copy.wait()
     out[...] = dot(grouped, out_rows[...]).astype(jnp.bfloat16)
 
@@ -107,35 +112,24 @@
 def mixer_half(first_batch, mixer_gain, shard, pair_maps, pool_scale):
     count_rows, width = first_batch.shape
     channels = pool_scale.shape[0]
+    low, high = neighbours(first_batch, 8)
     blocks = lax.all_gather(shard, TP)
     place = jnp.stack([lax.axis_index(ALL), jnp.int32(lax.axis_size(ALL))]).astype(jnp.int32)
-    held = [
-        pltpu.VMEM((channels, width), jnp.bfloat16),
-        pltpu.SemaphoreType.DMA((blocks.shape[0],)),
-    ]
-    cost = pl.CostEstimate(
-        flops=2 * count_rows * width * channels,
-        transcendentals=0,
-        bytes_accessed=4 * channels * width,
-    )
     whole = pl.BlockSpec()
-    pooled_in = pl.pallas_call(
-        project_body,
-        out_shape=jax.ShapeDtypeStruct((count_rows, channels), jnp.bfloat16),
-        in_specs=[whole, whole, in_place()],
-        scratch_shapes=held,
+    held = [(count_rows, width), low.shape, high.shape, (channels, width), (channels, width)]
+    return pl.pallas_call(
+        mixer_body,
+        out_shape=jax.ShapeDtypeStruct((count_rows, width), jnp.bfloat16),
+        in_specs=[in_scalars()] + [whole] * 3 + [in_place()] * 4,
+        scratch_shapes=[pltpu.VMEM(shape, jnp.bfloat16) for shape in held]
+        + [pltpu.SemaphoreType.DMA((n,)) for n in (3, blocks.shape[0], blocks.shape[0])],
         compiler_params=limit(59),
-        cost_estimate=cost,
-    )(first_batch, mixer_gain[None, :], blocks)
-    low, high = neighbours(pooled_in, 8)
-    return pl.pallas_call(
-        pool_body,
-        out_shape=jax.ShapeDtypeStruct((count_rows, width), jnp.bfloat16),
-        in_specs=[in_scalars()] + [whole] * 5 + [in_place()],
-        scratch_shapes=held,
-        compiler_params=limit(59),
-        cost_estimate=cost,
-    )(place, pooled_in, low, high, pair_maps, pool_scale[None, :], blocks)
+        cost_estimate=pl.CostEstimate(
+            flops=4 * count_rows * width * channels,
+            transcendentals=0,
+            bytes_accessed=8 * channels * width,
+        ),
+    )(place, mixer_gain[None, :], pair_maps, pool_scale[None, :], first_batch, low, high, blocks)
 
 
 def ranked(choice, experts):

time: 147 us -> 139 us (0.946)
  waiting for transfers between devices: 48.5 us -> 39.7 us
  starting transfers between devices: 42.5 us -> 45.1 us
  Pallas kernels: 17.1 us -> 15.5 us
    all_to_all x1, waiting for transfers between devices: 31.4 us -> 22.7 us  [expert_half(): returned = lax.all_to_all(leaving, ALL, 0, 0, tiled=True)]
    ppermute x1, starting transfers between devices: 2.1 us -> 6.2 us  [neighbours(): high = lax.ppermute(block[:width], ALL, backward)]
    pallas_call x2 -> x1, Pallas kernels: 8.23 us -> 6.61 us  [mixer_half(): pl.pallas_call(mixer_body, out_shape=jax.ShapeDtypeStruct((count_rows, wi...]
    ppermute x1, starting transfers between devices: 3.45 us -> 1.92 us  [neighbours(): low = lax.ppermute(block[block.shape[0] - width:], ALL, forward)]
  transfers between devices with their start and end apart: 8 -> 8, of which waited for: 3 -> 3; matrix products, arithmetic and copies ran while one was open for 2% -> 3% of each run, Pallas kernels for 4% -> 4%
where the time goes in v6:
time: 139 us
  starting transfers between devices  45.1 us (32%)
  waiting for transfers between devices  39.7 us (29%)
  blocking collectives  16.2 us (12%)
  Pallas kernels  15.5 us (11%)
  between operations  14.3 us (10%)
  local copies, waits for them, and re-layouts  5.01 us (4%)
  other arithmetic  2.83 us (2%)
    all_to_all x1, waiting for transfers between devices, expert_half(): returned = lax.all_to_all(leaving, ALL, 0, 0, tiled=True)  22.7 us
    all_to_all x1, waiting for transfers between devices, expert_half(): arrived = lax.all_to_all(outgoing, EP, 0, 0, tiled=True)  16.7 us
    all_gather x1, blocking collectives, expert_half(): whole = lax.all_gather(blended, TP)  16.2 us
    all_to_all x1, starting transfers between devices, expert_half(): returned = lax.all_to_all(leaving, ALL, 0, 0, tiled=True)  15.9 us
    all_to_all x1, starting transfers between devices, expert_half(): arrived = lax.all_to_all(outgoing, EP, 0, 0, tiled=True)  13.8 us
    pallas_call x1, Pallas kernels, mixer_half(): pl.pallas_call(mixer_body, out_shape=jax.ShapeDtypeStruct((count_rows, wi...  6.61 us
    ppermute x1, starting transfers between devices, neighbours(): high = lax.ppermute(block[:width], ALL, backward)  6.2 us
    pallas_call x1, Pallas kernels, expert_half(): pl.pallas_call(ffn_body, out_shape=jax.ShapeDtypeStruct(incoming.shape, j...  5.72 us
  transfers between devices with their start and end apart: 8, of which 3 were waited for; matrix products, arithmetic and copies ran while one was open for 3% of the time, Pallas kernels for 4%

profile of v6, /device:TPU:1, one launch (start us, length us, event | category | flops | bytes accessed | tf_op | source)
XLA Modules:
  0.0 138.9 jit_solution(3070546772056034231)
XLA Ops:
  7.2 2.8 %shard_map.140 = bf16[256,2048]{1,0:T(8,128)(2,1)} custom-call(s32[1]{0:T(128)} %bitcast.6.core, bf16[128,2048]{1,0:T(8,128)(2,1)} %rows_from.2, f32[1,2048]{1,0:T(1,128)} %bitcast.57, s32[2,128]{1,0:T(2,128)} %bitcast.45), custom_call_target="tpu_custom_call" | custom-call | flops 134217728 | bytes 1572864 | tf_op jit(solution)/shard_map/pallas_call | solution.py:251
  10.1 1.7 %pad_maximum_fusion = bf16[64,2048]{1,0:T(8,128)(2,1)} fusion(bf16[32,2048]{1,0:T(8,128)(2,1)} %param.18, bf16[32,2048]{1,0:T(8,128)(2,1)} %bitcast.56), kind=kLoop, calls=%fused_computation.1 | loop fusion | flops 524288 | bytes 524288 | tf_op jit(solution)/shard_map/concatenate | solution.py:270
  11.8 13.8 %all-to-all-start = ((bf16[32,8,2048]{2,1,0:T(8,128)(2,1)}), bf16[32,8,2048]{2,1,0:T(8,128)(2,1)}, u32[]{:S(2)}, u32[]{:S(2)}) async-start(bf16[32,8,2048]{2,1,0:T(8,128)(2,1)} %bitcast.50), calls=%async_computation | async-start | bytes 2097152 | tf_op jit(solution)/shard_map/all_to_all | solution.py:271
  25.6 2.9 %collective-permute-start.2 = (bf16[224,2048]{1,0:T(8,128)(2,1)S(1)}, bf16[224,2048]{1,0:T(8,128)(2,1)S(1)}, u32[]{:S(2)}, u32[]{:S(2)}) collective-permute-start(bf16[224,2048]{1,0:T(8,128)(2,1)S(1)} %bitcast.39), channel_id=1, source_target_pairs={{0,1},{1,0},{2,3},{3,2},{4,5},{5,4},{6,7},{7,6},{8,9},{9,8},{10,11... | collective-permute-start | bytes 2752520 | tf_op jit(solution)/shard_map/ppermute | solution.py:247
  28.5 1.9 %collective-permute-start.3 = (bf16[224,2048]{1,0:T(8,128)(2,1)S(1)}, bf16[224,2048]{1,0:T(8,128)(2,1)S(1)}, u32[]{:S(2)}, u32[]{:S(2)}) collective-permute-start(bf16[224,2048]{1,0:T(8,128)(2,1)S(1)} %bitcast.41), channel_id=1, source_target_pairs={{0,1},{1,0},{2,3},{3,2},{4,5},{5,4},{6,7},{7,6},{8,9},{9,8},{10,11... | collective-permute-start | bytes 2752520 | tf_op jit(solution)/shard_map/ppermute | solution.py:248
  30.5 2.4 %collective-permute-start.4 = (bf16[224,2048]{1,0:T(8,128)(2,1)S(1)}, bf16[224,2048]{1,0:T(8,128)(2,1)}, u32[]{:S(2)}, u32[]{:S(2)}) collective-permute-start(bf16[224,2048]{1,0:T(8,128)(2,1)S(1)} %bitcast.43), channel_id=1, source_target_pairs={{0,1},{1,0},{2,3},{3,2},{4,5},{5,4},{6,7},{7,6},{8,9},{9,8},{10,11... | collective-permute-start | bytes 2752520 | tf_op jit(solution)/shard_map/ppermute | solution.py:249
  32.9 0.9 copy-done.5
  33.8 1.0 copy-done.6
  34.8 0.3 collective-permute-done.4.refs_6_
  35.1 16.7 %all-to-all-done = bf16[32,8,2048]{2,1,0:T(8,128)(2,1)} async-done(((bf16[32,8,2048]{2,1,0:T(8,128)(2,1)}), bf16[32,8,2048]{2,1,0:T(8,128)(2,1)}, u32[]{:S(2)}, u32[]{:S(2)}) %all-to-all-start) | async-done | bytes 1048608 | tf_op jit(solution)/shard_map/all_to_all | solution.py:271
  51.8 5.7 %shard_map.143 = bf16[256,2048]{1,0:T(8,128)(2,1)} custom-call(bf16[256,2048]{1,0:T(8,128)(2,1)} %bitcast.13.refs_0_, bf16[224,2048]{1,0:T(8,128)(2,1)S(1)} %bitcast.40, bf16[224,2048]{1,0:T(8,128)(2,1)S(1)} %bitcast.42, bf16[224,2048]{1,0:T(8,128)(2,1)S(1)} %bitcast.44, bf16[224,2048]{1,0:T(8,128)(2,1)} %copy-done.5, bf16[224,2048]{1,0:T(8,128)(2,1)} %copy-done.6, ...), custom_call_target="tpu_custom_call" | custom-call | flops 1409286144 | bytes 7602176 | tf_op jit(solution)/shard_map/pallas_call | solution.py:274
  57.5 15.9 %all-to-all-start.1 = ((bf16[512,8,128]{2,1,0:T(8,128)(2,1)}), bf16[512,8,128]{2,1,0:T(8,128)(2,1)S(1)}, u32[]{:S(2)}, u32[]{:S(2)}) async-start(bf16[512,8,128]{2,1,0:T(8,128)(2,1)} %bitcast.51), calls=%async_computation.1 | async-start | bytes 2097152 | tf_op jit(solution)/shard_map/all_to_all | solution.py:293
  73.4 0.8 fusion.1
  74.2 6.2 %collective-permute-start.1 = (bf16[8,2048]{1,0:T(8,128)(2,1)S(1)}, bf16[8,2048]{1,0:T(8,128)(2,1)S(1)}, u32[]{:S(2)}, u32[]{:S(2)}) collective-permute-start(bf16[8,2048]{1,0:T(8,128)(2,1)S(1)} %get-tuple-element.8), channel_id=1, source_target_pairs={{1,0},{2,1},{3,2},{4,3},{5,4},{6,5},{7,6},{8,7},{9,8},{10,9},{11,1... | collective-permute-start | bytes 98312 | tf_op jit(solution)/shard_map/ppermute | solution.py:25
  80.4 1.9 %collective-permute-start = (bf16[8,2048]{1,0:T(8,128)(2,1)S(1)}, bf16[8,2048]{1,0:T(8,128)(2,1)S(1)}, u32[]{:S(2)}, u32[]{:S(2)}) collective-permute-start(bf16[8,2048]{1,0:T(8,128)(2,1)S(1)} %get-tuple-element.9), channel_id=1, source_target_pairs={{0,1},{1,2},{2,3},{3,4},{4,5},{5,6},{6,7},{7,8},{8,9},{9,10},{10,1... | collective-permute-start | bytes 98312 | tf_op jit(solution)/shard_map/ppermute | solution.py:24
  82.4 0.3 multiply_bitcast_fusion
  82.7 0.8 reshape.35.maps
  83.5 0.4 shard_map.142
  83.9 0.7 pad_add_fusion.place
  84.6 22.7 %all-to-all-done.1 = bf16[512,8,128]{2,1,0:T(8,128)(2,1)S(1)} async-done(((bf16[512,8,128]{2,1,0:T(8,128)(2,1)}), bf16[512,8,128]{2,1,0:T(8,128)(2,1)S(1)}, u32[]{:S(2)}, u32[]{:S(2)}) %all-to-all-start.1) | async-done | bytes 1048608 | tf_op jit(solution)/shard_map/all_to_all | solution.py:293
  107.7 16.2 %all-gather.1 = bf16[2048,128]{1,0:T(8,128)(2,1)S(1)} all-gather(bf16[128,128]{1,0:T(8,128)(2,1)S(1)} %fusion), channel_id=3, replica_groups=mesh['z'=8,'x'=4,'y'=8,'c'=2] {'y','c'}, dimensions={0}, use_global_device_ids=true | all-gather | bytes 557056 | tf_op jit(solution)/shard_map/all_gather | solution.py:308
  123.9 0.9 copy.18
  124.9 0.6 copy-done.8
  125.5 6.6 %shard_map.141 = bf16[128,2048]{1,0:T(8,128)(2,1)} custom-call(s32[2]{0:T(128)} %pad_add_fusion.place, f32[1,2048]{1,0:T(1,128)} %bitcast.58, bf16[4,128,128]{2,1,0:T(8,128)(2,1)} %reshape.35.maps, f32[1,512]{1,0:T(1,128)} %bitcast.59, bf16[128,2048]{1,0:T(8,128)(2,1)} %rows_from.3, bf16[8,2048]{1,0:T(8,128)(2,1)} %copy-done.9, bf16[8,2048]{1,0:T(8,128)(2,1)} %copy-done.8, ...), custom_call_target="tpu_custom_call" | custom-call | flops 536870912 | bytes 8388608 | tf_op jit(solution)/shard_map/pallas_call | solution.py:120
  (28 shorter events, 0.6 us)
Async XLA Ops:
  7.2 18.5 %copy-start = (bf16[1,2048,224]{1,2,0:T(8,128)(2,1)S(1)}, bf16[1,2048,224]{1,2,0:T(8,128)(2,1)}, u32[]{:S(2)}) copy-start(bf16[1,2048,224]{1,2,0:T(8,128)(2,1)} %param.23) | copy-start | bytes 2752516
  7.2 21.3 %copy-start.1 = (bf16[1,2048,224]{1,2,0:T(8,128)(2,1)S(1)}, bf16[1,2048,224]{1,2,0:T(8,128)(2,1)}, u32[]{:S(2)}) copy-start(bf16[1,2048,224]{1,2,0:T(8,128)(2,1)} %param.24) | copy-start | bytes 2752516
  7.2 23.3 %copy-start.2 = (bf16[1,224,2048]{2,1,0:T(8,128)(2,1)S(1)}, bf16[1,224,2048]{2,1,0:T(8,128)(2,1)}, u32[]{:S(2)}) copy-start(bf16[1,224,2048]{2,1,0:T(8,128)(2,1)} %param.25) | copy-start | bytes 2752516
  7.2 117.7 %all-gather.4.cloned.1.call-start = ((), (), s32[]{:S(2)}) async-start(), calls=%async_computation.2 | async-start | bytes 4456448 | tf_op jit(solution)/shard_map/all_gather | solution.py:116
  11.8 40.0 %all-to-all-start = ((bf16[32,8,2048]{2,1,0:T(8,128)(2,1)}), bf16[32,8,2048]{2,1,0:T(8,128)(2,1)}, u32[]{:S(2)}, u32[]{:S(2)}) async-start(bf16[32,8,2048]{2,1,0:T(8,128)(2,1)} %bitcast.50), calls=%async_computation | async-start | bytes 2097152 | tf_op jit(solution)/shard_map/all_to_all | solution.py:271
  25.6 7.2 %collective-permute-start.2 = (bf16[224,2048]{1,0:T(8,128)(2,1)S(1)}, bf16[224,2048]{1,0:T(8,128)(2,1)S(1)}, u32[]{:S(2)}, u32[]{:S(2)}) collective-permute-start(bf16[224,2048]{1,0:T(8,128)(2,1)S(1)} %bitcast.39), channel_id=1, source_target_pairs={{0,1},{1,0},{2,3},{3,2},{4,5},{5,4},{6,7},{7,6},{8,9},{9,8},{10,11... | collective-permute-start | bytes 2752520 | tf_op jit(solution)/shard_map/ppermute | solution.py:247
  28.5 4.4 %collective-permute-start.3 = (bf16[224,2048]{1,0:T(8,128)(2,1)S(1)}, bf16[224,2048]{1,0:T(8,128)(2,1)S(1)}, u32[]{:S(2)}, u32[]{:S(2)}) collective-permute-start(bf16[224,2048]{1,0:T(8,128)(2,1)S(1)} %bitcast.41), channel_id=1, source_target_pairs={{0,1},{1,0},{2,3},{3,2},{4,5},{5,4},{6,7},{7,6},{8,9},{9,8},{10,11... | collective-permute-start | bytes 2752520 | tf_op jit(solution)/shard_map/ppermute | solution.py:248
  30.5 4.6 %collective-permute-start.4 = (bf16[224,2048]{1,0:T(8,128)(2,1)S(1)}, bf16[224,2048]{1,0:T(8,128)(2,1)}, u32[]{:S(2)}, u32[]{:S(2)}) collective-permute-start(bf16[224,2048]{1,0:T(8,128)(2,1)S(1)} %bitcast.43), channel_id=1, source_target_pairs={{0,1},{1,0},{2,3},{3,2},{4,5},{5,4},{6,7},{7,6},{8,9},{9,8},{10,11... | collective-permute-start | bytes 2752520 | tf_op jit(solution)/shard_map/ppermute | solution.py:249
  32.9 0.9 copy-start.5
  33.8 1.0 copy-start.6
  51.8 30.6 %copy-start.7 = (bf16[8,64,64]{2,1,0:T(8,128)(2,1)S(1)}, bf16[8,64,64]{2,1,0:T(8,128)(2,1)}, u32[]{:S(2)}) copy-start(bf16[8,64,64]{2,1,0:T(8,128)(2,1)} %param.16) | copy-start | bytes 196612
  51.8 31.7 %copy-start.3 = (s32[128,2]{0,1:T(2,128)S(1)}, s32[128,2]{0,1:T(2,128)}, u32[]{:S(2)}) copy-start(s32[128,2]{0,1:T(2,128)} %param.21) | copy-start | bytes 3076
  51.8 31.7 %copy-start.4 = (f32[128,2]{0,1:T(2,128)S(1)}, f32[128,2]{0,1:T(2,128)}, u32[]{:S(2)}) copy-start(f32[128,2]{0,1:T(2,128)} %param.22) | copy-start | bytes 3076
  57.5 49.7 %all-to-all-start.1 = ((bf16[512,8,128]{2,1,0:T(8,128)(2,1)}), bf16[512,8,128]{2,1,0:T(8,128)(2,1)S(1)}, u32[]{:S(2)}, u32[]{:S(2)}) async-start(bf16[512,8,128]{2,1,0:T(8,128)(2,1)} %bitcast.51), calls=%async_computation.1 | async-start | bytes 2097152 | tf_op jit(solution)/shard_map/all_to_all | solution.py:293
  74.2 50.6 %collective-permute-start.1 = (bf16[8,2048]{1,0:T(8,128)(2,1)S(1)}, bf16[8,2048]{1,0:T(8,128)(2,1)S(1)}, u32[]{:S(2)}, u32[]{:S(2)}) collective-permute-start(bf16[8,2048]{1,0:T(8,128)(2,1)S(1)} %get-tuple-element.8), channel_id=1, source_target_pairs={{1,0},{2,1},{3,2},{4,3},{5,4},{6,5},{7,6},{8,7},{9,8},{10,9},{11,1... | collective-permute-start | bytes 98312 | tf_op jit(solution)/shard_map/ppermute | solution.py:25
  80.4 44.4 %collective-permute-start = (bf16[8,2048]{1,0:T(8,128)(2,1)S(1)}, bf16[8,2048]{1,0:T(8,128)(2,1)S(1)}, u32[]{:S(2)}, u32[]{:S(2)}) collective-permute-start(bf16[8,2048]{1,0:T(8,128)(2,1)S(1)} %get-tuple-element.9), channel_id=1, source_target_pairs={{0,1},{1,2},{2,3},{3,4},{4,5},{5,6},{6,7},{7,8},{8,9},{9,10},{10,1... | collective-permute-start | bytes 98312 | tf_op jit(solution)/shard_map/ppermute | solution.py:24
  124.8 0.6 copy-start.8
  124.9 0.6 copy-start.9
Sparse Core Ops, SparseCore 0:
  11.9 49.9 all-gather.3

commit v7 on v6

--- a/solution.py
+++ b/solution.py
@@ -153,15 +153,23 @@
     return dot(jnp.where(match, 1.0, 0.0).astype(jnp.bfloat16), values)
 
 
-def dispatch_body(core, rows_from, gain_from, choice_from, out, rows, gain, choice, done):
+def dispatch_body(core, rows_from, gain_from, choice_from, top, bottom, *refs):
+    out, joined, rows, gain, choice, result, done, left = refs
+    share = top.shape[0]
     copies = []
-    for k, (source, held) in enumerate(
-        ((choice_from, choice), (rows_from, rows), (gain_from, gain))
+    for k, (source, target) in enumerate(
+        (
+            (choice_from, choice),
+            (rows_from, rows),
+            (gain_from, gain),
+            (top, joined.at[pl.ds(0, share), :]),
+            (bottom, joined.at[pl.ds(share, share), :]),
+        )
     ):
-        copies.append(pltpu.make_async_copy(source, held, done.at[k]))
+        copies.append(pltpu.make_async_copy(source, target, done.at[k]))
         copies[-1].start()
     count = rows.shape[0]
-    slots = out.shape[0]
+    slots = result.shape[0]
     half = slots // EXPERTS
     slot = core[0] * half + lax.broadcasted_iota(jnp.int32, (slots, count), 0) % half
     copies[0].wait()
@@ -169,7 +177,17 @@
     spread = jnp.where(rank == slot.astype(jnp.float32), 1.0, 0.0).astype(jnp.bfloat16)
     copies[1].wait()
     copies[2].wait()
-    out[...] = dot(spread, norm(rows[...], gain[...])).astype(jnp.bfloat16)
+    normed = norm(rows[...], gain[...])
+    width = result.shape[1] // PARTS
+    leaving = []
+    for k in range(PARTS):
+        span = slice(k * width, (k + 1) * width)
+        result[:, span] = dot(spread, normed[:, span]).astype(jnp.bfloat16)
+        lanes = pl.ds(k * width, width)
+        leaving.append(pltpu.make_async_copy(result.at[:, lanes], out.at[:, lanes], left.at[k]))
+        leaving[-1].start()
+    for copy in copies[3:] + leaving:
+        copy.wait()
 
 
 def blend_body(choice, scores, out):
@@ -248,15 +266,23 @@
     up_far = lax.ppermute(up_own, "c", SWAP)
     down_far = lax.ppermute(down_own, "c", SWAP)
 
-    outgoing = pl.pallas_call(
+    joined_shape = (2 * mixer_out.shape[0], model_width)
+    sent_shape = (experts * half_slots, model_width)
+    outgoing, shard = pl.pallas_call(
         dispatch_body,
-        out_shape=jax.ShapeDtypeStruct((experts * half_slots, model_width), jnp.bfloat16),
-        in_specs=[in_scalars()] + [in_place()] * 3,
+        out_shape=(
+            jax.ShapeDtypeStruct(sent_shape, jnp.bfloat16),
+            jax.ShapeDtypeStruct(joined_shape, jnp.bfloat16),
+        ),
+        in_specs=[in_scalars()] + [in_place()] * 5,
+        out_specs=(in_place(), in_place()),
         scratch_shapes=[
             pltpu.VMEM(second_batch.shape, second_batch.dtype),
             pltpu.VMEM((1, model_width), jnp.float32),
             pltpu.VMEM((expert_choice.shape[1], row_count), jnp.int32),
-            pltpu.SemaphoreType.DMA((3,)),
+            pltpu.VMEM(sent_shape, jnp.bfloat16),
+            pltpu.SemaphoreType.DMA((5,)),
+            pltpu.SemaphoreType.DMA((PARTS,)),
         ],
         compiler_params=limit(61),
         cost_estimate=pl.CostEstimate(
@@ -264,10 +290,15 @@
             transcendentals=row_count,
             bytes_accessed=6 * second_batch.size,
         ),
-    )(core[None].astype(jnp.int32), second_batch, expert_gain[None, :], expert_choice.T)
+    )(
+        core[None].astype(jnp.int32),
+        second_batch,
+        expert_gain[None, :],
+        expert_choice.T,
+        mixer_in.T,
+        mixer_out,
+    )
     outgoing = outgoing.reshape(experts, half_slots, model_width)
-    mixer_in, mixer_out, outgoing = lax.optimization_barrier((mixer_in, mixer_out, outgoing))
-    shard = jnp.concatenate([mixer_in.T, mixer_out], axis=0)
     arrived = lax.all_to_all(outgoing, EP, 0, 0, tiled=True)
     incoming = arrived.reshape(experts * half_slots, model_width)
 
@@ -279,7 +310,7 @@
         scratch_shapes=[pltpu.VMEM(incoming.shape, jnp.bfloat16)]
         + [pltpu.VMEM(gate_own.shape, jnp.bfloat16)] * 6
         + [pltpu.VMEM(incoming.shape, jnp.bfloat16), pltpu.SemaphoreType.DMA((PARTS + 7,))],
-        compiler_params=limit(51),
+        compiler_params=limit(57),
         cost_estimate=pl.CostEstimate(
             flops=12 * incoming.size * gate_own.shape[0],
             transcendentals=2 * incoming.shape[0] * gate_own.shape[0],

time: 139 us -> 145 us (1.043)
  Pallas kernels: 15.5 us -> 22.1 us
  waiting for transfers between devices: 39.7 us -> 42.3 us
  other arithmetic: 2.83 us -> 1.08 us
    pallas_call x1, Pallas kernels: 2.82 us -> 9.13 us  [expert_half(): pl.pallas_call(dispatch_body, out_shape=(jax.ShapeDtypeStruct(sent_shape,...]
    ppermute x1, starting transfers between devices: 6.2 us -> 3.96 us  [neighbours(): high = lax.ppermute(block[:width], ALL, backward)]
    ppermute x1, waiting for transfers between devices: 0.3 us -> 2.17 us  [expert_half(): down_far = lax.ppermute(down_own, 'c', SWAP)]
    concatenate x1 -> x0, other arithmetic: 1.69 us -> none  [expert_half(): shard = jnp.concatenate([mixer_in.T, mixer_out], axis=0)]
    ppermute x1, starting transfers between devices: 1.92 us -> 3.53 us  [neighbours(): low = lax.ppermute(block[block.shape[0] - width:], ALL, forward)]
  transfers between devices with their start and end apart: 8 -> 8, of which waited for: 3 -> 4; matrix products, arithmetic and copies ran while one was open for 3% -> 3% of each run, Pallas kernels for 4% -> 4%
where the time goes in v7:
time: 145 us
  starting transfers between devices  44.3 us (31%)
  waiting for transfers between devices  42.3 us (29%)
  Pallas kernels  22.1 us (15%)
  blocking collectives  16.2 us (11%)
  between operations  14.2 us (10%)
  local copies, waits for them, and re-layouts  4.12 us (3%)
    all_to_all x1, waiting for transfers between devices, expert_half(): returned = lax.all_to_all(leaving, ALL, 0, 0, tiled=True)  23.3 us
    all_to_all x1, waiting for transfers between devices, expert_half(): arrived = lax.all_to_all(outgoing, EP, 0, 0, tiled=True)  16.6 us
    all_gather x1, blocking collectives, expert_half(): whole = lax.all_gather(blended, TP)  16.2 us
    all_to_all x1, starting transfers between devices, expert_half(): returned = lax.all_to_all(leaving, ALL, 0, 0, tiled=True)  15.9 us
    all_to_all x1, starting transfers between devices, expert_half(): arrived = lax.all_to_all(outgoing, EP, 0, 0, tiled=True)  13.7 us
    pallas_call x1, Pallas kernels, expert_half(): pl.pallas_call(dispatch_body, out_shape=(jax.ShapeDtypeStruct(sent_shape,...  9.13 us
    pallas_call x1, Pallas kernels, mixer_half(): pl.pallas_call(mixer_body, out_shape=jax.ShapeDtypeStruct((count_rows, wi...  6.61 us
    pallas_call x1, Pallas kernels, expert_half(): pl.pallas_call(ffn_body, out_shape=jax.ShapeDtypeStruct(incoming.shape, j...  5.95 us
  transfers between devices with their start and end apart: 8, of which 4 were waited for; matrix products, arithmetic and copies ran while one was open for 3% of the time, Pallas kernels for 4%

profile of v7, /device:TPU:1, one launch (start us, length us, event | category | flops | bytes accessed | tf_op | source)
XLA Modules:
  0.0 144.7 jit_solution(2386663400821297644)
XLA Ops:
  7.2 9.1 %shard_map.140 = (bf16[256,2048]{1,0:T(8,128)(2,1)}, bf16[64,2048]{1,0:T(8,128)(2,1)}) custom-call(s32[1]{0:T(128)} %bitcast.6.core, bf16[128,2048]{1,0:T(8,128)(2,1)} %rows_from.2, f32[1,2048]{1,0:T(1,128)} %bitcast.58, s32[2,128]{1,0:T(2,128)} %bitcast.39, bf16[32,2048]{1,0:T(8,128)(2,1)} %bitcast.57, bf16[32,2048]{1,0:T(8,128)(2,1)} %bottom.1), custom_call_target="tpu_custom_call" | custom-call | flops 134217728 | bytes 1572864 | tf_op jit(solution)/shard_map/pallas_call | solution.py:271
  16.4 13.7 %all-to-all-start = ((bf16[32,8,2048]{2,1,0:T(8,128)(2,1)}), bf16[32,8,2048]{2,1,0:T(8,128)(2,1)S(1)}, u32[]{:S(2)}, u32[]{:S(2)}) async-start(bf16[32,8,2048]{2,1,0:T(8,128)(2,1)} %bitcast.47), calls=%async_computation | async-start | bytes 2097152 | tf_op jit(solution)/shard_map/all_to_all | solution.py:302
  30.1 2.9 %collective-permute-start.2 = (bf16[224,2048]{1,0:T(8,128)(2,1)}, bf16[224,2048]{1,0:T(8,128)(2,1)S(1)}, u32[]{:S(2)}, u32[]{:S(2)}) collective-permute-start(bf16[224,2048]{1,0:T(8,128)(2,1)} %bitcast.48), channel_id=1, source_target_pairs={{0,1},{1,0},{2,3},{3,2},{4,5},{5,4},{6,7},{7,6},{8,9},{9,8},{10,11... | collective-permute-start | bytes 2752520 | tf_op jit(solution)/shard_map/ppermute | solution.py:265
  33.0 1.9 %collective-permute-start.3 = (bf16[224,2048]{1,0:T(8,128)(2,1)}, bf16[224,2048]{1,0:T(8,128)(2,1)S(1)}, u32[]{:S(2)}, u32[]{:S(2)}) collective-permute-start(bf16[224,2048]{1,0:T(8,128)(2,1)} %bitcast.50), channel_id=1, source_target_pairs={{0,1},{1,0},{2,3},{3,2},{4,5},{5,4},{6,7},{7,6},{8,9},{9,8},{10,11... | collective-permute-start | bytes 2752520 | tf_op jit(solution)/shard_map/ppermute | solution.py:266
  34.9 2.4 %collective-permute-start.4 = (bf16[224,2048]{1,0:T(8,128)(2,1)}, bf16[224,2048]{1,0:T(8,128)(2,1)}, u32[]{:S(2)}, u32[]{:S(2)}) collective-permute-start(bf16[224,2048]{1,0:T(8,128)(2,1)} %bitcast.52), channel_id=1, source_target_pairs={{0,1},{1,0},{2,3},{3,2},{4,5},{5,4},{6,7},{7,6},{8,9},{9,8},{10,11... | collective-permute-start | bytes 2752520 | tf_op jit(solution)/shard_map/ppermute | solution.py:267
  37.3 0.2 collective-permute-done.3.refs_5_
  37.6 2.2 %collective-permute-done.4.refs_6_ = bf16[224,2048]{1,0:T(8,128)(2,1)} collective-permute-done((bf16[224,2048]{1,0:T(8,128)(2,1)}, bf16[224,2048]{1,0:T(8,128)(2,1)}, u32[]{:S(2)}, u32[]{:S(2)}) %collective-permute-start.4) | collective-permute-done | bytes 917536 | tf_op jit(solution)/shard_map/ppermute | solution.py:267
  39.7 16.6 %all-to-all-done = bf16[32,8,2048]{2,1,0:T(8,128)(2,1)S(1)} async-done(((bf16[32,8,2048]{2,1,0:T(8,128)(2,1)}), bf16[32,8,2048]{2,1,0:T(8,128)(2,1)S(1)}, u32[]{:S(2)}, u32[]{:S(2)}) %all-to-all-start) | async-done | bytes 1048608 | tf_op jit(solution)/shard_map/all_to_all | solution.py:302
  56.3 1.0 copy-done.2
  57.3 6.0 %shard_map.143 = bf16[256,2048]{1,0:T(8,128)(2,1)} custom-call(bf16[256,2048]{1,0:T(8,128)(2,1)} %bitcast.45, bf16[224,2048]{1,0:T(8,128)(2,1)} %bitcast.49, bf16[224,2048]{1,0:T(8,128)(2,1)} %bitcast.51, bf16[224,2048]{1,0:T(8,128)(2,1)} %bitcast.53, bf16[224,2048]{1,0:T(8,128)(2,1)} %copy-done.3, bf16[224,2048]{1,0:T(8,128)(2,1)} %copy-done.4, ...), custom_call_target="tpu_custom_call" | custom-call | flops 1409286144 | bytes 7602176 | tf_op jit(solution)/shard_map/pallas_call | solution.py:305
  63.3 15.9 %all-to-all-start.1 = ((bf16[512,8,128]{2,1,0:T(8,128)(2,1)}), bf16[512,8,128]{2,1,0:T(8,128)(2,1)S(1)}, u32[]{:S(2)}, u32[]{:S(2)}) async-start(bf16[512,8,128]{2,1,0:T(8,128)(2,1)} %bitcast.44), calls=%async_computation.1 | async-start | bytes 2097152 | tf_op jit(solution)/shard_map/all_to_all | solution.py:324
  79.2 0.8 fusion.1
  80.0 3.5 %collective-permute-start = (bf16[8,2048]{1,0:T(8,128)(2,1)S(1)}, bf16[8,2048]{1,0:T(8,128)(2,1)S(1)}, u32[]{:S(2)}, u32[]{:S(2)}) collective-permute-start(bf16[8,2048]{1,0:T(8,128)(2,1)S(1)} %get-tuple-element.7), channel_id=1, source_target_pairs={{0,1},{1,2},{2,3},{3,4},{4,5},{5,6},{6,7},{7,8},{8,9},{9,10},{10,1... | collective-permute-start | bytes 98312 | tf_op jit(solution)/shard_map/ppermute | solution.py:24
  83.5 4.0 %collective-permute-start.1 = (bf16[8,2048]{1,0:T(8,128)(2,1)S(1)}, bf16[8,2048]{1,0:T(8,128)(2,1)S(1)}, u32[]{:S(2)}, u32[]{:S(2)}) collective-permute-start(bf16[8,2048]{1,0:T(8,128)(2,1)S(1)} %get-tuple-element.6), channel_id=1, source_target_pairs={{1,0},{2,1},{3,2},{4,3},{5,4},{6,5},{7,6},{8,7},{9,8},{10,9},{11,1... | collective-permute-start | bytes 98312 | tf_op jit(solution)/shard_map/ppermute | solution.py:25
  87.5 0.3 multiply_bitcast_fusion
  87.8 0.8 reshape.35.maps
  88.6 0.4 shard_map.142
  89.0 0.6 pad_add_fusion.place
  89.6 23.3 %all-to-all-done.1 = bf16[512,8,128]{2,1,0:T(8,128)(2,1)S(1)} async-done(((bf16[512,8,128]{2,1,0:T(8,128)(2,1)}), bf16[512,8,128]{2,1,0:T(8,128)(2,1)S(1)}, u32[]{:S(2)}, u32[]{:S(2)}) %all-to-all-start.1) | async-done | bytes 1048608 | tf_op jit(solution)/shard_map/all_to_all | solution.py:324
  113.1 0.3 fusion.2
  113.4 16.2 %all-gather.1 = bf16[2048,128]{1,0:T(8,128)(2,1)S(1)} all-gather(bf16[128,128]{1,0:T(8,128)(2,1)S(1)} %fusion), channel_id=3, replica_groups=mesh['z'=8,'x'=4,'y'=8,'c'=2] {'y','c'}, dimensions={0}, use_global_device_ids=true | all-gather | bytes 557056 | tf_op jit(solution)/shard_map/all_gather | solution.py:339
  129.6 0.9 copy.18
  130.6 0.6 copy-done.6
  131.2 6.6 %shard_map.141 = bf16[128,2048]{1,0:T(8,128)(2,1)} custom-call(s32[2]{0:T(128)} %pad_add_fusion.place, f32[1,2048]{1,0:T(1,128)} %bitcast.59, bf16[4,128,128]{2,1,0:T(8,128)(2,1)} %reshape.35.maps, f32[1,512]{1,0:T(1,128)} %bitcast.60, bf16[128,2048]{1,0:T(8,128)(2,1)} %rows_from.3, bf16[8,2048]{1,0:T(8,128)(2,1)} %copy-done.6, bf16[8,2048]{1,0:T(8,128)(2,1)} %copy-done.7, ...), custom_call_target="tpu_custom_call" | custom-call | flops 536870912 | bytes 8388608 | tf_op jit(solution)/shard_map/pallas_call | solution.py:120
  (23 shorter events, 0.3 us)
Async XLA Ops:
  7.2 123.5 %all-gather.4.cloned.1.call-start = ((), (), s32[]{:S(2)}) async-start(), calls=%async_computation.2 | async-start | bytes 4456448 | tf_op jit(solution)/shard_map/all_gather | solution.py:116
  16.4 39.9 %all-to-all-start = ((bf16[32,8,2048]{2,1,0:T(8,128)(2,1)}), bf16[32,8,2048]{2,1,0:T(8,128)(2,1)S(1)}, u32[]{:S(2)}, u32[]{:S(2)}) async-start(bf16[32,8,2048]{2,1,0:T(8,128)(2,1)} %bitcast.47), calls=%async_computation | async-start | bytes 2097152 | tf_op jit(solution)/shard_map/all_to_all | solution.py:302
  30.1 7.2 %collective-permute-start.2 = (bf16[224,2048]{1,0:T(8,128)(2,1)}, bf16[224,2048]{1,0:T(8,128)(2,1)S(1)}, u32[]{:S(2)}, u32[]{:S(2)}) collective-permute-start(bf16[224,2048]{1,0:T(8,128)(2,1)} %bitcast.48), channel_id=1, source_target_pairs={{0,1},{1,0},{2,3},{3,2},{4,5},{5,4},{6,7},{7,6},{8,9},{9,8},{10,11... | collective-permute-start | bytes 2752520 | tf_op jit(solution)/shard_map/ppermute | solution.py:265
  33.0 4.6 %collective-permute-start.3 = (bf16[224,2048]{1,0:T(8,128)(2,1)}, bf16[224,2048]{1,0:T(8,128)(2,1)S(1)}, u32[]{:S(2)}, u32[]{:S(2)}) collective-permute-start(bf16[224,2048]{1,0:T(8,128)(2,1)} %bitcast.50), channel_id=1, source_target_pairs={{0,1},{1,0},{2,3},{3,2},{4,5},{5,4},{6,7},{7,6},{8,9},{9,8},{10,11... | collective-permute-start | bytes 2752520 | tf_op jit(solution)/shard_map/ppermute | solution.py:266
  34.9 4.8 %collective-permute-start.4 = (bf16[224,2048]{1,0:T(8,128)(2,1)}, bf16[224,2048]{1,0:T(8,128)(2,1)}, u32[]{:S(2)}, u32[]{:S(2)}) collective-permute-start(bf16[224,2048]{1,0:T(8,128)(2,1)} %bitcast.52), channel_id=1, source_target_pairs={{0,1},{1,0},{2,3},{3,2},{4,5},{5,4},{6,7},{7,6},{8,9},{9,8},{10,11... | collective-permute-start | bytes 2752520 | tf_op jit(solution)/shard_map/ppermute | solution.py:267
  37.3 19.0 %copy-start.3 = (bf16[224,2048]{1,0:T(8,128)(2,1)}, bf16[224,2048]{1,0:T(8,128)(2,1)S(1)}, u32[]{:S(2)}) copy-start(bf16[224,2048]{1,0:T(8,128)(2,1)S(1)} %collective-permute-done.2.refs_4_) | copy-start | bytes 2752516
  37.6 18.7 %copy-start.4 = (bf16[224,2048]{1,0:T(8,128)(2,1)}, bf16[224,2048]{1,0:T(8,128)(2,1)S(1)}, u32[]{:S(2)}) copy-start(bf16[224,2048]{1,0:T(8,128)(2,1)S(1)} %collective-permute-done.3.refs_5_) | copy-start | bytes 2752516
  56.3 1.0 copy-start.2
  57.3 30.2 %copy-start.5 = (bf16[8,64,64]{2,1,0:T(8,128)(2,1)S(1)}, bf16[8,64,64]{2,1,0:T(8,128)(2,1)}, u32[]{:S(2)}) copy-start(bf16[8,64,64]{2,1,0:T(8,128)(2,1)} %param.16) | copy-start | bytes 196612
  57.3 31.3 %copy-start = (s32[128,2]{0,1:T(2,128)S(1)}, s32[128,2]{0,1:T(2,128)}, u32[]{:S(2)}) copy-start(s32[128,2]{0,1:T(2,128)} %param.21) | copy-start | bytes 3076
  57.3 31.3 %copy-start.1 = (f32[128,2]{0,1:T(2,128)S(1)}, f32[128,2]{0,1:T(2,128)}, u32[]{:S(2)}) copy-start(f32[128,2]{0,1:T(2,128)} %param.22) | copy-start | bytes 3076
  63.3 49.7 %all-to-all-start.1 = ((bf16[512,8,128]{2,1,0:T(8,128)(2,1)}), bf16[512,8,128]{2,1,0:T(8,128)(2,1)S(1)}, u32[]{:S(2)}, u32[]{:S(2)}) async-start(bf16[512,8,128]{2,1,0:T(8,128)(2,1)} %bitcast.44), calls=%async_computation.1 | async-start | bytes 2097152 | tf_op jit(solution)/shard_map/all_to_all | solution.py:324
  80.0 50.6 %collective-permute-start = (bf16[8,2048]{1,0:T(8,128)(2,1)S(1)}, bf16[8,2048]{1,0:T(8,128)(2,1)S(1)}, u32[]{:S(2)}, u32[]{:S(2)}) collective-permute-start(bf16[8,2048]{1,0:T(8,128)(2,1)S(1)} %get-tuple-element.7), channel_id=1, source_target_pairs={{0,1},{1,2},{2,3},{3,4},{4,5},{5,6},{6,7},{7,8},{8,9},{9,10},{10,1... | collective-permute-start | bytes 98312 | tf_op jit(solution)/shard_map/ppermute | solution.py:24
  83.5 47.1 %collective-permute-start.1 = (bf16[8,2048]{1,0:T(8,128)(2,1)S(1)}, bf16[8,2048]{1,0:T(8,128)(2,1)S(1)}, u32[]{:S(2)}, u32[]{:S(2)}) collective-permute-start(bf16[8,2048]{1,0:T(8,128)(2,1)S(1)} %get-tuple-element.6), channel_id=1, source_target_pairs={{1,0},{2,1},{3,2},{4,3},{5,4},{6,5},{7,6},{8,7},{9,8},{10,9},{11,1... | collective-permute-start | bytes 98312 | tf_op jit(solution)/shard_map/ppermute | solution.py:25
  130.6 0.6 copy-start.6
  130.6 0.6 copy-start.7
Sparse Core Ops, SparseCore 0:
  16.5 50.3 all-gather.3

commit v8 on v6

--- a/solution.py
+++ b/solution.py
@@ -153,7 +153,8 @@
     return dot(jnp.where(match, 1.0, 0.0).astype(jnp.bfloat16), values)
 
 
-def dispatch_body(core, rows_from, gain_from, choice_from, out, rows, gain, choice, done):
+def dispatch_body(core, rows_from, gain_from, choice_from, out, *held):
+    rows, gain, choice, result, done, left = held
     copies = []
     for k, (source, held) in enumerate(
         ((choice_from, choice), (rows_from, rows), (gain_from, gain))
@@ -161,7 +162,7 @@
         copies.append(pltpu.make_async_copy(source, held, done.at[k]))
         copies[-1].start()
     count = rows.shape[0]
-    slots = out.shape[0]
+    slots = result.shape[0]
     half = slots // EXPERTS
     slot = core[0] * half + lax.broadcasted_iota(jnp.int32, (slots, count), 0) % half
     copies[0].wait()
@@ -169,7 +170,17 @@
     spread = jnp.where(rank == slot.astype(jnp.float32), 1.0, 0.0).astype(jnp.bfloat16)
     copies[1].wait()
     copies[2].wait()
-    out[...] = dot(spread, norm(rows[...], gain[...])).astype(jnp.bfloat16)
+    normed = norm(rows[...], gain[...])
+    width = result.shape[1] // PARTS
+    leaving = []
+    for k in range(PARTS):
+        span = slice(k * width, (k + 1) * width)
+        result[:, span] = dot(spread, normed[:, span]).astype(jnp.bfloat16)
+        lanes = pl.ds(k * width, width)
+        leaving.append(pltpu.make_async_copy(result.at[:, lanes], out.at[:, lanes], left.at[k]))
+        leaving[-1].start()
+    for copy in leaving:
+        copy.wait()
 
 
 def blend_body(choice, scores, out):
@@ -256,8 +267,11 @@
             pltpu.VMEM(second_batch.shape, second_batch.dtype),
             pltpu.VMEM((1, model_width), jnp.float32),
             pltpu.VMEM((expert_choice.shape[1], row_count), jnp.int32),
+            pltpu.VMEM((experts * half_slots, model_width), jnp.bfloat16),
             pltpu.SemaphoreType.DMA((3,)),
+            pltpu.SemaphoreType.DMA((PARTS,)),
         ],
+        out_specs=in_place(),
         compiler_params=limit(61),
         cost_estimate=pl.CostEstimate(
             flops=2 * experts * half_slots * second_batch.size,

time: 139 us -> 139 us (level)
  no operation moved by 1% of the time
where the time goes in v8:
time: 139 us
  starting transfers between devices  45.1 us (32%)
  waiting for transfers between devices  39.7 us (29%)
  blocking collectives  16.2 us (12%)
  Pallas kernels  15.4 us (11%)
  between operations  14.3 us (10%)
  local copies, waits for them, and re-layouts  5.01 us (4%)
  other arithmetic  2.83 us (2%)
    all_to_all x1, waiting for transfers between devices, expert_half(): returned = lax.all_to_all(leaving, ALL, 0, 0, tiled=True)  22.7 us
    all_to_all x1, waiting for transfers between devices, expert_half(): arrived = lax.all_to_all(outgoing, EP, 0, 0, tiled=True)  16.7 us
    all_gather x1, blocking collectives, expert_half(): whole = lax.all_gather(blended, TP)  16.2 us
    all_to_all x1, starting transfers between devices, expert_half(): returned = lax.all_to_all(leaving, ALL, 0, 0, tiled=True)  15.9 us
    all_to_all x1, starting transfers between devices, expert_half(): arrived = lax.all_to_all(outgoing, EP, 0, 0, tiled=True)  13.8 us
    pallas_call x1, Pallas kernels, mixer_half(): pl.pallas_call(mixer_body, out_shape=jax.ShapeDtypeStruct((count_rows, wi...  6.62 us
    ppermute x1, starting transfers between devices, neighbours(): high = lax.ppermute(block[:width], ALL, backward)  6.2 us
    pallas_call x1, Pallas kernels, expert_half(): pl.pallas_call(ffn_body, out_shape=jax.ShapeDtypeStruct(incoming.shape, j...  5.72 us
  transfers between devices with their start and end apart: 8, of which 3 were waited for; matrix products, arithmetic and copies ran while one was open for 3% of the time, Pallas kernels for 4%

profile of v8, /device:TPU:1, one launch (start us, length us, event | category | flops | bytes accessed | tf_op | source)
XLA Modules:
  0.0 138.8 jit_solution(3109012270664012508)
XLA Ops:
  7.2 2.7 %shard_map.140 = bf16[256,2048]{1,0:T(8,128)(2,1)} custom-call(s32[1]{0:T(128)} %bitcast.6.core, bf16[128,2048]{1,0:T(8,128)(2,1)} %rows_from.2, f32[1,2048]{1,0:T(1,128)} %bitcast.57, s32[2,128]{1,0:T(2,128)} %bitcast.45), custom_call_target="tpu_custom_call" | custom-call | flops 134217728 | bytes 1572864 | tf_op jit(solution)/shard_map/pallas_call | solution.py:262
  9.9 1.7 %pad_maximum_fusion = bf16[64,2048]{1,0:T(8,128)(2,1)} fusion(bf16[32,2048]{1,0:T(8,128)(2,1)} %param.18, bf16[32,2048]{1,0:T(8,128)(2,1)} %bitcast.56), kind=kLoop, calls=%fused_computation.1 | loop fusion | flops 524288 | bytes 524288 | tf_op jit(solution)/shard_map/concatenate | solution.py:284
  11.6 13.8 %all-to-all-start = ((bf16[32,8,2048]{2,1,0:T(8,128)(2,1)}), bf16[32,8,2048]{2,1,0:T(8,128)(2,1)}, u32[]{:S(2)}, u32[]{:S(2)}) async-start(bf16[32,8,2048]{2,1,0:T(8,128)(2,1)} %bitcast.50), calls=%async_computation | async-start | bytes 2097152 | tf_op jit(solution)/shard_map/all_to_all | solution.py:285
  25.5 2.9 %collective-permute-start.2 = (bf16[224,2048]{1,0:T(8,128)(2,1)S(1)}, bf16[224,2048]{1,0:T(8,128)(2,1)S(1)}, u32[]{:S(2)}, u32[]{:S(2)}) collective-permute-start(bf16[224,2048]{1,0:T(8,128)(2,1)S(1)} %bitcast.39), channel_id=1, source_target_pairs={{0,1},{1,0},{2,3},{3,2},{4,5},{5,4},{6,7},{7,6},{8,9},{9,8},{10,11... | collective-permute-start | bytes 2752520 | tf_op jit(solution)/shard_map/ppermute | solution.py:258
  28.4 1.9 %collective-permute-start.3 = (bf16[224,2048]{1,0:T(8,128)(2,1)S(1)}, bf16[224,2048]{1,0:T(8,128)(2,1)S(1)}, u32[]{:S(2)}, u32[]{:S(2)}) collective-permute-start(bf16[224,2048]{1,0:T(8,128)(2,1)S(1)} %bitcast.41), channel_id=1, source_target_pairs={{0,1},{1,0},{2,3},{3,2},{4,5},{5,4},{6,7},{7,6},{8,9},{9,8},{10,11... | collective-permute-start | bytes 2752520 | tf_op jit(solution)/shard_map/ppermute | solution.py:259
  30.3 2.4 %collective-permute-start.4 = (bf16[224,2048]{1,0:T(8,128)(2,1)S(1)}, bf16[224,2048]{1,0:T(8,128)(2,1)}, u32[]{:S(2)}, u32[]{:S(2)}) collective-permute-start(bf16[224,2048]{1,0:T(8,128)(2,1)S(1)} %bitcast.43), channel_id=1, source_target_pairs={{0,1},{1,0},{2,3},{3,2},{4,5},{5,4},{6,7},{7,6},{8,9},{9,8},{10,11... | collective-permute-start | bytes 2752520 | tf_op jit(solution)/shard_map/ppermute | solution.py:260
  32.8 0.9 copy-done.5
  33.7 1.0 copy-done.6
  34.6 0.3 collective-permute-done.4.refs_6_
  34.9 16.7 %all-to-all-done = bf16[32,8,2048]{2,1,0:T(8,128)(2,1)} async-done(((bf16[32,8,2048]{2,1,0:T(8,128)(2,1)}), bf16[32,8,2048]{2,1,0:T(8,128)(2,1)}, u32[]{:S(2)}, u32[]{:S(2)}) %all-to-all-start) | async-done | bytes 1048608 | tf_op jit(solution)/shard_map/all_to_all | solution.py:285
  51.7 5.7 %shard_map.143 = bf16[256,2048]{1,0:T(8,128)(2,1)} custom-call(bf16[256,2048]{1,0:T(8,128)(2,1)} %bitcast.13.refs_0_, bf16[224,2048]{1,0:T(8,128)(2,1)S(1)} %bitcast.40, bf16[224,2048]{1,0:T(8,128)(2,1)S(1)} %bitcast.42, bf16[224,2048]{1,0:T(8,128)(2,1)S(1)} %bitcast.44, bf16[224,2048]{1,0:T(8,128)(2,1)} %copy-done.5, bf16[224,2048]{1,0:T(8,128)(2,1)} %copy-done.6, ...), custom_call_target="tpu_custom_call" | custom-call | flops 1409286144 | bytes 7602176 | tf_op jit(solution)/shard_map/pallas_call | solution.py:288
  57.4 15.9 %all-to-all-start.1 = ((bf16[512,8,128]{2,1,0:T(8,128)(2,1)}), bf16[512,8,128]{2,1,0:T(8,128)(2,1)S(1)}, u32[]{:S(2)}, u32[]{:S(2)}) async-start(bf16[512,8,128]{2,1,0:T(8,128)(2,1)} %bitcast.51), calls=%async_computation.1 | async-start | bytes 2097152 | tf_op jit(solution)/shard_map/all_to_all | solution.py:307
  73.3 0.8 fusion.1
  74.1 6.2 %collective-permute-start.1 = (bf16[8,2048]{1,0:T(8,128)(2,1)S(1)}, bf16[8,2048]{1,0:T(8,128)(2,1)S(1)}, u32[]{:S(2)}, u32[]{:S(2)}) collective-permute-start(bf16[8,2048]{1,0:T(8,128)(2,1)S(1)} %get-tuple-element.8), channel_id=1, source_target_pairs={{1,0},{2,1},{3,2},{4,3},{5,4},{6,5},{7,6},{8,7},{9,8},{10,9},{11,1... | collective-permute-start | bytes 98312 | tf_op jit(solution)/shard_map/ppermute | solution.py:25
  80.3 1.9 %collective-permute-start = (bf16[8,2048]{1,0:T(8,128)(2,1)S(1)}, bf16[8,2048]{1,0:T(8,128)(2,1)S(1)}, u32[]{:S(2)}, u32[]{:S(2)}) collective-permute-start(bf16[8,2048]{1,0:T(8,128)(2,1)S(1)} %get-tuple-element.9), channel_id=1, source_target_pairs={{0,1},{1,2},{2,3},{3,4},{4,5},{5,6},{6,7},{7,8},{8,9},{9,10},{10,1... | collective-permute-start | bytes 98312 | tf_op jit(solution)/shard_map/ppermute | solution.py:24
  82.2 0.3 multiply_bitcast_fusion
  82.5 0.8 reshape.35.maps
  83.4 0.4 shard_map.142
  83.8 0.7 pad_add_fusion.place
  84.4 22.7 %all-to-all-done.1 = bf16[512,8,128]{2,1,0:T(8,128)(2,1)S(1)} async-done(((bf16[512,8,128]{2,1,0:T(8,128)(2,1)}), bf16[512,8,128]{2,1,0:T(8,128)(2,1)S(1)}, u32[]{:S(2)}, u32[]{:S(2)}) %all-to-all-start.1) | async-done | bytes 1048608 | tf_op jit(solution)/shard_map/all_to_all | solution.py:307
  107.5 16.2 %all-gather.1 = bf16[2048,128]{1,0:T(8,128)(2,1)S(1)} all-gather(bf16[128,128]{1,0:T(8,128)(2,1)S(1)} %fusion), channel_id=3, replica_groups=mesh['z'=8,'x'=4,'y'=8,'c'=2] {'y','c'}, dimensions={0}, use_global_device_ids=true | all-gather | bytes 557056 | tf_op jit(solution)/shard_map/all_gather | solution.py:322
  123.8 0.9 copy.18
  124.7 0.6 copy-done.8
  125.3 6.6 %shard_map.141 = bf16[128,2048]{1,0:T(8,128)(2,1)} custom-call(s32[2]{0:T(128)} %pad_add_fusion.place, f32[1,2048]{1,0:T(1,128)} %bitcast.58, bf16[4,128,128]{2,1,0:T(8,128)(2,1)} %reshape.35.maps, f32[1,512]{1,0:T(1,128)} %bitcast.59, bf16[128,2048]{1,0:T(8,128)(2,1)} %rows_from.3, bf16[8,2048]{1,0:T(8,128)(2,1)} %copy-done.9, bf16[8,2048]{1,0:T(8,128)(2,1)} %copy-done.8, ...), custom_call_target="tpu_custom_call" | custom-call | flops 536870912 | bytes 8388608 | tf_op jit(solution)/shard_map/pallas_call | solution.py:120
  (28 shorter events, 0.6 us)
Async XLA Ops:
  7.2 18.3 %copy-start = (bf16[1,2048,224]{1,2,0:T(8,128)(2,1)S(1)}, bf16[1,2048,224]{1,2,0:T(8,128)(2,1)}, u32[]{:S(2)}) copy-start(bf16[1,2048,224]{1,2,0:T(8,128)(2,1)} %param.23) | copy-start | bytes 2752516
  7.2 21.2 %copy-start.1 = (bf16[1,2048,224]{1,2,0:T(8,128)(2,1)S(1)}, bf16[1,2048,224]{1,2,0:T(8,128)(2,1)}, u32[]{:S(2)}) copy-start(bf16[1,2048,224]{1,2,0:T(8,128)(2,1)} %param.24) | copy-start | bytes 2752516
  7.2 23.1 %copy-start.2 = (bf16[1,224,2048]{2,1,0:T(8,128)(2,1)S(1)}, bf16[1,224,2048]{2,1,0:T(8,128)(2,1)}, u32[]{:S(2)}) copy-start(bf16[1,224,2048]{2,1,0:T(8,128)(2,1)} %param.25) | copy-start | bytes 2752516
  7.2 117.5 %all-gather.4.cloned.1.call-start = ((), (), s32[]{:S(2)}) async-start(), calls=%async_computation.2 | async-start | bytes 4456448 | tf_op jit(solution)/shard_map/all_gather | solution.py:116
  11.6 40.0 %all-to-all-start = ((bf16[32,8,2048]{2,1,0:T(8,128)(2,1)}), bf16[32,8,2048]{2,1,0:T(8,128)(2,1)}, u32[]{:S(2)}, u32[]{:S(2)}) async-start(bf16[32,8,2048]{2,1,0:T(8,128)(2,1)} %bitcast.50), calls=%async_computation | async-start | bytes 2097152 | tf_op jit(solution)/shard_map/all_to_all | solution.py:285
  25.5 7.2 %collective-permute-start.2 = (bf16[224,2048]{1,0:T(8,128)(2,1)S(1)}, bf16[224,2048]{1,0:T(8,128)(2,1)S(1)}, u32[]{:S(2)}, u32[]{:S(2)}) collective-permute-start(bf16[224,2048]{1,0:T(8,128)(2,1)S(1)} %bitcast.39), channel_id=1, source_target_pairs={{0,1},{1,0},{2,3},{3,2},{4,5},{5,4},{6,7},{7,6},{8,9},{9,8},{10,11... | collective-permute-start | bytes 2752520 | tf_op jit(solution)/shard_map/ppermute | solution.py:258
  28.4 4.4 %collective-permute-start.3 = (bf16[224,2048]{1,0:T(8,128)(2,1)S(1)}, bf16[224,2048]{1,0:T(8,128)(2,1)S(1)}, u32[]{:S(2)}, u32[]{:S(2)}) collective-permute-start(bf16[224,2048]{1,0:T(8,128)(2,1)S(1)} %bitcast.41), channel_id=1, source_target_pairs={{0,1},{1,0},{2,3},{3,2},{4,5},{5,4},{6,7},{7,6},{8,9},{9,8},{10,11... | collective-permute-start | bytes 2752520 | tf_op jit(solution)/shard_map/ppermute | solution.py:259
  30.3 4.6 %collective-permute-start.4 = (bf16[224,2048]{1,0:T(8,128)(2,1)S(1)}, bf16[224,2048]{1,0:T(8,128)(2,1)}, u32[]{:S(2)}, u32[]{:S(2)}) collective-permute-start(bf16[224,2048]{1,0:T(8,128)(2,1)S(1)} %bitcast.43), channel_id=1, source_target_pairs={{0,1},{1,0},{2,3},{3,2},{4,5},{5,4},{6,7},{7,6},{8,9},{9,8},{10,11... | collective-permute-start | bytes 2752520 | tf_op jit(solution)/shard_map/ppermute | solution.py:260
  32.7 0.9 copy-start.5
  33.7 1.0 copy-start.6
  51.7 30.6 %copy-start.7 = (bf16[8,64,64]{2,1,0:T(8,128)(2,1)S(1)}, bf16[8,64,64]{2,1,0:T(8,128)(2,1)}, u32[]{:S(2)}) copy-start(bf16[8,64,64]{2,1,0:T(8,128)(2,1)} %param.16) | copy-start | bytes 196612
  51.7 31.7 %copy-start.3 = (s32[128,2]{0,1:T(2,128)S(1)}, s32[128,2]{0,1:T(2,128)}, u32[]{:S(2)}) copy-start(s32[128,2]{0,1:T(2,128)} %param.21) | copy-start | bytes 3076
  51.7 31.7 %copy-start.4 = (f32[128,2]{0,1:T(2,128)S(1)}, f32[128,2]{0,1:T(2,128)}, u32[]{:S(2)}) copy-start(f32[128,2]{0,1:T(2,128)} %param.22) | copy-start | bytes 3076
  57.4 49.7 %all-to-all-start.1 = ((bf16[512,8,128]{2,1,0:T(8,128)(2,1)}), bf16[512,8,128]{2,1,0:T(8,128)(2,1)S(1)}, u32[]{:S(2)}, u32[]{:S(2)}) async-start(bf16[512,8,128]{2,1,0:T(8,128)(2,1)} %bitcast.51), calls=%async_computation.1 | async-start | bytes 2097152 | tf_op jit(solution)/shard_map/all_to_all | solution.py:307
  74.1 50.6 %collective-permute-start.1 = (bf16[8,2048]{1,0:T(8,128)(2,1)S(1)}, bf16[8,2048]{1,0:T(8,128)(2,1)S(1)}, u32[]{:S(2)}, u32[]{:S(2)}) collective-permute-start(bf16[8,2048]{1,0:T(8,128)(2,1)S(1)} %get-tuple-element.8), channel_id=1, source_target_pairs={{1,0},{2,1},{3,2},{4,3},{5,4},{6,5},{7,6},{8,7},{9,8},{10,9},{11,1... | collective-permute-start | bytes 98312 | tf_op jit(solution)/shard_map/ppermute | solution.py:25
  80.3 44.4 %collective-permute-start = (bf16[8,2048]{1,0:T(8,128)(2,1)S(1)}, bf16[8,2048]{1,0:T(8,128)(2,1)S(1)}, u32[]{:S(2)}, u32[]{:S(2)}) collective-permute-start(bf16[8,2048]{1,0:T(8,128)(2,1)S(1)} %get-tuple-element.9), channel_id=1, source_target_pairs={{0,1},{1,2},{2,3},{3,4},{4,5},{5,6},{6,7},{7,8},{8,9},{9,10},{10,1... | collective-permute-start | bytes 98312 | tf_op jit(solution)/shard_map/ppermute | solution.py:24
  124.7 0.6 copy-start.8
  124.7 0.6 copy-start.9
Sparse Core Ops, SparseCore 0:
  11.7 49.9 all-gather.3
